TPU v7x, 512 devices: a whole 4x8x8 slice. The times are simulated.
512 devices in a mesh: dp: 4 (over x), kv: 64 (over z, y), tp: 2 (over core).
Axes of the slice: x: 4, y: 8, z: 8, core: 2. Of those that a mesh axis runs over, the one named last changes fastest.
Arguments:
- tokens: bfloat16 [64, 16, 2048], P('dp', None, ('kv', 'tp')), may hold values from -190 to 190
- gain_in: float32 [2048], P(('kv', 'tp')), may hold values from 0.1 to 1.9
- w_qdown: bfloat16 [2048, 512], P(('kv', 'tp')), may hold values from -0.125 to 0.125
- w_kvdown: bfloat16 [2048, 256], P(('kv', 'tp')), may hold values from -0.125 to 0.125
- w_ropek: bfloat16 [2048, 32], replicated, may hold values from -0.125 to 0.125
- gain_qlat: float32 [512], replicated, may hold values from 0.1 to 1.9
- gain_kvlat: float32 [256], replicated, may hold values from 0.1 to 1.9
- w_qup: bfloat16 [512, 16, 96], P(None, 'tp'), may hold values from -0.25 to 0.25
- gain_q: float32 [96], replicated, may hold values from 0.4 to 20
- w_ukey: bfloat16 [256, 16, 64], P(None, 'tp'), may hold values from -0.75 to 0.75
- w_uval: bfloat16 [256, 16, 128], P(None, 'tp'), may hold values from -0.375 to 0.375
- w_out: bfloat16 [2048, 2048], P('tp', 'kv'), may hold values from -2.5 to 2.5
- gain_out: float32 [2048], P(('kv', 'tp')), may hold values from 0.1 to 1.9
- cache_lat: bfloat16 [64, 16384, 256], P('dp', 'kv'), may hold values from -6 to 6
- cache_rope: bfloat16 [64, 32, 16384], P('dp', None, 'kv'), may hold values from -6 to 6
- parents: int32 [64, 16], P('dp'), may hold values from -1 to 14, as said below
- lengths: int32 [64], P('dp'), may hold values from 8192 to 16352
- accepted: int32 [64], P('dp'), may hold values from 0 to 16
Outputs:
- attn_out: bfloat16 [64, 16, 2048], P('dp', None, ('kv', 'tp'))
- lat_cache_out: bfloat16 [64, 16384, 256], P('dp', 'kv')
- rope_cache_out: bfloat16 [64, 32, 16384], P('dp', None, 'kv')
Inputs may be any that keep to these rules, and one draw needn't show every extreme that they name: `parents`: proposal j's parent is -1 (the last accepted token) or a proposal before j. Rows 0 .. lengths + accepted - 1 of a sequence's cache hold its past; the 16 positions after them lie inside the cache.
All inputs are finite; a program needn't handle non-finite values.
Results may differ from a plain program's by a relative error of at most 0.0102.
The roundings to bfloat16 on the way count: a program that leaves them out, or rounds other values in their place, can miss the bound.
Values may be sent and summed in bfloat16 or wider, within the bound.
No kernel may reach another device: no remote copies, remote signals or barrier semaphores. Data moves between devices by JAX's collectives and lax.ppermute only.
A program may use at most 64 MiB of HBM per device.

v0:
```python
import functools
import math

import jax
import jax.numpy as jnp
from jax import lax
from jax.sharding import Mesh
from jax.sharding import PartitionSpec as P

KV_TP = ("kv_0", "kv_1", "tp")
KV = ("kv_0", "kv_1")


epsilon = 1e-06


def cut_along(shard, dim, count):
    dims = shard.shape
    parts = shard.reshape(*dims[:dim], count, dims[dim] // count, *dims[dim + 1 :])
    return jnp.moveaxis(parts, dim, 0)


def sum_at_owner(shard, axis, dim):
    parts = cut_along(shard, dim, lax.axis_size(axis))
    arrived = lax.all_to_all(parts, axis, split_axis=0, concat_axis=0, tiled=True)
    return arrived.sum(axis=0)


def sum_in_two_steps(shard, axes, dim):
    far, near = axes
    parts = cut_along(shard, dim, lax.axis_size(far))
    nearer = sum_at_owner(parts, near, dim + 1)
    arrived = lax.all_to_all(nearer, far, split_axis=0, concat_axis=0, tiled=True)
    return arrived.sum(axis=0)


def sent_together(arrays, axis, dim, along):
    widths = [math.prod(a.shape[along:]) for a in arrays]
    both = jnp.concatenate(
        [a.reshape(*a.shape[:along], w) for a, w in zip(arrays, widths)], axis=along
    )
    result = sum_in_two_steps(both, axis, dim)
    parts = jnp.split(result, [sum(widths[:k]) for k in range(1, len(widths))], axis=along)
    return tuple(
        (b.reshape(*result.shape[:along], *a.shape[along:]) for a, b in zip(arrays, parts))
    )


def in_one_piece(arrays, axis, dim, along):
    ends, at = ([], 0)
    for a in arrays[:-1]:
        at += a.shape[along]
        ends.append(at)
    both = jnp.concatenate(arrays, axis=along)
    return tuple(jnp.split(lax.all_gather(both, axis, axis=dim, tiled=True), ends, axis=along))


def by_axis(shard, axes):
    return functools.reduce(lax.pmax, axes, shard)


def padded_to(lines, count):
    spare = -lines.shape[0] % count
    if not spare:
        return lines
    return jnp.concatenate([lines, jnp.zeros((spare, *lines.shape[1:]), lines.dtype)])


def from_everyone(shard, axis):
    count = lax.axis_size(axis)
    return lax.all_to_all(
        jnp.broadcast_to(shard[None], (count, *shard.shape)), axis, 0, 0, tiled=True
    )


def in_order(parts, dim):
    parts = jnp.moveaxis(parts, 0, dim)
    dims = parts.shape
    return parts.reshape(*dims[:dim], dims[dim] * dims[dim + 1], *dims[dim + 2 :])


def gathered_copies(shard, axis, dim):
    parts = from_everyone(shard, axis)
    return in_order(parts, dim)


def nested_sum(shard, axes):
    own = sum_at_owner(padded_to(shard, lax.axis_size(axes)), axes, 0)
    whole = gathered_copies(own, axes, 0)
    return whole[: len(shard)].reshape(shard.shape)


def together(arrays, axis):
    ravelled, at, gathered = (jnp.concatenate([a.reshape(-1) for a in arrays]), 0, [])
    total = nested_sum(ravelled, axis)
    for a in arrays:
        gathered.append(total[at : at + a.size].reshape(a.shape))
        at += a.size
    return tuple(gathered)


def of_everyone(shard, axis):
    return from_everyone(shard, axis).sum(axis=0)


def over_axes(shard, axes):
    far, near = axes
    nearer = of_everyone(shard, near)
    return of_everyone(nearer, far)


def normed(values, gain_vec):
    return (
        values * lax.rsqrt(jnp.mean(values * values, axis=-1, keepdims=True) + epsilon) * gain_vec
    )


def rope_angles(position, half_dim):
    frequency = 10000.0 ** (-(jnp.arange(half_dim, dtype=jnp.float32) * 2.0) / (2 * half_dim))
    return position.astype(jnp.float32)[..., None] * frequency


def ancestry(parents):
    proposals = parents.shape[-1]
    parent_link = (parents[..., :, None] == jnp.arange(proposals, dtype=jnp.int32)).astype(
        jnp.float32
    )
    identity = jnp.broadcast_to(jnp.eye(proposals, dtype=jnp.float32), parent_link.shape)

    def extend(iteration, state_pair):
        reaches, current = state_pair
        current = jnp.einsum("sij,sjk->sik", current, parent_link, precision=lax.Precision.HIGHEST)
        return (reaches + current, current)

    reaches, current = lax.fori_loop(0, proposals - 1, extend, (identity, identity))
    depths = (jnp.sum(reaches, axis=-1) - 1.0).astype(jnp.int32)
    return (reaches, depths)


def latents(summed, squares, full_width, gain_qlat, gain_kvlat):
    qrank = gain_qlat.shape[0]
    kvrank = gain_kvlat.shape[0]
    scaled_rows = summed * lax.rsqrt(squares / full_width + epsilon)[:, None]
    query_latent = normed(scaled_rows[:, :qrank], gain_qlat).astype(jnp.bfloat16)
    new_latent = normed(scaled_rows[:, qrank : qrank + kvrank], gain_kvlat).astype(jnp.bfloat16)
    new_rope = scaled_rows[:, qrank + kvrank :].astype(jnp.bfloat16)
    return (query_latent, new_latent, new_rope)


def apply_values(numer_rows, value_map):
    return jnp.einsum("...hk,khv->...hv", numer_rows, value_map, precision=lax.Precision.HIGHEST)


def local(
    tokens,
    gain_in,
    w_qdown,
    w_kvdown,
    w_ropek,
    gain_qlat,
    gain_kvlat,
    w_qup,
    gain_q,
    w_ukey,
    w_uval,
    w_out,
    gain_out,
    cache_lat,
    cache_rope,
    parents,
    lengths,
    accepted,
):
    seq_count, proposals, local_width = tokens.shape
    full_width = local_width * lax.axis_size(KV_TP)
    tok_rows = tokens.astype(jnp.float32).reshape(seq_count * proposals, local_width)
    scaled = (tok_rows * gain_in).astype(jnp.bfloat16)
    squares = jnp.sum(tok_rows * tok_rows, axis=-1)
    rope_rows = lax.dynamic_slice_in_dim(
        w_ropek, lax.axis_index(KV_TP) * local_width, local_width, 0
    )
    joined = jnp.concatenate([w_qdown, w_kvdown, rope_rows], axis=1)
    partial_rows = jnp.dot(scaled, joined, preferred_element_type=jnp.float32)
    summed, total_squares = sent_together((partial_rows, squares), (("kv_0", "kv_1"), "tp"), 0, 1)
    share_query, share_latent, share_rope = latents(
        summed, total_squares, full_width, gain_qlat, gain_kvlat
    )
    query_latent, new_latent, new_rope = in_one_piece(
        (share_query, share_latent, share_rope), KV_TP, 0, 1
    )
    qrank = w_qup.shape[0]
    heads_here = w_qup.shape[1]
    qkhead = w_qup.shape[2]
    kvrank = w_ukey.shape[0]
    nope_dim = w_ukey.shape[2]
    vhead = w_uval.shape[2]
    rope_dim = cache_rope.shape[1]
    half_dim = rope_dim // 2
    reaches, depths = ancestry(parents)
    starts = lengths + accepted
    query_pos = starts[:, None] + depths
    queries = jnp.dot(
        query_latent, w_qup.reshape(qrank, heads_here * qkhead), preferred_element_type=jnp.float32
    )
    queries = normed(queries.reshape(seq_count, proposals, heads_here, qkhead), gain_q)
    query_nope = queries[..., :nope_dim].astype(jnp.bfloat16)
    angles = rope_angles(query_pos, half_dim)[:, :, None, :]
    cosine = jnp.cos(angles)
    sines = jnp.sin(angles)
    lower_half = queries[..., nope_dim : nope_dim + half_dim]
    upper_half = queries[..., nope_dim + half_dim :]
    query_rot = jnp.concatenate(
        [lower_half * cosine - upper_half * sines, upper_half * cosine + lower_half * sines],
        axis=-1,
    ).astype(jnp.bfloat16)
    query_lat = jnp.einsum(
        "sihn,khn->sihk", query_nope, w_ukey, preferred_element_type=jnp.float32
    ).astype(jnp.bfloat16)
    pos_count = cache_lat.shape[1]
    slots = lax.axis_index(KV) * pos_count + jnp.arange(pos_count, dtype=jnp.int32)
    offset = slots[None, :] - starts[:, None]
    inside = (offset >= 0) & (offset < proposals)
    matches = offset[:, :, None] == jnp.arange(proposals, dtype=jnp.int32)
    selector = matches.astype(jnp.bfloat16)
    new_latent = new_latent.reshape(seq_count, proposals, kvrank)
    new_rope = new_rope.reshape(seq_count, proposals, rope_dim)
    placed = jnp.einsum(
        "spj,sjk->spk", selector, new_latent, preferred_element_type=jnp.float32
    ).astype(jnp.bfloat16)
    lat_out = jnp.where(inside[:, :, None], placed, cache_lat)
    placed_rope = jnp.einsum(
        "spj,sjr->srp", selector, new_rope, preferred_element_type=jnp.float32
    ).astype(jnp.bfloat16)
    rope_out = jnp.where(inside[:, None, :], placed_rope, cache_rope)
    key_pos = jnp.where(
        inside,
        starts[:, None] + jnp.sum(jnp.where(matches, depths[:, None, :], 0), axis=-1),
        slots[None, :],
    )
    ancestor = jnp.einsum(
        "sij,spj->sip", reaches, matches.astype(jnp.float32), precision=lax.Precision.HIGHEST
    )
    visible = (offset < 0)[:, None, :] | (ancestor > 0.5)
    key_angles = jnp.swapaxes(rope_angles(key_pos, half_dim), 1, 2)
    key_cos = jnp.cos(key_angles)
    key_sin = jnp.sin(key_angles)
    rope32 = rope_out.astype(jnp.float32)
    key_low = rope32[:, :half_dim, :]
    key_high = rope32[:, half_dim:, :]
    key_rot = jnp.concatenate(
        [key_low * key_cos - key_high * key_sin, key_high * key_cos + key_low * key_sin], axis=1
    ).astype(jnp.bfloat16)
    scores = (
        jnp.einsum("sihk,spk->sihp", query_lat, lat_out, preferred_element_type=jnp.float32)
        + jnp.einsum("sihr,srp->sihp", query_rot, key_rot, preferred_element_type=jnp.float32)
    ) * qkhead ** (-0.5)
    masked = jnp.where(visible[:, :, None, :], scores, -jnp.inf)
    row_max = by_axis(jnp.max(masked, axis=-1), KV)
    weights32 = jnp.exp(masked - row_max[..., None])
    denominator = jnp.sum(weights32, axis=-1)
    weights = weights32.astype(jnp.bfloat16)
    numerator = jnp.einsum("sihp,spk->sihk", weights, lat_out, preferred_element_type=jnp.float32)
    value_map = w_uval.astype(jnp.float32)
    numer_values = apply_values(numerator, value_map)
    values_all, denom_all = together((numer_values, denominator), KV)
    head_out = (values_all / denom_all[..., None]).astype(jnp.bfloat16)
    head_rows = head_out.reshape(seq_count * proposals, heads_here * vhead)
    partial_out = jnp.dot(head_rows, w_out, preferred_element_type=jnp.float32).reshape(
        seq_count, proposals, w_out.shape[1]
    )
    mixed = sum_at_owner(partial_out, "tp", 2)
    local_squares = jnp.sum(mixed * mixed, axis=-1)
    norm_total = over_axes(local_squares, (("kv_0", "kv_1"), "tp"))
    result = (mixed * lax.rsqrt(norm_total / full_width + epsilon)[..., None] * gain_out).astype(
        jnp.bfloat16
    )
    return (result, lat_out, rope_out)


def solution(mesh):
    torus = Mesh(
        mesh.devices.reshape(mesh.shape["dp"], 8, 8, mesh.shape["tp"]), ("dp", "kv_0", "kv_1", "tp")
    )
    return jax.shard_map(
        local,
        mesh=torus,
        in_specs=(
            P("dp", None, KV_TP),
            P(KV_TP),
            P(KV_TP, None),
            P(KV_TP, None),
            P(),
            P(),
            P(),
            P(None, "tp", None),
            P(),
            P(None, "tp", None),
            P(None, "tp", None),
            P("tp", KV),
            P(KV_TP),
            P("dp", KV, None),
            P("dp", None, KV),
            P("dp", None),
            P("dp"),
            P("dp"),
        ),
        out_specs=(P("dp", None, KV_TP), P("dp", KV, None), P("dp", None, KV)),
        check_vma=False,
    )
```

profile of v0, /device:TPU:4, one launch (start us, length us, event | category | flops | bytes accessed | tf_op | source)
XLA Modules:
  0.0 272.6 jit_solution(1491793479865517452)
XLA Ops:
  1.6 1.0 multiply_reduce_fusion.2
  4.5 1.1 fusion.37
  5.8 4.5 %all_to_all.40 = f32[2,64,2,801]{3,1,2,0:T(8,128)S(1)} all-to-all(f32[2,64,2,801]{3,1,2,0:T(8,128)S(1)} %maximum_bitcast_fusion), channel_id=1, replica_groups=mesh['dp'=4,'kv_0'=8,'kv_1'=8,'tp'=2] {'tp'}, dimensions={0} | all-to-all | bytes 1640448 | tf_op jit(solution)/shard_map/all_to_all | solution.py:25
  10.4 1.1 copy.75
  11.5 16.6 %all-to-all-start.1 = ((f32[64,2,801]{2,1,0:T(2,128)}), f32[64,2,801]{2,1,0:T(2,128)S(1)}, u32[]{:S(2)}, u32[]{:S(2)}) async-start(f32[64,2,801]{2,1,0:T(2,128)} %copy.75), calls=%async_computation.1 | async-start | bytes 917504 | tf_op jit(solution)/shard_map/all_to_all | solution.py:33
  28.4 5.6 %while.13 = (s32[]{:T(128)}, f32[16,16,16]{2,1,0:T(8,128)S(1)}, f32[16,16,16]{2,1,0:T(8,128)S(1)}, s32[16,16]{1,0:T(8,128)S(1)}, s32[]{:T(128)}) while((s32[]{:T(128)}, f32[16,16,16]{2,1,0:T(8,128)S(1)}, f32[16,16,16]{2,1,0:T(8,128)S(1)}, s32[16,16]{1,0:T(8,128)S(1)}, s32[]{:T(128)}) %tuple.39), condition=%wide.region_1.0_spmd.clone, body=%wide.region_0.0_spmd.clone.sunk | while | flops 798722 | bytes 99389 | solution.py:135
  35.3 11.5 %all-to-all-done.1 = f32[64,2,801]{2,1,0:T(2,128)S(1)} async-done(((f32[64,2,801]{2,1,0:T(2,128)}), f32[64,2,801]{2,1,0:T(2,128)S(1)}, u32[]{:S(2)}, u32[]{:S(2)}) %all-to-all-start.1) | async-done | bytes 410144 | tf_op jit(solution)/shard_map/all_to_all | solution.py:33
  47.7 48.4 %all-gather = bf16[128,2,800]{2,1,0:T(2,128)(2,1)S(1)} all-gather(bf16[1,2,800]{2,1,0:T(2,128)(2,1)S(1)} %maximum_bitcast_fusion.5), channel_id=1, replica_groups=mesh['dp'=4,'kv_0'=8,'kv_1'=8,'tp'=2] {'kv_0','kv_1','tp'}, dimensions={0}, use_global_device_ids=true | all-gather | bytes 412800 | tf_op jit(solution)/shard_map/all_gather | solution.py:55
  99.6 1.4 convert_select_fusion
  102.2 1.0 fusion.51
  103.2 1.1 fusion.28
  104.4 2.0 fusion.52
  106.4 30.2 %pmax.14 = f32[16,16,8]{2,1,0:T(8,128)S(1)} all-reduce(f32[16,16,8]{2,1,0:T(8,128)S(1)} %get-tuple-element.61), channel_id=1, replica_groups=mesh['dp'=4,'kv_0'=8,'kv_1'=8,'tp'=2] {'kv_0'}, use_global_device_ids=true, to_apply=%region_11.12 | all-reduce | flops 2048 | bytes 16384 | tf_op jit(solution)/shard_map/pmax | solution.py:59
  136.6 29.4 %pmax.15 = f32[16,16,8]{2,1,0:T(8,128)S(1)} all-reduce(f32[16,16,8]{2,1,0:T(8,128)S(1)} %pmax.14), channel_id=1, replica_groups=mesh['dp'=4,'kv_0'=8,'kv_1'=8,'tp'=2] {'kv_1'}, use_global_device_ids=true, to_apply=%region_12.13 | all-reduce | flops 2048 | bytes 16384 | tf_op jit(solution)/shard_map/pmax | solution.py:59
  166.1 2.3 fusion.10
  169.4 1.1 convolution_bitcast_fusion
  171.3 1.4 all_to_all.27
  172.8 27.8 %all_to_all.41 = f32[64,1,4128]{2,1,0:T(1,128)S(1)} all-to-all(f32[64,1,4128]{2,1,0:T(1,128)S(1)} %all_to_all.27), channel_id=1, replica_groups=mesh['dp'=4,'kv_0'=8,'kv_1'=8,'tp'=2] {'kv_0','kv_1'}, dimensions={0} | all-to-all | bytes 2113536 | tf_op jit(solution)/shard_map/all_to_all | solution.py:25
  201.8 26.4 %all_to_all.42 = f32[64,1,4128]{2,1,0:T(1,128)S(1)} all-to-all(f32[64,1,4128]{2,1,0:T(1,128)S(1)} %broadcast_in_dim.63), channel_id=1, replica_groups=mesh['dp'=4,'kv_0'=8,'kv_1'=8,'tp'=2] {'kv_0','kv_1'}, dimensions={0} | all-to-all | bytes 2113536 | tf_op jit(solution)/shard_map/all_to_all | solution.py:71
  228.2 2.6 reduce.3
  230.8 8.3 %slice.44 = f32[2064,16,8,1]{2,1,0,3:T(8,128)} reshape(f32[64,4128]{1,0:T(8,128)S(1)} %reduce.3) | data formatting | bytes 2113536 | tf_op jit(solution)/shard_map/slice | solution.py:97
  242.1 3.7 %all_to_all.43 = f32[2,1,4096]{2,1,0:T(1,128)S(1)} all-to-all(f32[2,1,4096]{2,1,0:T(1,128)S(1)} %reshape.334), channel_id=1, replica_groups=mesh['dp'=4,'kv_0'=8,'kv_1'=8,'tp'=2] {'tp'}, dimensions={0} | all-to-all | bytes 65536 | tf_op jit(solution)/shard_map/all_to_all | solution.py:25
  247.5 3.7 %all_to_all.44 = f32[2,1,256]{2,1,0:T(1,128)S(1)} all-to-all(f32[2,1,256]{2,1,0:T(1,128)S(1)} %reshape.336), channel_id=1, replica_groups=mesh['dp'=4,'kv_0'=8,'kv_1'=8,'tp'=2] {'tp'}, dimensions={0} | all-to-all | bytes 4096 | tf_op jit(solution)/shard_map/all_to_all | solution.py:71
  252.2 18.5 %all_to_all.45 = f32[64,1,256]{2,1,0:T(1,128)S(1)} all-to-all(f32[64,1,256]{2,1,0:T(1,128)S(1)} %reshape.338), channel_id=1, replica_groups=mesh['dp'=4,'kv_0'=8,'kv_1'=8,'tp'=2] {'kv_0','kv_1'}, dimensions={0} | all-to-all | bytes 131072 | tf_op jit(solution)/shard_map/all_to_all | solution.py:71
  (137 shorter events, 25.7 us)
Async XLA Ops:
  0.6 95.8 %copy-start = (bf16[512,8,96]{0,2,1:T(8,128)(2,1)S(1)}, bf16[512,8,96]{0,2,1:T(8,128)(2,1)}, u32[]{:S(2)}) copy-start(bf16[512,8,96]{0,2,1:T(8,128)(2,1)} %param.27) | copy-start | bytes 2359300
  5.8 22.3 %copy-start.13 = (s32[16]{0:T(128)S(1)}, s32[16]{0:T(128)}, u32[]{:S(2)}) copy-start(s32[16]{0:T(128)} %param.36) | copy-start | bytes 196
  5.8 22.3 %copy-start.14 = (s32[16]{0:T(128)S(1)}, s32[16]{0:T(128)}, u32[]{:S(2)}) copy-start(s32[16]{0:T(128)} %param.37) | copy-start | bytes 196
  10.3 18.1 %copy-start.7 = (s32[16,16]{1,0:T(8,128)S(1)}, s32[16,16]{1,0:T(8,128)}, u32[]{:S(2)}) copy-start(s32[16,16]{1,0:T(8,128)} %param.35) | copy-start | bytes 3076
  11.5 35.3 %all-to-all-start.1 = ((f32[64,2,801]{2,1,0:T(2,128)}), f32[64,2,801]{2,1,0:T(2,128)S(1)}, u32[]{:S(2)}, u32[]{:S(2)}) async-start(f32[64,2,801]{2,1,0:T(2,128)} %copy.75), calls=%async_computation.1 | async-start | bytes 917504 | tf_op jit(solution)/shard_map/all_to_all | solution.py:33
  28.4 19.2 %copy-start.8 = (f32[512]{0:T(512)S(1)}, f32[512]{0:T(512)}, u32[]{:S(2)}) copy-start(f32[512]{0:T(512)} %param.25) | copy-start | bytes 6148
  28.4 19.2 %copy-start.9 = (f32[256]{0:T(256)S(1)}, f32[256]{0:T(256)}, u32[]{:S(2)}) copy-start(f32[256]{0:T(256)} %param.26) | copy-start | bytes 3076
  96.1 1.1 copy-start.10
  96.4 1.0 copy-start.3
  96.5 1.1 copy-start.5
  98.0 1.6 copy-start.2
  98.0 1.6 slice-start
  101.0 67.4 %copy-start.1 = (bf16[16,256,256]{2,1,0:T(8,128)(2,1)}, bf16[16,256,256]{2,1,0:T(8,128)(2,1)S(1)}, u32[]{:S(2)}) copy-start(bf16[16,256,256]{2,1,0:T(8,128)(2,1)S(1)} %convert_select_fusion) | copy-start | bytes 6291460
  101.0 0.9 slice-start.1
  101.0 1.2 copy-start.6
  168.4 1.0 copy-start.4
  240.8 0.8 copy-start.12
  241.9 29.9 %copy-start.11 = (f32[16]{0:T(128)S(1)}, f32[16]{0:T(128)}, u32[]{:S(2)}) copy-start(f32[16]{0:T(128)} %param.32) | copy-start | bytes 196
where the time goes:
time: 273 us
  blocking collectives  193 us (71%)
  local copies, waits for them, and re-layouts  21.1 us (8%)
  starting transfers between devices  16.6 us (6%)
  matrix products  14.6 us (5%)
  other arithmetic  14.4 us (5%)
  waiting for transfers between devices  11.5 us (4%)
    pmax x2, blocking collectives, by_axis(): return functools.reduce(lax.pmax, axes, shard)  59.7 us
    all_to_all x3, blocking collectives, from_everyone(): lax.all_to_all(jnp.broadcast_to(shard[None], (count, *shard.shape)), axis...  48.6 us
    all_gather x1, blocking collectives, in_one_piece(): lax.all_gather(both, axis, axis=dim, tiled=True)  48.4 us
    all_to_all x3, blocking collectives, sum_at_owner(): lax.all_to_all(parts, axis, split_axis=0, concat_axis=0, tiled=True)  36 us
    all_to_all x1, starting transfers between devices, sum_in_two_steps(): lax.all_to_all(nearer, far, split_axis=0, concat_axis=0, tiled=True)  16.6 us
    all_to_all x1, waiting for transfers between devices, sum_in_two_steps(): lax.all_to_all(nearer, far, split_axis=0, concat_axis=0, tiled=True)  11.5 us
    slice x1, local copies, waits for them, and re-layouts, together(): gathered.append(total[at:at + a.size].reshape(a.shape))  8.31 us
  transfers between devices with their start and end apart: 1, of which 1 were waited for; matrix products, arithmetic and copies ran while one was open for 2% of the time, Pallas kernels for 0%

commit v1 on v0

v1 whole, which is shorter than its diff:
```python
import jax
import jax.numpy as jnp
from jax import lax
from jax.sharding import Mesh
from jax.sharding import PartitionSpec as P

KV_TP = ("kv_0", "kv_1", "tp")
KV = ("kv_0", "kv_1")

epsilon = 1e-06
F32 = jnp.float32
BF16 = jnp.bfloat16


def exchange(parts, axes):
    return lax.all_to_all(parts, axes, split_axis=0, concat_axis=0, tiled=True)


def from_everyone(shard, axes):
    return exchange(jnp.broadcast_to(shard[None], (lax.axis_size(axes), *shard.shape)), axes)


def bf16_terms(values, count):
    terms = []
    for _ in range(count):
        term = lax.reduce_precision(values, 8, 7)
        terms.append(term.astype(BF16))
        values = values - term
    return terms


def normed(values, gain_vec):
    return (
        values * lax.rsqrt(jnp.mean(values * values, axis=-1, keepdims=True) + epsilon) * gain_vec
    )


def rope_angles(position, half_dim):
    frequency = 10000.0 ** (-(jnp.arange(half_dim, dtype=jnp.float32) * 2.0) / (2 * half_dim))
    return position.astype(jnp.float32)[..., None] * frequency


def ancestry(parents):
    proposals = parents.shape[-1]
    step = (parents[..., :, None] == jnp.arange(proposals, dtype=jnp.int32)).astype(BF16)
    reaches = step + jnp.eye(proposals, dtype=BF16)
    covered = 2
    while covered < proposals:
        step = jnp.einsum("sij,sjk->sik", step, step, preferred_element_type=F32).astype(BF16)
        reaches = reaches + jnp.einsum(
            "sij,sjk->sik", reaches, step, preferred_element_type=F32
        ).astype(BF16)
        covered *= 2
    reaches = reaches.astype(F32)
    depths = (jnp.sum(reaches, axis=-1) - 1.0).astype(jnp.int32)
    return (reaches, depths)


def local(
    tokens,
    gain_in,
    w_qdown,
    w_kvdown,
    w_ropek,
    gain_qlat,
    gain_kvlat,
    w_qup,
    gain_q,
    w_ukey,
    w_uval,
    w_out,
    gain_out,
    cache_lat,
    cache_rope,
    parents,
    lengths,
    accepted,
):
    seq_count, proposals, local_width = tokens.shape
    rows = seq_count * proposals
    owners = lax.axis_size(KV)
    full_width = local_width * lax.axis_size(KV_TP)
    qrank, heads_here, qkhead = w_qup.shape
    kvrank, _, nope_dim = w_ukey.shape
    vhead = w_uval.shape[2]
    rope_dim = cache_rope.shape[1]
    half_dim = rope_dim // 2
    width = qrank + kvrank + rope_dim

    rope_rows = lax.dynamic_slice_in_dim(
        w_ropek, lax.axis_index(KV_TP) * local_width, local_width, 0
    )
    joined = jnp.concatenate([w_qdown, w_kvdown, rope_rows], axis=1)
    half = rows // lax.axis_size("tp")
    pair_tokens, pair_gain, pair_weights = lax.all_gather(
        (tokens.reshape(rows, local_width), gain_in[None], joined), "tp"
    )
    pair_tokens = lax.dynamic_slice_in_dim(pair_tokens, lax.axis_index("tp") * half, half, 1)
    tok_rows = pair_tokens.astype(F32)
    scaled = (tok_rows * pair_gain).astype(BF16)
    squares = jnp.sum(tok_rows * tok_rows, axis=(0, 2))
    partial_rows = jnp.einsum("crd,cdk->rk", scaled, pair_weights, preferred_element_type=F32)
    sent = jnp.concatenate([partial_rows, squares[:, None]], axis=1)
    arrived = exchange(sent.reshape(owners, half // owners, width + 1), KV)
    summed = arrived.sum(axis=0)
    latent_rows = summed[:, :width] * lax.rsqrt(summed[:, width] / full_width + epsilon)[:, None]
    share = jnp.concatenate(
        [
            normed(latent_rows[:, :qrank], gain_qlat).astype(BF16),
            normed(latent_rows[:, qrank : qrank + kvrank], gain_kvlat).astype(BF16),
            latent_rows[:, qrank + kvrank :].astype(BF16),
        ],
        axis=1,
    )
    everyone = from_everyone(share, KV).reshape(half, width)
    everyone = lax.all_gather(everyone, "tp", axis=0, tiled=True)
    query_latent = everyone[:, :qrank]
    new_latent = everyone[:, qrank : qrank + kvrank]
    new_rope = everyone[:, qrank + kvrank :]
    reaches, depths = ancestry(parents)
    starts = lengths + accepted
    query_pos = starts[:, None] + depths
    queries = jnp.dot(
        query_latent, w_qup.reshape(qrank, heads_here * qkhead), preferred_element_type=jnp.float32
    )
    queries = normed(queries.reshape(seq_count, proposals, heads_here, qkhead), gain_q)
    query_nope = queries[..., :nope_dim].astype(jnp.bfloat16)
    angles = rope_angles(query_pos, half_dim)[:, :, None, :]
    cosine = jnp.cos(angles)
    sines = jnp.sin(angles)
    lower_half = queries[..., nope_dim : nope_dim + half_dim]
    upper_half = queries[..., nope_dim + half_dim :]
    query_rot = jnp.concatenate(
        [lower_half * cosine - upper_half * sines, upper_half * cosine + lower_half * sines],
        axis=-1,
    ).astype(jnp.bfloat16)
    query_lat = jnp.einsum(
        "sihn,khn->sihk", query_nope, w_ukey, preferred_element_type=jnp.float32
    ).astype(jnp.bfloat16)
    pos_count = cache_lat.shape[1]
    slots = lax.axis_index(KV) * pos_count + jnp.arange(pos_count, dtype=jnp.int32)
    offset = slots[None, :] - starts[:, None]
    inside = (offset >= 0) & (offset < proposals)
    matches = offset[:, :, None] == jnp.arange(proposals, dtype=jnp.int32)
    selector = matches.astype(jnp.bfloat16)
    new_latent = new_latent.reshape(seq_count, proposals, kvrank)
    new_rope = new_rope.reshape(seq_count, proposals, rope_dim)
    placed = jnp.einsum(
        "spj,sjk->spk", selector, new_latent, preferred_element_type=jnp.float32
    ).astype(jnp.bfloat16)
    lat_out = jnp.where(inside[:, :, None], placed, cache_lat)
    placed_rope = jnp.einsum(
        "spj,sjr->srp", selector, new_rope, preferred_element_type=jnp.float32
    ).astype(jnp.bfloat16)
    rope_out = jnp.where(inside[:, None, :], placed_rope, cache_rope)
    key_pos = jnp.where(
        inside,
        starts[:, None] + jnp.sum(jnp.where(matches, depths[:, None, :], 0), axis=-1),
        slots[None, :],
    )
    ancestor = jnp.einsum(
        "sij,spj->sip", reaches, matches.astype(jnp.float32), precision=lax.Precision.HIGHEST
    )
    visible = (offset < 0)[:, None, :] | (ancestor > 0.5)
    key_angles = jnp.swapaxes(rope_angles(key_pos, half_dim), 1, 2)
    key_cos = jnp.cos(key_angles)
    key_sin = jnp.sin(key_angles)
    rope32 = rope_out.astype(jnp.float32)
    key_low = rope32[:, :half_dim, :]
    key_high = rope32[:, half_dim:, :]
    key_rot = jnp.concatenate(
        [key_low * key_cos - key_high * key_sin, key_high * key_cos + key_low * key_sin], axis=1
    ).astype(jnp.bfloat16)
    scores = (
        jnp.einsum("sihk,spk->sihp", query_lat, lat_out, preferred_element_type=jnp.float32)
        + jnp.einsum("sihr,srp->sihp", query_rot, key_rot, preferred_element_type=jnp.float32)
    ) * qkhead ** (-0.5)
    masked = jnp.where(visible[:, :, None, :], scores, -jnp.inf)
    row_max = jnp.maximum(jnp.max(masked, axis=-1), -1e30)
    weights32 = jnp.exp(masked - row_max[..., None])
    denominator = jnp.sum(weights32, axis=-1)
    weights = weights32.astype(BF16)
    numerator = jnp.einsum("sihp,spk->sihk", weights, lat_out, preferred_element_type=F32)
    numer_values = jnp.einsum(
        "...hk,khv->...hv", numerator, w_uval.astype(F32), precision=lax.Precision.HIGHEST
    )
    value_width = heads_here * vhead
    sent = jnp.concatenate(
        [
            numer_values.reshape(rows, value_width).astype(BF16),
            *(t.reshape(rows, heads_here) for t in bf16_terms(row_max, 3)),
            *(t.reshape(rows, heads_here) for t in bf16_terms(denominator, 3)),
        ],
        axis=1,
    )
    arrived = exchange(sent.reshape(owners, rows // owners, sent.shape[1]), KV).astype(F32)
    extras = arrived[..., value_width:].reshape(owners, rows // owners, 2, 3, heads_here).sum(3)
    maxima = extras[:, :, 0]
    factor = jnp.exp(maxima - jnp.max(maxima, axis=0))
    denom_all = jnp.sum(factor * extras[:, :, 1], axis=0)
    values_all = jnp.sum(
        factor[..., None] * arrived[..., :value_width].reshape(*factor.shape, vhead), axis=0
    )
    head_share = (values_all / denom_all[..., None]).astype(BF16)
    head_rows = from_everyone(head_share.reshape(rows // owners, value_width), KV)
    partial_out = jnp.dot(
        head_rows.reshape(rows, value_width), w_out, preferred_element_type=F32
    )
    mixed = lax.all_gather(partial_out, "tp").sum(axis=0)
    local_squares = jnp.sum(mixed * mixed, axis=-1)
    norm_total = from_everyone(local_squares[None], KV).sum(axis=(0, 1))
    own = lax.dynamic_slice_in_dim(mixed, lax.axis_index("tp") * local_width, local_width, 1)
    result = own * lax.rsqrt(norm_total / full_width + epsilon)[:, None] * gain_out
    result = result.astype(BF16).reshape(seq_count, proposals, local_width)
    return (result, lat_out, rope_out)


def solution(mesh):
    torus = Mesh(
        mesh.devices.reshape(mesh.shape["dp"], 8, 8, mesh.shape["tp"]), ("dp", "kv_0", "kv_1", "tp")
    )
    return jax.shard_map(
        local,
        mesh=torus,
        in_specs=(
            P("dp", None, KV_TP),
            P(KV_TP),
            P(KV_TP, None),
            P(KV_TP, None),
            P(),
            P(),
            P(),
            P(None, "tp", None),
            P(),
            P(None, "tp", None),
            P(None, "tp", None),
            P("tp", KV),
            P(KV_TP),
            P("dp", KV, None),
            P("dp", None, KV),
            P("dp", None),
            P("dp"),
            P("dp"),
        ),
        out_specs=(P("dp", None, KV_TP), P("dp", KV, None), P("dp", None, KV)),
        check_vma=False,
    )
```

time: 273 us -> 161 us (0.59)
  the two profiles are of different devices: /device:TPU:4 before, /device:TPU:2 now
where the time goes in v1:
time: 161 us
  blocking collectives  59.7 us (37%)
  waiting for transfers between devices  42.2 us (26%)
  starting transfers between devices  26.6 us (17%)
  local copies, waits for them, and re-layouts  13.8 us (9%)
  matrix products  8.51 us (5%)
  other arithmetic  7.8 us (5%)
  between operations  1.93 us (1%)
    all_to_all x2, blocking collectives, exchange(): return lax.all_to_all(parts, axes, split_axis=0, concat_axis=0, tiled=True)  49.4 us
    all_to_all x3, waiting for transfers between devices, exchange(): return lax.all_to_all(parts, axes, split_axis=0, concat_axis=0, tiled=True)  42.2 us
    all_to_all x3, starting transfers between devices, exchange(): return lax.all_to_all(parts, axes, split_axis=0, concat_axis=0, tiled=True)  26.6 us
    unnamed x35, local copies, waits for them, and re-layouts  4.64 us
    all_gather x2, blocking collectives, local(): lax.all_gather((tokens.reshape(rows, local_width), gain_in[None], joined)...  3.66 us
  transfers between devices with their start and end apart: 3, of which 3 were waited for; matrix products, arithmetic and copies ran while one was open for 1% of the time, Pallas kernels for 0%

profile of v1, /device:TPU:2, one launch (start us, length us, event | category | flops | bytes accessed | tf_op | source)
XLA Modules:
  0.0 160.6 jit_solution(15171704565413910662)
XLA Ops:
  0.7 0.8 constant_dynamic-slice_fusion
  2.3 1.8 %all-gather.1 = bf16[32,800]{1,0:T(8,128)(2,1)S(1)} all-gather(bf16[16,800]{1,0:T(8,128)(2,1)S(1)} %pad_maximum_fusion.2), channel_id=3, replica_groups=mesh['dp'=4,'kv_0'=8,'kv_1'=8,'tp'=2] {'tp'}, dimensions={0}, use_global_device_ids=true | all-gather | bytes 76800 | tf_op jit(solution)/shard_map/all_gather | solution.py:95
  4.2 1.3 dynamic-slice
  6.1 0.9 dynamic-update-slice
  7.0 2.4 %all-reduce = f32[32]{0:T(128)S(1)} all-reduce(f32[32]{0:T(128)S(1)} %dynamic-update-slice), channel_id=2, replica_groups=mesh['dp'=4,'kv_0'=8,'kv_1'=8,'tp'=2] {'tp'}, use_global_device_ids=true, to_apply=%add | all-reduce | flops 32 | bytes 256
  9.5 0.9 copy.223
  10.4 1.8 %all_gather.21 = bf16[2,256,16]{1,2,0:T(8,128)(2,1)S(1)} all-gather(bf16[1,256,16]{1,2,0:T(8,128)(2,1)S(1)} %copy.223), channel_id=1, replica_groups=mesh['dp'=4,'kv_0'=8,'kv_1'=8,'tp'=2] {'tp'}, dimensions={0}, use_global_device_ids=true | all-gather | bytes 24576 | tf_op jit(solution)/shard_map/all_gather | solution.py:95
  13.1 1.0 pad_maximum_fusion.1
  14.2 16.6 %all-to-all-start = ((f32[64,2,801]{2,1,0:T(2,128)}), f32[64,2,801]{2,1,0:T(2,128)S(1)}, u32[]{:S(2)}, u32[]{:S(2)}) async-start(f32[64,2,801]{2,1,0:T(2,128)} %pad_maximum_fusion.1), calls=%async_computation | async-start | bytes 917504 | tf_op jit(solution)/shard_map/all_to_all | solution.py:16
  32.6 16.8 %all-to-all-done = f32[64,2,801]{2,1,0:T(2,128)S(1)} async-done(((f32[64,2,801]{2,1,0:T(2,128)}), f32[64,2,801]{2,1,0:T(2,128)S(1)}, u32[]{:S(2)}, u32[]{:S(2)}) %all-to-all-start) | async-done | bytes 410144 | tf_op jit(solution)/shard_map/all_to_all | solution.py:16
  51.2 4.9 %all-to-all-start.1 = ((bf16[64,2,800]{2,1,0:T(2,128)(2,1)}), bf16[64,2,800]{2,1,0:T(2,128)(2,1)S(1)}, u32[]{:S(2)}, u32[]{:S(2)}) async-start(bf16[64,2,800]{2,1,0:T(2,128)(2,1)} %broadcast_in_dim.42), calls=%async_computation.1 | async-start | bytes 458752 | tf_op jit(solution)/shard_map/all_to_all | solution.py:16
  56.7 13.2 %all-to-all-done.1 = bf16[64,2,800]{2,1,0:T(2,128)(2,1)S(1)} async-done(((bf16[64,2,800]{2,1,0:T(2,128)(2,1)}), bf16[64,2,800]{2,1,0:T(2,128)(2,1)S(1)}, u32[]{:S(2)}, u32[]{:S(2)}) %all-to-all-start.1) | async-done | bytes 204832 | tf_op jit(solution)/shard_map/all_to_all | solution.py:16
  70.1 2.3 %all_gather.25 = bf16[256,800]{1,0:T(8,128)(2,1)S(1)} all-gather(bf16[128,800]{1,0:T(8,128)(2,1)S(1)} %reshape.332), channel_id=1, replica_groups=mesh['dp'=4,'kv_0'=8,'kv_1'=8,'tp'=2] {'tp'}, dimensions={0}, use_global_device_ids=true | all-gather | bytes 614400 | tf_op jit(solution)/shard_map/all_gather | solution.py:116
  75.6 1.4 convert_select_fusion
  77.0 0.9 fusion
  78.2 1.0 fusion.63
  79.2 1.1 fusion.26
  82.9 1.1 fusion.7
  85.5 2.5 %concatenate.33 = bf16[64,4,1072]{2,1,0:T(4,128)(2,1)S(1)} concatenate(bf16[64,4,1024]{2,1,0:T(4,128)(2,1)S(1)} %convert_element_type.170, bf16[64,4,8]{2,1,0:T(4,128)(2,1)S(1)} %copy.197, bf16[64,4,8]{2,1,0:T(4,128)(2,1)S(1)} %copy.198, bf16[64,4,8]{2,1,0:T(4,128)(2,1)S(1)} %copy.199, bf16[64,4,8]{2,1,0:T(4,128)(2,1)S(1)} %copy.200, bf16[64,4,8]{2,1,0:T(4,128)(2,1)S(1)} %copy.201, ...), dimensions={2} | concatenate | bytes 1097728 | tf_op jit(solution)/shard_map/concatenate | solution.py:188
  87.9 24.3 %all_to_all.25 = bf16[64,4,1072]{2,1,0:T(4,128)(2,1)S(1)} all-to-all(bf16[64,4,1072]{2,1,0:T(4,128)(2,1)S(1)} %concatenate.33), channel_id=1, replica_groups=mesh['dp'=4,'kv_0'=8,'kv_1'=8,'tp'=2] {'kv_0','kv_1'}, dimensions={0} | all-to-all | bytes 1097728 | tf_op jit(solution)/shard_map/all_to_all | solution.py:16
  114.1 25.1 %all_to_all.26 = bf16[64,4,1024]{2,1,0:T(4,128)(2,1)S(1)} all-to-all(bf16[64,4,1024]{2,1,0:T(4,128)(2,1)S(1)} %broadcast_in_dim.55), channel_id=1, replica_groups=mesh['dp'=4,'kv_0'=8,'kv_1'=8,'tp'=2] {'kv_0','kv_1'}, dimensions={0} | all-to-all | bytes 1048576 | tf_op jit(solution)/shard_map/all_to_all | solution.py:16
  139.7 1.9 %all-gather.2 = f32[512,32]{0,1:T(8,128)S(1)} all-gather(f32[256,32]{0,1:T(8,128)S(1)} %fusion.65), channel_id=4, replica_groups=mesh['dp'=4,'kv_0'=8,'kv_1'=8,'tp'=2] {'tp'}, dimensions={0}, use_global_device_ids=true | all-gather | bytes 98304 | tf_op jit(solution)/shard_map/all_gather | solution.py:209
  142.3 5.1 %all-to-all-start.4 = ((f32[64,1,256]{2,1,0:T(1,128)}), f32[64,1,256]{2,1,0:T(1,128)S(1)}, u32[]{:S(2)}, u32[]{:S(2)}) async-start(f32[64,1,256]{2,1,0:T(1,128)} %broadcast_in_dim.56), calls=%async_computation.4 | async-start | bytes 131072 | tf_op jit(solution)/shard_map/all_to_all | solution.py:16
  147.4 12.2 %all-to-all-done.4 = f32[64,1,256]{2,1,0:T(1,128)S(1)} async-done(((f32[64,1,256]{2,1,0:T(1,128)}), f32[64,1,256]{2,1,0:T(1,128)S(1)}, u32[]{:S(2)}, u32[]{:S(2)}) %all-to-all-start.4) | async-done | bytes 65568 | tf_op jit(solution)/shard_map/all_to_all | solution.py:16
  (118 shorter events, 17.3 us)
Async XLA Ops:
  0.6 71.8 %copy-start = (bf16[512,8,96]{0,2,1:T(8,128)(2,1)S(1)}, bf16[512,8,96]{0,2,1:T(8,128)(2,1)}, u32[]{:S(2)}) copy-start(bf16[512,8,96]{0,2,1:T(8,128)(2,1)} %param.25) | copy-start | bytes 2359300
  0.6 30.1 %copy-start.12 = (s32[16,16]{1,0:T(8,128)S(1)}, s32[16,16]{1,0:T(8,128)}, u32[]{:S(2)}) copy-start(s32[16,16]{1,0:T(8,128)} %param.33) | copy-start | bytes 3076
  12.2 19.7 %copy-start.13 = (s32[16]{0:T(128)S(1)}, s32[16]{0:T(128)}, u32[]{:S(2)}) copy-start(s32[16]{0:T(128)} %param.34) | copy-start | bytes 196
  12.2 19.7 %copy-start.14 = (s32[16]{0:T(128)S(1)}, s32[16]{0:T(128)}, u32[]{:S(2)}) copy-start(s32[16]{0:T(128)} %param.35) | copy-start | bytes 196
  12.9 37.3 %copy-start.8 = (f32[512]{0:T(512)S(1)}, f32[512]{0:T(512)}, u32[]{:S(2)}) copy-start(f32[512]{0:T(512)} %param.23) | copy-start | bytes 6148
  12.9 37.4 %copy-start.9 = (f32[256]{0:T(256)S(1)}, f32[256]{0:T(256)}, u32[]{:S(2)}) copy-start(f32[256]{0:T(256)} %param.24) | copy-start | bytes 3076
  14.2 35.3 %all-to-all-start = ((f32[64,2,801]{2,1,0:T(2,128)}), f32[64,2,801]{2,1,0:T(2,128)S(1)}, u32[]{:S(2)}, u32[]{:S(2)}) async-start(f32[64,2,801]{2,1,0:T(2,128)} %pad_maximum_fusion.1), calls=%async_computation | async-start | bytes 917504 | tf_op jit(solution)/shard_map/all_to_all | solution.py:16
  51.2 18.7 %all-to-all-start.1 = ((bf16[64,2,800]{2,1,0:T(2,128)(2,1)}), bf16[64,2,800]{2,1,0:T(2,128)(2,1)S(1)}, u32[]{:S(2)}, u32[]{:S(2)}) async-start(bf16[64,2,800]{2,1,0:T(2,128)(2,1)} %broadcast_in_dim.42), calls=%async_computation.1 | async-start | bytes 458752 | tf_op jit(solution)/shard_map/all_to_all | solution.py:16
  56.7 16.4 %copy-start.10 = (f32[96]{0:T(128)S(1)}, f32[96]{0:T(128)}, u32[]{:S(2)}) copy-start(f32[96]{0:T(128)} %param.26) | copy-start | bytes 1156
  72.4 1.0 copy-start.3
  72.4 1.1 copy-start.5
  74.0 1.6 copy-start.2
  74.0 1.6 slice-start
  76.9 4.9 %copy-start.1 = (bf16[16,256,256]{2,1,0:T(8,128)(2,1)}, bf16[16,256,256]{2,1,0:T(8,128)(2,1)S(1)}, u32[]{:S(2)}) copy-start(bf16[16,256,256]{2,1,0:T(8,128)(2,1)S(1)} %convert_select_fusion) | copy-start | bytes 6291460
  76.9 0.9 slice-start.1
  77.0 1.2 copy-start.6
  81.8 1.0 copy-start.4
  113.6 25.8 %copy-start.7 = (bf16[1024,32]{0,1:T(8,128)(2,1)S(1)}, bf16[1024,32]{0,1:T(8,128)(2,1)}, u32[]{:S(2)}) copy-start(bf16[1024,32]{0,1:T(8,128)(2,1)} %param.29) | copy-start | bytes 196612
  114.0 45.8 %copy-start.11 = (f32[16]{0:T(128)S(1)}, f32[16]{0:T(128)}, u32[]{:S(2)}) copy-start(f32[16]{0:T(128)} %param.30) | copy-start | bytes 196
  142.3 17.3 %all-to-all-start.4 = ((f32[64,1,256]{2,1,0:T(1,128)}), f32[64,1,256]{2,1,0:T(1,128)S(1)}, u32[]{:S(2)}, u32[]{:S(2)}) async-start(f32[64,1,256]{2,1,0:T(1,128)} %broadcast_in_dim.56), calls=%async_computation.4 | async-start | bytes 131072 | tf_op jit(solution)/shard_map/all_to_all | solution.py:16

commit v2 on v1

v2 whole, which is shorter than its diff:
```python
import jax
import jax.numpy as jnp
from jax import lax
from jax.experimental import pallas as pl
from jax.experimental.pallas import tpu as pltpu
from jax.sharding import Mesh
from jax.sharding import PartitionSpec as P

KV_TP = ("kv_0", "kv_1", "tp")
KV = ("kv_0", "kv_1")

epsilon = 1e-06
F32 = jnp.float32
BF16 = jnp.bfloat16
LOWEST = -1e30
HIDDEN = -3e38


def exchange(parts, axes):
    return lax.all_to_all(parts, axes, split_axis=0, concat_axis=0, tiled=True)


def from_everyone(shard, axes):
    return exchange(jnp.broadcast_to(shard[None], (lax.axis_size(axes), *shard.shape)), axes)


def normed(values, gain_vec):
    return (
        values * lax.rsqrt(jnp.mean(values * values, axis=-1, keepdims=True) + epsilon) * gain_vec
    )


def rope_angles(position, half_dim):
    frequency = 10000.0 ** (-(jnp.arange(half_dim, dtype=jnp.float32) * 2.0) / (2 * half_dim))
    return position.astype(jnp.float32)[..., None] * frequency


def ancestry(parents):
    proposals = parents.shape[-1]
    step = (parents[..., :, None] == jnp.arange(proposals, dtype=jnp.int32)).astype(BF16)
    reaches = step + jnp.eye(proposals, dtype=BF16)
    covered = 2
    while covered < proposals:
        step = jnp.einsum("sij,sjk->sik", step, step, preferred_element_type=F32).astype(BF16)
        reaches = reaches + jnp.einsum(
            "sij,sjk->sik", reaches, step, preferred_element_type=F32
        ).astype(BF16)
        covered *= 2
    reaches = reaches.astype(F32)
    depths = (jnp.sum(reaches, axis=-1) - 1.0).astype(jnp.int32)
    return (reaches, depths)


def attend_kernel(
    starts,
    base,
    lat_rows,
    w_query,
    gain,
    w_key,
    w_value,
    query_cos,
    query_sin,
    key_cos,
    key_sin,
    reach,
    cache_lat,
    cache_rope,
    lat_out,
    rope_out,
    sent,
    q_lat,
    q_rot,
    k_rot,
    bias,
    numer,
):
    step = pl.program_id(0)
    block, pos_count, kvrank = cache_lat.shape
    heads = w_key.shape[0]
    rope_dim = cache_rope.shape[1]
    half_dim = rope_dim // 2
    proposals = reach.shape[2]
    seq_count = q_lat.shape[0]
    qrank = w_query.shape[0]
    lanes = w_key.shape[1]
    qkhead = lanes - rope_dim
    scale = qkhead ** (-0.5)

    @pl.when(step == 0)
    def _():
        projected = jnp.dot(
            lat_rows[:, :qrank], w_query[...], preferred_element_type=F32
        )
        counted = lax.broadcasted_iota(jnp.int32, (1, lanes), 1) < qkhead
        for h in range(heads):
            one = projected[:, h * lanes : (h + 1) * lanes]
            mean = (
                jnp.sum(jnp.where(counted, one * one, 0.0), axis=1, keepdims=True) / qkhead
            )
            one = one * lax.rsqrt(mean + epsilon) * gain[...]
            at = pl.ds(h * proposals, proposals)
            moved = jnp.dot(one.astype(BF16), w_key[h], preferred_element_type=F32)
            q_lat[:, at, :] = moved.astype(BF16).reshape(seq_count, proposals, kvrank)
            turned = one * query_cos[...] + pltpu.roll(one, rope_dim, 1) * query_sin[...]
            q_rot[:, at, :] = turned.astype(BF16).reshape(seq_count, proposals, lanes)

    for j in range(block):
        s = step * block + j
        offset = base[0] - starts[s]
        rope32 = cache_rope[j].astype(F32)
        low, high = rope32[:half_dim], rope32[half_dim:]
        cosine, sine = key_cos[...], key_sin[...]
        k_rot[j, :half_dim] = (low * cosine - high * sine).astype(BF16)
        k_rot[j, half_dim:] = (high * cosine + low * sine).astype(BF16)
        hit = (offset > -pos_count) & (offset < proposals)

        @pl.when(jnp.logical_not(hit))
        def _():
            lat_out[j] = cache_lat[j]
            rope_out[j] = cache_rope[j]
            bias[j] = jnp.full(bias.shape[1:], jnp.where(offset < 0, 0.0, HIDDEN), F32)

        @pl.when(hit)
        def _():
            rows = pl.ds(pl.multiple_of(s * proposals, proposals), proposals)
            down = lax.broadcasted_iota(jnp.int32, (pos_count, proposals), 0) + offset
            picked = down == lax.broadcasted_iota(jnp.int32, (pos_count, proposals), 1)
            across = lax.broadcasted_iota(jnp.int32, (proposals, pos_count), 1) + offset
            chosen = across == lax.broadcasted_iota(jnp.int32, (proposals, pos_count), 0)
            chosen = chosen.astype(F32).astype(BF16)
            along = lax.broadcasted_iota(jnp.int32, (1, pos_count), 1) + offset
            inside = (along >= 0) & (along < proposals)
            beneath = lax.broadcasted_iota(jnp.int32, (pos_count, 1), 0) + offset
            placed = jnp.dot(
                picked.astype(F32).astype(BF16),
                lat_rows[rows, qrank : qrank + kvrank],
                preferred_element_type=F32,
            )
            lat_out[j] = jnp.where(
                (beneath >= 0) & (beneath < proposals), placed, cache_lat[j].astype(F32)
            ).astype(BF16)
            new_rope = lat_rows[rows, qrank + kvrank :].astype(F32)
            swapped = jnp.concatenate([new_rope[:, half_dim:], new_rope[:, :half_dim]], axis=1)
            turned = (
                new_rope * query_cos[rows, :rope_dim] + swapped * query_sin[rows, :rope_dim]
            )
            contract = (((0,), (0,)), ((), ()))
            put = lax.dot_general(
                new_rope.astype(BF16), chosen, contract, preferred_element_type=F32
            )
            rope_out[j] = jnp.where(inside, put, rope32).astype(BF16)
            put = lax.dot_general(
                turned.astype(BF16), chosen, contract, preferred_element_type=F32
            )
            k_rot[j] = jnp.where(inside, put, k_rot[j].astype(F32)).astype(BF16)
            seen = jnp.dot(reach[s], chosen, preferred_element_type=F32)
            bias[j] = jnp.where((seen > 0.5) | (along < 0), 0.0, HIDDEN)

    for j in range(block):
        s = step * block + j
        keys = lat_out[j]
        score = lax.dot_general(
            q_lat[s], keys, (((1,), (1,)), ((), ())), preferred_element_type=F32
        )
        score = score + jnp.dot(
            q_rot[s][:, :rope_dim], k_rot[j], preferred_element_type=F32
        )
        score = score * scale + bias[j]
        top = jnp.maximum(jnp.max(score, axis=1, keepdims=True), LOWEST)
        weights = jnp.exp(score - top)
        total = jnp.sum(weights, axis=1, keepdims=True)
        numer[j] = jnp.dot(weights.astype(BF16), keys, preferred_element_type=F32)
        lane = lax.broadcasted_iota(jnp.int32, (1, 128), 1)
        terms = jnp.zeros((heads * proposals, 128), F32)
        for first, rest in ((0, top), (3, total)):
            for k in range(3):
                term = rest.astype(BF16).astype(F32)
                terms = jnp.where(lane == first + k, term, terms)
                rest = rest - term
        extra = jnp.transpose(terms)[:8].astype(BF16)
        for c in range(heads // 2):
            sent[j * (heads // 2) + c, 2 * proposals :, :] = extra

    for h in range(heads):
        part = numer[:, pl.ds(h * proposals, proposals), :].reshape(block * proposals, kvrank)
        upper = part.astype(BF16)
        lower = (part - upper.astype(F32)).astype(BF16)
        both = jnp.dot(
            jnp.concatenate([upper, lower], axis=0), w_value[h], preferred_element_type=F32
        )
        value = (both[: block * proposals] + both[block * proposals :]).astype(BF16)
        for j in range(block):
            sent[
                j * (heads // 2) + h // 2,
                (h % 2) * proposals : (h % 2 + 1) * proposals,
                :,
            ] = value[j * proposals : (j + 1) * proposals]


def attend(starts, base, lat_rows, weights, tables, reach, cache_lat, cache_rope):
    w_query, gain, w_key, w_value = weights
    seq_count, pos_count, kvrank = cache_lat.shape
    rope_dim = cache_rope.shape[1]
    heads, lanes, _ = w_key.shape
    proposals = reach.shape[2]
    rows = heads * proposals
    block = 4
    whole = pl.BlockSpec(memory_space=pltpu.VMEM)
    smem = pl.BlockSpec(memory_space=pltpu.SMEM)
    lat_spec = pl.BlockSpec((block, pos_count, kvrank), lambda g: (g, 0, 0))
    rope_spec = pl.BlockSpec((block, rope_dim, pos_count), lambda g: (g, 0, 0))
    chunks = heads // 2
    sent_shape = (seq_count * chunks, 2 * proposals + 8, w_value.shape[2])
    return pl.pallas_call(
        attend_kernel,
        grid=(seq_count // block,),
        in_specs=[smem, smem, *[whole] * 10, lat_spec, rope_spec],
        out_specs=[
            lat_spec,
            rope_spec,
            pl.BlockSpec((block * chunks, *sent_shape[1:]), lambda g: (g, 0, 0)),
        ],
        out_shape=[
            jax.ShapeDtypeStruct(cache_lat.shape, BF16),
            jax.ShapeDtypeStruct(cache_rope.shape, BF16),
            jax.ShapeDtypeStruct(sent_shape, BF16),
        ],
        scratch_shapes=[
            pltpu.VMEM((seq_count, rows, kvrank), BF16),
            pltpu.VMEM((seq_count, rows, lanes), BF16),
            pltpu.VMEM((block, rope_dim, pos_count), BF16),
            pltpu.VMEM((block, rows, pos_count), F32),
            pltpu.VMEM((block, rows, kvrank), F32),
        ],
        compiler_params=pltpu.CompilerParams(vmem_limit_bytes=24 * 1024 * 1024),
        cost_estimate=pl.CostEstimate(
            flops=10**9, bytes_accessed=8 * 10**6, transcendentals=10**6
        ),
    )(starts, base, lat_rows, w_query, gain, w_key, w_value, *tables, reach, cache_lat, cache_rope)


def project_kernel(heads_in, w_out, result):
    seq_count, heads, proposals, vhead = heads_in.shape
    total = jnp.zeros(result.shape, F32)
    for h in range(heads):
        total += jnp.dot(
            heads_in[:, h].reshape(seq_count * proposals, vhead),
            w_out[h * vhead : (h + 1) * vhead, :],
            preferred_element_type=F32,
        )
    result[...] = total


def project(heads_in, w_out):
    seq_count, heads, proposals, vhead = heads_in.shape
    return pl.pallas_call(
        project_kernel,
        out_shape=jax.ShapeDtypeStruct((seq_count * proposals, w_out.shape[1]), F32),
        in_specs=[pl.BlockSpec(memory_space=pltpu.VMEM)] * 2,
        out_specs=pl.BlockSpec(memory_space=pltpu.VMEM),
        compiler_params=pltpu.CompilerParams(vmem_limit_bytes=8 * 1024 * 1024),
        cost_estimate=pl.CostEstimate(
            flops=2 * 10**7, bytes_accessed=6 * 10**5, transcendentals=0
        ),
    )(heads_in, w_out)


def local(
    tokens,
    gain_in,
    w_qdown,
    w_kvdown,
    w_ropek,
    gain_qlat,
    gain_kvlat,
    w_qup,
    gain_q,
    w_ukey,
    w_uval,
    w_out,
    gain_out,
    cache_lat,
    cache_rope,
    parents,
    lengths,
    accepted,
):
    seq_count, proposals, local_width = tokens.shape
    rows = seq_count * proposals
    owners = lax.axis_size(KV)
    full_width = local_width * lax.axis_size(KV_TP)
    qrank, heads_here, qkhead = w_qup.shape
    kvrank, _, nope_dim = w_ukey.shape
    vhead = w_uval.shape[2]
    rope_dim = cache_rope.shape[1]
    half_dim = rope_dim // 2
    width = qrank + kvrank + rope_dim

    rope_rows = lax.dynamic_slice_in_dim(
        w_ropek, lax.axis_index(KV_TP) * local_width, local_width, 0
    )
    joined = jnp.concatenate([w_qdown, w_kvdown, rope_rows], axis=1)
    half = rows // lax.axis_size("tp")
    pair_tokens, pair_gain, pair_weights = lax.all_gather(
        (tokens.reshape(rows, local_width), gain_in[None], joined), "tp"
    )
    pair_tokens = lax.dynamic_slice_in_dim(pair_tokens, lax.axis_index("tp") * half, half, 1)
    tok_rows = pair_tokens.astype(F32)
    scaled = (tok_rows * pair_gain).astype(BF16)
    squares = jnp.sum(tok_rows * tok_rows, axis=(0, 2))
    partial_rows = jnp.einsum("crd,cdk->rk", scaled, pair_weights, preferred_element_type=F32)
    sent = jnp.concatenate([partial_rows, squares[:, None]], axis=1)
    arrived = exchange(sent.reshape(owners, half // owners, width + 1), KV)
    summed = arrived.sum(axis=0)
    latent_rows = summed[:, :width] * lax.rsqrt(summed[:, width] / full_width + epsilon)[:, None]
    share = jnp.concatenate(
        [
            normed(latent_rows[:, :qrank], gain_qlat).astype(BF16),
            normed(latent_rows[:, qrank : qrank + kvrank], gain_kvlat).astype(BF16),
            latent_rows[:, qrank + kvrank :].astype(BF16),
        ],
        axis=1,
    )
    everyone = from_everyone(share, KV).reshape(half, width)
    everyone = lax.all_gather(everyone, "tp", axis=0, tiled=True)
    reaches, depths = ancestry(parents)
    starts = lengths + accepted
    angles = rope_angles(starts[:, None] + depths, half_dim).reshape(rows, half_dim)
    cosine, sine = jnp.cos(angles), jnp.sin(angles)
    lanes = qkhead + rope_dim
    spare = ((0, 0), (0, lanes - rope_dim))
    pos_count = cache_lat.shape[1]
    base = lax.axis_index(KV) * pos_count
    slot_angles = rope_angles(base + jnp.arange(pos_count, dtype=jnp.int32), half_dim).T
    tables = (
        jnp.pad(jnp.concatenate([cosine, cosine], axis=1), spare),
        jnp.pad(jnp.concatenate([-sine, sine], axis=1), spare),
        jnp.cos(slot_angles),
        jnp.sin(slot_angles),
    )

    def arranged(values):
        nope, low, high = jnp.split(values, [nope_dim, nope_dim + half_dim], axis=-1)
        return jnp.concatenate([low, high, nope, high, low], axis=-1)

    weights = (
        arranged(w_qup).reshape(qrank, heads_here * lanes),
        arranged(gain_q)[None],
        jnp.pad(jnp.transpose(w_ukey, (1, 2, 0)), ((0, 0), (rope_dim, rope_dim), (0, 0))),
        jnp.transpose(w_uval, (1, 0, 2)),
    )
    reach = jnp.tile(reaches.astype(BF16), (1, heads_here, 1))
    lat_out, rope_out, sent = attend(
        starts, base[None], everyone, weights, tables, reach, cache_lat, cache_rope
    )
    arrived = exchange(sent, KV).astype(F32)
    group = 2 * proposals
    chunk = lax.rem(lax.axis_index(KV), heads_here // 2)
    extras = lax.dynamic_slice_in_dim(arrived[:, group:], chunk * group, group, 2)
    maxima = extras[:, 0] + extras[:, 1] + extras[:, 2]
    denominators = extras[:, 3] + extras[:, 4] + extras[:, 5]
    factor = jnp.exp(maxima - jnp.max(maxima, axis=0))
    denom_all = jnp.sum(factor * denominators, axis=0)
    values_all = jnp.sum(factor[..., None] * arrived[:, :group], axis=0)
    head_share = (values_all / denom_all[:, None]).astype(BF16)
    head_rows = from_everyone(head_share, KV)
    partial_out = project(head_rows.reshape(seq_count, heads_here, proposals, vhead), w_out)
    mixed = lax.all_gather(partial_out, "tp").sum(axis=0)
    local_squares = jnp.sum(mixed * mixed, axis=-1)
    norm_total = from_everyone(local_squares[None], KV).sum(axis=(0, 1))
    own = lax.dynamic_slice_in_dim(mixed, lax.axis_index("tp") * local_width, local_width, 1)
    result = own * lax.rsqrt(norm_total / full_width + epsilon)[:, None] * gain_out
    result = result.astype(BF16).reshape(seq_count, proposals, local_width)
    return (result, lat_out, rope_out)


def solution(mesh):
    torus = Mesh(
        mesh.devices.reshape(mesh.shape["dp"], 8, 8, mesh.shape["tp"]), ("dp", "kv_0", "kv_1", "tp")
    )
    return jax.shard_map(
        local,
        mesh=torus,
        in_specs=(
            P("dp", None, KV_TP),
            P(KV_TP),
            P(KV_TP, None),
            P(KV_TP, None),
            P(),
            P(),
            P(),
            P(None, "tp", None),
            P(),
            P(None, "tp", None),
            P(None, "tp", None),
            P("tp", KV),
            P(KV_TP),
            P("dp", KV, None),
            P("dp", None, KV),
            P("dp", None),
            P("dp"),
            P("dp"),
        ),
        out_specs=(P("dp", None, KV_TP), P("dp", KV, None), P("dp", None, KV)),
        check_vma=False,
    )
```

time: 161 us -> 168 us (1.043)
  blocking collectives: 59.7 us -> 10.4 us
  waiting for transfers between devices: 42.2 us -> 74.2 us
  starting transfers between devices: 26.6 us -> 38.5 us
  Pallas kernels: 0 us -> 8.97 us
  local copies, waits for them, and re-layouts: 13.8 us -> 21.9 us
  matrix products: 8.51 us -> 1.45 us
    all_to_all x2 -> x0, blocking collectives: 49.4 us -> none  [exchange(): return lax.all_to_all(parts, axes, split_axis=0, concat_axis=0, tiled=True)]
    all_to_all x3 -> x5, waiting for transfers between devices: 42.2 us -> 74.2 us  [exchange(): return lax.all_to_all(parts, axes, split_axis=0, concat_axis=0, tiled=True)]
    all_to_all x3 -> x5, starting transfers between devices: 26.6 us -> 38.5 us  [exchange(): return lax.all_to_all(parts, axes, split_axis=0, concat_axis=0, tiled=True)]
    pallas_call x0 -> x2, Pallas kernels: none -> 8.97 us  [the longest x1 8.69 us: attend(): pl.pallas_call(attend_kernel, grid=(seq_count // block,), in_specs=[smem,...]
    dot_general x10 -> x0, matrix products: 7.05 us -> none  [the longest x1 1.36 us: local(): jnp.einsum('spj,sjk->spk', selector, new_latent, preferred_element_type=j...]
    unnamed x35 -> x45, local copies, waits for them, and re-layouts: 4.64 us -> 10.4 us
    concatenate x1 -> x2, local copies, waits for them, and re-layouts: 2.48 us -> 0.19 us  [the longest x1 0.1 us: local(): jnp.concatenate([cosine, cosine], axis=1)]
    pad x0 -> x3, local copies, waits for them, and re-layouts: none -> 1.95 us  [the longest x1 1.93 us: local(): jnp.pad(jnp.transpose(w_ukey, (1, 2, 0)), ((0, 0), (rope_dim, rope_dim),...]
  transfers between devices with their start and end apart: 3 -> 5, of which waited for: 3 -> 5; matrix products, arithmetic and copies ran while one was open for 1% -> 6% of each run, Pallas kernels for 0% -> 0%
where the time goes in v2:
time: 168 us; the launch traced here: 167 us
  waiting for transfers between devices  74.2 us (44%)
  starting transfers between devices  38.5 us (23%)
  local copies, waits for them, and re-layouts  21.9 us (13%)
  blocking collectives  10.4 us (6%)
  other arithmetic  9.36 us (6%)
  Pallas kernels  8.97 us (5%)
  between operations  1.77 us (1%)
    all_to_all x5, waiting for transfers between devices, exchange(): return lax.all_to_all(parts, axes, split_axis=0, concat_axis=0, tiled=True)  74.2 us
    all_to_all x5, starting transfers between devices, exchange(): return lax.all_to_all(parts, axes, split_axis=0, concat_axis=0, tiled=True)  38.5 us
    unnamed x45, local copies, waits for them, and re-layouts  10.4 us
    pallas_call x1, Pallas kernels, attend(): pl.pallas_call(attend_kernel, grid=(seq_count // block,), in_specs=[smem,...  8.69 us
    all_gather x2, blocking collectives, local(): lax.all_gather((tokens.reshape(rows, local_width), gain_in[None], joined)...  3.66 us
  transfers between devices with their start and end apart: 5, of which 5 were waited for; matrix products, arithmetic and copies ran while one was open for 6% of the time, Pallas kernels for 0%

profile of v2, /device:TPU:2, one launch (start us, length us, event | category | flops | bytes accessed | tf_op | source)
XLA Modules:
  0.0 166.7 jit_solution(1978200459926137305)
XLA Ops:
  2.5 1.8 %all-gather.1 = bf16[32,800]{1,0:T(8,128)(2,1)S(1)} all-gather(bf16[16,800]{1,0:T(8,128)(2,1)S(1)} %pad_maximum_fusion.4), channel_id=3, replica_groups=mesh['dp'=4,'kv_0'=8,'kv_1'=8,'tp'=2] {'tp'}, dimensions={0}, use_global_device_ids=true | all-gather | bytes 76800 | tf_op jit(solution)/shard_map/all_gather | solution.py:305
  4.3 1.3 dynamic-slice
  7.1 2.4 %all-reduce.3 = f32[32]{0:T(128)S(1)} all-reduce(f32[32]{0:T(128)S(1)} %dynamic-update-slice), channel_id=2, replica_groups=mesh['dp'=4,'kv_0'=8,'kv_1'=8,'tp'=2] {'tp'}, use_global_device_ids=true, to_apply=%add.3 | all-reduce | flops 32 | bytes 256
  10.5 1.8 %all_gather.21 = bf16[2,256,16]{1,2,0:T(8,128)(2,1)S(1)} all-gather(bf16[1,256,16]{1,2,0:T(8,128)(2,1)S(1)} %copy.151), channel_id=1, replica_groups=mesh['dp'=4,'kv_0'=8,'kv_1'=8,'tp'=2] {'tp'}, dimensions={0}, use_global_device_ids=true | all-gather | bytes 24576 | tf_op jit(solution)/shard_map/all_gather | solution.py:305
  13.2 1.1 pad_maximum_fusion.1
  14.3 16.8 %all-to-all-start = ((f32[64,2,801]{2,1,0:T(2,128)}), f32[64,2,801]{2,1,0:T(2,128)}, u32[]{:S(2)}, u32[]{:S(2)}) async-start(f32[64,2,801]{2,1,0:T(2,128)} %pad_maximum_fusion.1), calls=%async_computation | async-start | bytes 917504 | tf_op jit(solution)/shard_map/all_to_all | solution.py:20
  36.4 1.9 %pad.11.w_key = bf16[8,128,256]{2,1,0:T(8,128)(2,1)} pad(bf16[8,64,256]{2,1,0:T(8,128)(2,1)} %bitcast.47, bf16[]{:T(256)} %constant.56.clone.1), padding=0_0x32_32x0_0 | pad | bytes 786434 | tf_op jit(solution)/shard_map/jit(_pad)/pad | solution.py:350
  39.0 10.7 %all-to-all-done = f32[64,2,801]{2,1,0:T(2,128)} async-done(((f32[64,2,801]{2,1,0:T(2,128)}), f32[64,2,801]{2,1,0:T(2,128)}, u32[]{:S(2)}, u32[]{:S(2)}) %all-to-all-start) | async-done | bytes 410144 | tf_op jit(solution)/shard_map/all_to_all | solution.py:20
  49.7 1.2 reduce_sum.91
  53.1 5.4 %all-to-all-start.1 = ((bf16[64,2,800]{2,1,0:T(2,128)(2,1)}), bf16[64,2,800]{2,1,0:T(2,128)(2,1)}, u32[]{:S(2)}, u32[]{:S(2)}) async-start(bf16[64,2,800]{2,1,0:T(2,128)(2,1)} %broadcast_in_dim.11), calls=%async_computation.1 | async-start | bytes 458752 | tf_op jit(solution)/shard_map/all_to_all | solution.py:20
  58.5 1.3 maximum_bitcast_fusion.gain
  59.8 1.3 multiply_sine_fusion
  61.1 10.8 %all-to-all-done.1 = bf16[64,2,800]{2,1,0:T(2,128)(2,1)} async-done(((bf16[64,2,800]{2,1,0:T(2,128)(2,1)}), bf16[64,2,800]{2,1,0:T(2,128)(2,1)}, u32[]{:S(2)}, u32[]{:S(2)}) %all-to-all-start.1) | async-done | bytes 204832 | tf_op jit(solution)/shard_map/all_to_all | solution.py:20
  72.0 1.8 %reshape.155 = bf16[128,800]{1,0:T(8,128)(2,1)} reshape(bf16[64,2,800]{2,1,0:T(2,128)(2,1)} %all-to-all-done.1) | data formatting | bytes 409600 | tf_op jit(solution)/shard_map/reshape | solution.py:325
  73.8 2.3 %all_gather.25.lat_rows = bf16[256,800]{1,0:T(8,128)(2,1)S(1)} all-gather(bf16[128,800]{1,0:T(8,128)(2,1)} %reshape.155), channel_id=1, replica_groups=mesh['dp'=4,'kv_0'=8,'kv_1'=8,'tp'=2] {'tp'}, dimensions={0}, use_global_device_ids=true | all-gather | bytes 614400 | tf_op jit(solution)/shard_map/all_gather | solution.py:326
  78.1 1.0 copy-done.3
  82.0 8.7 %shard_map.193 = (bf16[16,256,256]{2,1,0:T(8,128)(2,1)}, bf16[16,32,256]{2,1,0:T(8,128)(2,1)}, bf16[64,40,128]{2,1,0:T(8,128)(2,1)S(1)}) custom-call(s32[16]{0:T(128)S(1)} %copy-done.8, s32[1]{0:T(128)} %bitcast.base, bf16[256,800]{1,0:T(8,128)(2,1)S(1)} %all_gather.25.lat_rows, bf16[512,1024]{1,0:T(8,128)(2,1)S(1)} %copy.153.w_query, ...), custom_call_target="tpu_custom_call" | custom-call | flops 1000000000 | bytes 8000000 | tf_op jit(solution)/shard_map/pallas_call | solution.py:215
  91.6 4.6 %all-to-all-start.2 = ((bf16[64,40,128]{2,1,0:T(8,128)(2,1)}), bf16[64,40,128]{2,1,0:T(8,128)(2,1)S(1)}, u32[]{:S(2)}, u32[]{:S(2)}) async-start(bf16[64,40,128]{2,1,0:T(8,128)(2,1)} %copy-done.4), calls=%async_computation.2 | async-start | bytes 1310720 | tf_op jit(solution)/shard_map/all_to_all | solution.py:20
  96.2 21.8 %all-to-all-done.2 = bf16[64,40,128]{2,1,0:T(8,128)(2,1)S(1)} async-done(((bf16[64,40,128]{2,1,0:T(8,128)(2,1)}), bf16[64,40,128]{2,1,0:T(8,128)(2,1)S(1)}, u32[]{:S(2)}, u32[]{:S(2)}) %all-to-all-start.2) | async-done | bytes 655392 | tf_op jit(solution)/shard_map/all_to_all | solution.py:20
  120.0 6.4 %all-to-all-start.3 = ((bf16[64,32,128]{2,1,0:T(8,128)(2,1)}), bf16[64,32,128]{2,1,0:T(8,128)(2,1)S(1)}, u32[]{:S(2)}, u32[]{:S(2)}) async-start(bf16[64,32,128]{2,1,0:T(8,128)(2,1)} %broadcast_in_dim.13), calls=%async_computation.3 | async-start | bytes 1048576 | tf_op jit(solution)/shard_map/all_to_all | solution.py:20
  126.7 18.6 %all-to-all-done.3 = bf16[64,32,128]{2,1,0:T(8,128)(2,1)S(1)} async-done(((bf16[64,32,128]{2,1,0:T(8,128)(2,1)}), bf16[64,32,128]{2,1,0:T(8,128)(2,1)S(1)}, u32[]{:S(2)}, u32[]{:S(2)}) %all-to-all-start.3) | async-done | bytes 524320 | tf_op jit(solution)/shard_map/all_to_all | solution.py:20
  145.6 2.0 %all-gather.2 = f32[512,32]{1,0:T(8,128)S(1)} all-gather(f32[256,32]{1,0:T(8,128)S(1)} %shard_map.194), channel_id=4, replica_groups=mesh['dp'=4,'kv_0'=8,'kv_1'=8,'tp'=2] {'tp'}, dimensions={0}, use_global_device_ids=true | all-gather | bytes 98304 | tf_op jit(solution)/shard_map/all_gather | solution.py:369
  148.4 5.2 %all-to-all-start.4 = ((f32[64,1,256]{2,1,0:T(1,128)}), f32[64,1,256]{2,1,0:T(1,128)S(1)}, u32[]{:S(2)}, u32[]{:S(2)}) async-start(f32[64,1,256]{2,1,0:T(1,128)} %broadcast_in_dim.14), calls=%async_computation.4 | async-start | bytes 131072 | tf_op jit(solution)/shard_map/all_to_all | solution.py:20
  153.6 12.2 %all-to-all-done.4 = f32[64,1,256]{2,1,0:T(1,128)S(1)} async-done(((f32[64,1,256]{2,1,0:T(1,128)}), f32[64,1,256]{2,1,0:T(1,128)S(1)}, u32[]{:S(2)}, u32[]{:S(2)}) %all-to-all-start.4) | async-done | bytes 65568 | tf_op jit(solution)/shard_map/all_to_all | solution.py:20
  (106 shorter events, 22.1 us)
Async XLA Ops:
  0.6 0.9 copy-start
  0.6 30.5 %copy-start.17 = (s32[16,16]{1,0:T(8,128)S(1)}, s32[16,16]{1,0:T(8,128)}, u32[]{:S(2)}) copy-start(s32[16,16]{1,0:T(8,128)} %param.33) | copy-start | bytes 3076
  12.3 20.0 %copy-start.18 = (s32[16]{0:T(128)S(1)}, s32[16]{0:T(128)}, u32[]{:S(2)}) copy-start(s32[16]{0:T(128)} %param.34) | copy-start | bytes 196
  12.3 20.0 %copy-start.19 = (s32[16]{0:T(128)S(1)}, s32[16]{0:T(128)}, u32[]{:S(2)}) copy-start(s32[16]{0:T(128)} %param.35) | copy-start | bytes 196
  14.3 35.4 %all-to-all-start = ((f32[64,2,801]{2,1,0:T(2,128)}), f32[64,2,801]{2,1,0:T(2,128)}, u32[]{:S(2)}, u32[]{:S(2)}) async-start(f32[64,2,801]{2,1,0:T(2,128)} %pad_maximum_fusion.1), calls=%async_computation | async-start | bytes 917504 | tf_op jit(solution)/shard_map/all_to_all | solution.py:20
  31.1 3.1 %copy-start.10 = (bf16[512,8,96]{0,2,1:T(8,128)(2,1)S(1)}, bf16[512,8,96]{0,2,1:T(8,128)(2,1)}, u32[]{:S(2)}) copy-start(bf16[512,8,96]{0,2,1:T(8,128)(2,1)} %param.25) | copy-start | bytes 2359300
  31.1 2.1 %copy-start.14 = (f32[16]{0:T(128)}, f32[16]{0:T(128)S(1)}, u32[]{:S(2)}) copy-start(f32[16]{0:T(128)S(1)} %multiply_power_fusion) | copy-start | bytes 196
  31.4 2.8 %slice-start = ((bf16[512,8,96]{0,2,1:T(8,128)(2,1)}), bf16[512,8,64]{0,2,1:T(8,128)(2,1)S(1)}, s32[]{:S(2)}) async-start(bf16[512,8,96]{0,2,1:T(8,128)(2,1)} %param.25), calls=%async_computation.5 | async-start | bytes 1048576 | tf_op jit(solution)/shard_map/split | solution.py:344
  31.4 2.8 %slice-start.1 = ((bf16[512,8,96]{0,2,1:T(8,128)(2,1)}), bf16[512,8,32]{0,2,1:T(8,128)(2,1)S(1)}, s32[]{:S(2)}) async-start(bf16[512,8,96]{0,2,1:T(8,128)(2,1)} %param.25), calls=%async_computation.6 | async-start | bytes 524288 | tf_op jit(solution)/shard_map/split | solution.py:344
  34.2 0.7 copy-start.13
  34.2 1.3 copy-start.11
  34.3 17.1 %copy-start.15 = (f32[512]{0:T(512)S(1)}, f32[512]{0:T(512)}, u32[]{:S(2)}) copy-start(f32[512]{0:T(512)} %param.23) | copy-start | bytes 6148
  36.4 40.6 %copy-start.1 = (bf16[16,256,256]{2,1,0:T(8,128)(2,1)S(1)}, bf16[16,256,256]{2,1,0:T(8,128)(2,1)}, u32[]{:S(2)}) copy-start(bf16[16,256,256]{2,1,0:T(8,128)(2,1)} %cache_lat.1) | copy-start | bytes 6291460
  53.1 18.9 %all-to-all-start.1 = ((bf16[64,2,800]{2,1,0:T(2,128)(2,1)}), bf16[64,2,800]{2,1,0:T(2,128)(2,1)}, u32[]{:S(2)}, u32[]{:S(2)}) async-start(bf16[64,2,800]{2,1,0:T(2,128)(2,1)} %broadcast_in_dim.11), calls=%async_computation.1 | async-start | bytes 458752 | tf_op jit(solution)/shard_map/all_to_all | solution.py:20
  77.0 1.0 copy-start.2
  78.1 1.0 copy-start.3
  79.1 0.9 copy-start.5
  80.1 0.7 copy-start.6
  90.7 0.8 copy-start.4
  91.6 26.5 %all-to-all-start.2 = ((bf16[64,40,128]{2,1,0:T(8,128)(2,1)}), bf16[64,40,128]{2,1,0:T(8,128)(2,1)S(1)}, u32[]{:S(2)}, u32[]{:S(2)}) async-start(bf16[64,40,128]{2,1,0:T(8,128)(2,1)} %copy-done.4), calls=%async_computation.2 | async-start | bytes 1310720 | tf_op jit(solution)/shard_map/all_to_all | solution.py:20
  118.6 7.9 %copy-start.12 = (bf16[1024,32]{0,1:T(8,128)(2,1)S(1)}, bf16[1024,32]{0,1:T(8,128)(2,1)}, u32[]{:S(2)}) copy-start(bf16[1024,32]{0,1:T(8,128)(2,1)} %param.29) | copy-start | bytes 196612
  119.1 46.8 %copy-start.16 = (f32[16]{0:T(128)S(1)}, f32[16]{0:T(128)}, u32[]{:S(2)}) copy-start(f32[16]{0:T(128)} %param.30) | copy-start | bytes 196
  120.0 25.3 %all-to-all-start.3 = ((bf16[64,32,128]{2,1,0:T(8,128)(2,1)}), bf16[64,32,128]{2,1,0:T(8,128)(2,1)S(1)}, u32[]{:S(2)}, u32[]{:S(2)}) async-start(bf16[64,32,128]{2,1,0:T(8,128)(2,1)} %broadcast_in_dim.13), calls=%async_computation.3 | async-start | bytes 1048576 | tf_op jit(solution)/shard_map/all_to_all | solution.py:20
  148.4 17.4 %all-to-all-start.4 = ((f32[64,1,256]{2,1,0:T(1,128)}), f32[64,1,256]{2,1,0:T(1,128)S(1)}, u32[]{:S(2)}, u32[]{:S(2)}) async-start(f32[64,1,256]{2,1,0:T(1,128)} %broadcast_in_dim.14), calls=%async_computation.4 | async-start | bytes 131072 | tf_op jit(solution)/shard_map/all_to_all | solution.py:20
  (3 other events, 1.7 us)

commit v3 on v2

--- a/solution.py
+++ b/solution.py
@@ -1,3 +1,5 @@
+import functools
+
 import jax
 import jax.numpy as jnp
 from jax import lax
@@ -51,10 +53,100 @@
     return (reaches, depths)
 
 
+def gather_kernel(index, tokens, gain, w_qdown, w_kvdown, rope_columns, out):
+    width = tokens.shape[2]
+    rows = tokens.shape[0] * tokens.shape[1]
+    qrank, kvrank = w_qdown.shape[1], w_kvdown.shape[1]
+    rope_dim, lanes = rope_columns.shape
+    tok_rows = tokens[...].astype(F32).reshape(rows, width)
+    scaled = (tok_rows * gain[...]).astype(BF16).astype(F32)
+    out[:width, :rows] = jnp.transpose(scaled).astype(BF16)
+    out[:width, rows : rows + qrank] = w_qdown[...]
+    out[:width, rows + qrank : rows + qrank + kvrank] = w_kvdown[...]
+    at = rows + qrank + kvrank
+    shift = lax.rem(lanes - lax.rem(index[0] * width, lanes), lanes)
+    turned = pltpu.roll(rope_columns[...].astype(F32), shift, 1)
+    padded = jnp.concatenate([turned, jnp.zeros((lanes - rope_dim, lanes), F32)], axis=0)
+    out[:width, at:] = jnp.transpose(padded)[:width].astype(BF16)
+    flipped = jnp.transpose(tok_rows)
+    squares = jnp.sum(flipped * flipped, axis=0, keepdims=True)
+    row = lax.broadcasted_iota(jnp.int32, (width, rows), 0)
+    terms = jnp.zeros((width, rows), F32)
+    for k in range(3):
+        term = squares.astype(BF16).astype(F32)
+        terms = jnp.where(row == k, term, terms)
+        squares = squares - term
+    out[width:, :rows] = terms.astype(BF16)
+    out[width:, rows:at] = jnp.zeros((width, at - rows), BF16)
+    row = lax.broadcasted_iota(jnp.int32, (width, lanes), 0)
+    lane = lax.broadcasted_iota(jnp.int32, (width, lanes), 1)
+    out[width:, at:] = jnp.where((row < 3) & (lane == rope_dim), 1.0, 0.0).astype(BF16)
+
+
+def gather_inputs(index, tokens, gain_in, w_qdown, w_kvdown, w_ropek):
+    width = tokens.shape[2]
+    rows = tokens.shape[0] * tokens.shape[1]
+    lanes = 128
+    whole = pl.BlockSpec(memory_space=pltpu.VMEM)
+    shape = (2 * width, rows + w_qdown.shape[1] + w_kvdown.shape[1] + lanes)
+    return pl.pallas_call(
+        gather_kernel,
+        grid_spec=pltpu.PrefetchScalarGridSpec(
+            num_scalar_prefetch=1,
+            grid=(1,),
+            in_specs=[
+                *[whole] * 4,
+                pl.BlockSpec(
+                    (w_ropek.shape[1], lanes), lambda g, index: (0, index[0] * width // lanes)
+                ),
+            ],
+            out_specs=whole,
+        ),
+        out_shape=jax.ShapeDtypeStruct(shape, BF16),
+        cost_estimate=pl.CostEstimate(flops=10**5, bytes_accessed=10**5, transcendentals=0),
+    )(index, tokens, gain_in[None], w_qdown, w_kvdown, w_ropek.T)
+
+
+def latent_kernel(full_width, arrived, gain_qlat, gain_kvlat, out):
+    qrank, kvrank = gain_qlat.shape[1], gain_kvlat.shape[1]
+    summed = jnp.sum(arrived[...], axis=0)
+    lanes = 128
+    at = qrank + kvrank
+    lane = lax.broadcasted_iota(jnp.int32, (1, lanes), 1)
+    last = summed[:, at:]
+    rope_dim = 32
+    squares = jnp.sum(jnp.where(lane == rope_dim, last, 0.0), axis=1, keepdims=True)
+    rescale = lax.rsqrt(squares / full_width + epsilon)
+    share = jnp.concatenate(
+        [
+            normed(summed[:, :qrank] * rescale, gain_qlat[...]),
+            normed(summed[:, qrank:at] * rescale, gain_kvlat[...]),
+            jnp.where(lane < rope_dim, last * rescale, 0.0),
+            jnp.zeros(last.shape, F32),
+        ],
+        axis=1,
+    )
+    pieces = [share[:, c * lanes : (c + 1) * lanes] for c in range(share.shape[1] // lanes)]
+    stacked = jnp.concatenate(pieces, axis=0).astype(BF16)
+    out[...] = jnp.broadcast_to(stacked[None], out.shape)
+
+
+def latents(arrived, full_width, gain_qlat, gain_kvlat):
+    owners = arrived.shape[0]
+    return pl.pallas_call(
+        functools.partial(latent_kernel, full_width),
+        in_specs=[pl.BlockSpec(memory_space=pltpu.VMEM)] * 3,
+        out_specs=pl.BlockSpec(memory_space=pltpu.VMEM),
+        out_shape=jax.ShapeDtypeStruct((owners, 16, 128), BF16),
+        compiler_params=pltpu.CompilerParams(vmem_limit_bytes=8 * 1024 * 1024),
+        cost_estimate=pl.CostEstimate(flops=10**5, bytes_accessed=10**6, transcendentals=0),
+    )(arrived, gain_qlat[None], gain_kvlat[None])
+
+
 def attend_kernel(
     starts,
     base,
-    lat_rows,
+    packed,
     w_query,
     gain,
     w_key,
@@ -74,6 +166,7 @@
     k_rot,
     bias,
     numer,
+    lat_rows,
 ):
     step = pl.program_id(0)
     block, pos_count, kvrank = cache_lat.shape
@@ -89,6 +182,9 @@
 
     @pl.when(step == 0)
     def _():
+        for c in range(lat_rows.shape[1] // 128):
+            piece = packed[:, 2 * c : 2 * c + 2, :]
+            lat_rows[:, c * 128 : (c + 1) * 128] = piece.reshape(lat_rows.shape[0], 128)
         projected = jnp.dot(
             lat_rows[:, :qrank], w_query[...], preferred_element_type=F32
         )
@@ -140,7 +236,7 @@
             lat_out[j] = jnp.where(
                 (beneath >= 0) & (beneath < proposals), placed, cache_lat[j].astype(F32)
             ).astype(BF16)
-            new_rope = lat_rows[rows, qrank + kvrank :].astype(F32)
+            new_rope = lat_rows[rows, qrank + kvrank :].astype(F32)[:, :rope_dim]
             swapped = jnp.concatenate([new_rope[:, half_dim:], new_rope[:, :half_dim]], axis=1)
             turned = (
                 new_rope * query_cos[rows, :rope_dim] + swapped * query_sin[rows, :rope_dim]
@@ -155,7 +251,9 @@
             )
             k_rot[j] = jnp.where(inside, put, k_rot[j].astype(F32)).astype(BF16)
             seen = jnp.dot(reach[s], chosen, preferred_element_type=F32)
-            bias[j] = jnp.where((seen > 0.5) | (along < 0), 0.0, HIDDEN)
+            shown = jnp.where((seen > 0.5) | (along < 0), 0.0, HIDDEN)
+            for h in range(heads):
+                bias[j, h * proposals : (h + 1) * proposals, :] = shown
 
     for j in range(block):
         s = step * block + j
@@ -205,6 +303,7 @@
     heads, lanes, _ = w_key.shape
     proposals = reach.shape[2]
     rows = heads * proposals
+    lat_width = w_query.shape[0] + kvrank + 128
     block = 4
     whole = pl.BlockSpec(memory_space=pltpu.VMEM)
     smem = pl.BlockSpec(memory_space=pltpu.SMEM)
@@ -232,8 +331,8 @@
             pltpu.VMEM((block, rope_dim, pos_count), BF16),
             pltpu.VMEM((block, rows, pos_count), F32),
             pltpu.VMEM((block, rows, kvrank), F32),
+            pltpu.VMEM((seq_count * proposals, lat_width), BF16),
         ],
-        compiler_params=pltpu.CompilerParams(vmem_limit_bytes=24 * 1024 * 1024),
         cost_estimate=pl.CostEstimate(
             flops=10**9, bytes_accessed=8 * 10**6, transcendentals=10**6
         ),
@@ -246,7 +345,7 @@
     for h in range(heads):
         total += jnp.dot(
             heads_in[:, h].reshape(seq_count * proposals, vhead),
-            w_out[h * vhead : (h + 1) * vhead, :],
+            w_out[:, h * vhead : (h + 1) * vhead].T,
             preferred_element_type=F32,
         )
     result[...] = total
@@ -256,7 +355,7 @@
     seq_count, heads, proposals, vhead = heads_in.shape
     return pl.pallas_call(
         project_kernel,
-        out_shape=jax.ShapeDtypeStruct((seq_count * proposals, w_out.shape[1]), F32),
+        out_shape=jax.ShapeDtypeStruct((seq_count * proposals, w_out.shape[0]), F32),
         in_specs=[pl.BlockSpec(memory_space=pltpu.VMEM)] * 2,
         out_specs=pl.BlockSpec(memory_space=pltpu.VMEM),
         compiler_params=pltpu.CompilerParams(vmem_limit_bytes=8 * 1024 * 1024),
@@ -295,34 +394,18 @@
     vhead = w_uval.shape[2]
     rope_dim = cache_rope.shape[1]
     half_dim = rope_dim // 2
-    width = qrank + kvrank + rope_dim
-
-    rope_rows = lax.dynamic_slice_in_dim(
-        w_ropek, lax.axis_index(KV_TP) * local_width, local_width, 0
-    )
-    joined = jnp.concatenate([w_qdown, w_kvdown, rope_rows], axis=1)
+
     half = rows // lax.axis_size("tp")
-    pair_tokens, pair_gain, pair_weights = lax.all_gather(
-        (tokens.reshape(rows, local_width), gain_in[None], joined), "tp"
-    )
-    pair_tokens = lax.dynamic_slice_in_dim(pair_tokens, lax.axis_index("tp") * half, half, 1)
-    tok_rows = pair_tokens.astype(F32)
-    scaled = (tok_rows * pair_gain).astype(BF16)
-    squares = jnp.sum(tok_rows * tok_rows, axis=(0, 2))
-    partial_rows = jnp.einsum("crd,cdk->rk", scaled, pair_weights, preferred_element_type=F32)
-    sent = jnp.concatenate([partial_rows, squares[:, None]], axis=1)
-    arrived = exchange(sent.reshape(owners, half // owners, width + 1), KV)
-    summed = arrived.sum(axis=0)
-    latent_rows = summed[:, :width] * lax.rsqrt(summed[:, width] / full_width + epsilon)[:, None]
-    share = jnp.concatenate(
-        [
-            normed(latent_rows[:, :qrank], gain_qlat).astype(BF16),
-            normed(latent_rows[:, qrank : qrank + kvrank], gain_kvlat).astype(BF16),
-            latent_rows[:, qrank + kvrank :].astype(BF16),
-        ],
-        axis=1,
-    )
-    everyone = from_everyone(share, KV).reshape(half, width)
+    inputs = gather_inputs(
+        lax.axis_index(KV_TP)[None], tokens, gain_in, w_qdown, w_kvdown, w_ropek
+    )
+    inputs = lax.all_gather(inputs, "tp", axis=0, tiled=True)
+    own_rows = lax.dynamic_slice_in_dim(inputs, lax.axis_index("tp") * half, half, 1)
+    partial_rows = lax.dot_general(
+        own_rows, inputs[:, rows:], (((0,), (0,)), ((), ())), preferred_element_type=F32
+    )
+    arrived = exchange(partial_rows.reshape(owners, half // owners, -1), KV)
+    everyone = exchange(latents(arrived, full_width, gain_qlat, gain_kvlat), KV)
     everyone = lax.all_gather(everyone, "tp", axis=0, tiled=True)
     reaches, depths = ancestry(parents)
     starts = lengths + accepted
@@ -350,7 +433,7 @@
         jnp.pad(jnp.transpose(w_ukey, (1, 2, 0)), ((0, 0), (rope_dim, rope_dim), (0, 0))),
         jnp.transpose(w_uval, (1, 0, 2)),
     )
-    reach = jnp.tile(reaches.astype(BF16), (1, heads_here, 1))
+    reach = reaches.astype(BF16)
     lat_out, rope_out, sent = attend(
         starts, base[None], everyone, weights, tables, reach, cache_lat, cache_rope
     )
@@ -365,7 +448,7 @@
     values_all = jnp.sum(factor[..., None] * arrived[:, :group], axis=0)
     head_share = (values_all / denom_all[:, None]).astype(BF16)
     head_rows = from_everyone(head_share, KV)
-    partial_out = project(head_rows.reshape(seq_count, heads_here, proposals, vhead), w_out)
+    partial_out = project(head_rows.reshape(seq_count, heads_here, proposals, vhead), w_out.T)
     mixed = lax.all_gather(partial_out, "tp").sum(axis=0)
     local_squares = jnp.sum(mixed * mixed, axis=-1)
     norm_total = from_everyone(local_squares[None], KV).sum(axis=(0, 1))

time: 168 us -> 150 us (0.89)
  blocking collectives: 10.4 us -> 31.6 us
  waiting for transfers between devices: 74.2 us -> 58.3 us
  local copies, waits for them, and re-layouts: 21.9 us -> 6.66 us
  starting transfers between devices: 38.5 us -> 31.9 us
  other arithmetic: 9.36 us -> 3.71 us
  Pallas kernels: 8.97 us -> 14.2 us
    all_to_all x0 -> x1, blocking collectives: none -> 25 us  [exchange(): return lax.all_to_all(parts, axes, split_axis=0, concat_axis=0, tiled=True)]
    all_to_all x5 -> x4, waiting for transfers between devices: 74.2 us -> 58.3 us  [exchange(): return lax.all_to_all(parts, axes, split_axis=0, concat_axis=0, tiled=True)]
    unnamed x45 -> x25, local copies, waits for them, and re-layouts: 10.4 us -> 0.95 us
    all_to_all x5 -> x4, starting transfers between devices: 38.5 us -> 31.9 us  [exchange(): return lax.all_to_all(parts, axes, split_axis=0, concat_axis=0, tiled=True)]
    pallas_call x0 -> x2, Pallas kernels: none -> 2.72 us  [the longest x1 1.68 us: gather_inputs(): pl.pallas_call(gather_kernel, grid_spec=pltpu.PrefetchScalarGridSpec(num_...]
    pallas_call x1, Pallas kernels: 8.69 us -> 11.2 us  [attend(): pl.pallas_call(attend_kernel, grid=(seq_count // block,), in_specs=[smem,...]
    unnamed x1 -> x0, blocking collectives: 2.44 us -> none
    concatenate x3 -> x0, other arithmetic: 1.81 us -> none  [the longest x1 1.06 us: local(): sent = jnp.concatenate([partial_rows, squares[:, None]], axis=1)]
  transfers between devices with their start and end apart: 5 -> 4, of which waited for: 5 -> 4; matrix products, arithmetic and copies ran while one was open for 6% -> 5% of each run, Pallas kernels for 0% -> 0%
where the time goes in v3:
time: 150 us; the launch traced here: 149 us
  waiting for transfers between devices  58.3 us (39%)
  starting transfers between devices  31.9 us (21%)
  blocking collectives  31.6 us (21%)
  Pallas kernels  14.2 us (9%)
  local copies, waits for them, and re-layouts  6.66 us (4%)
  other arithmetic  3.71 us (2%)
  matrix products  1.95 us (1%)
    all_to_all x4, waiting for transfers between devices, exchange(): return lax.all_to_all(parts, axes, split_axis=0, concat_axis=0, tiled=True)  58.3 us
    all_to_all x4, starting transfers between devices, exchange(): return lax.all_to_all(parts, axes, split_axis=0, concat_axis=0, tiled=True)  31.9 us
    all_to_all x1, blocking collectives, exchange(): return lax.all_to_all(parts, axes, split_axis=0, concat_axis=0, tiled=True)  25 us
    pallas_call x1, Pallas kernels, attend(): pl.pallas_call(attend_kernel, grid=(seq_count // block,), in_specs=[smem,...  11.2 us
  transfers between devices with their start and end apart: 4, of which 4 were waited for; matrix products, arithmetic and copies ran while one was open for 5% of the time, Pallas kernels for 0%

profile of v3, /device:TPU:2, one launch (start us, length us, event | category | flops | bytes accessed | tf_op | source)
XLA Modules:
  0.0 149.3 jit_solution(11728614642900347707)
XLA Ops:
  0.6 1.7 %shard_map.193 = bf16[32,1152]{1,0:T(8,128)(2,1)} custom-call(s32[1]{0:T(128)} %bitcast.1.index, bf16[16,16,16]{2,1,0:T(8,128)(2,1)} %tokens.1, f32[1,16]{1,0:T(1,128)} %bitcast.53, bf16[16,512]{1,0:T(8,128)(2,1)} %w_qdown.1, bf16[16,256]{1,0:T(8,128)(2,1)} %w_kvdown.1, bf16[32,2048]{1,0:T(8,128)(2,1)} %bitcast.50), custom_call_target="tpu_custom_call" | custom-call | flops 100000 | bytes 100000 | tf_op jit(solution)/shard_map/pallas_call | solution.py:92
  2.3 2.2 %all_gather.12 = bf16[64,1152]{1,0:T(8,128)(2,1)S(1)} all-gather(bf16[32,1152]{1,0:T(8,128)(2,1)} %shard_map.193), channel_id=1, replica_groups=mesh['dp'=4,'kv_0'=8,'kv_1'=8,'tp'=2] {'tp'}, dimensions={0}, use_global_device_ids=true | all-gather | bytes 221184 | tf_op jit(solution)/shard_map/all_gather | solution.py:402
  4.9 1.0 reshape.128
  5.9 16.7 %all-to-all-start = ((f32[64,2,896]{2,1,0:T(2,128)}), f32[64,2,896]{2,1,0:T(2,128)S(1)}, u32[]{:S(2)}, u32[]{:S(2)}) async-start(f32[64,2,896]{2,1,0:T(2,128)} %reshape.128), calls=%async_computation | async-start | bytes 917504 | tf_op jit(solution)/shard_map/all_to_all | solution.py:22
  23.5 0.9 convert_reduce_fusion
  25.0 16.3 %all-to-all-done.arrived = f32[64,2,896]{2,1,0:T(2,128)S(1)} async-done(((f32[64,2,896]{2,1,0:T(2,128)}), f32[64,2,896]{2,1,0:T(2,128)S(1)}, u32[]{:S(2)}, u32[]{:S(2)}) %all-to-all-start) | async-done | bytes 458784 | tf_op jit(solution)/shard_map/all_to_all | solution.py:22
  41.3 1.0 shard_map.194
  42.4 4.9 %all-to-all-start.1 = ((bf16[64,16,128]{2,1,0:T(8,128)(2,1)}), bf16[64,16,128]{2,1,0:T(8,128)(2,1)S(1)}, u32[]{:S(2)}, u32[]{:S(2)}) async-start(bf16[64,16,128]{2,1,0:T(8,128)(2,1)} %shard_map.194), calls=%async_computation.1 | async-start | bytes 524288 | tf_op jit(solution)/shard_map/all_to_all | solution.py:22
  47.5 0.7 pad.12.query_cos
  48.9 1.3 copy.76.w_query
  50.2 0.9 copy.82
  51.1 0.8 pad.11.w_key
  52.5 0.8 multiply_sine_fusion
  53.2 8.3 %all-to-all-done.1 = bf16[64,16,128]{2,1,0:T(8,128)(2,1)S(1)} async-done(((bf16[64,16,128]{2,1,0:T(8,128)(2,1)}), bf16[64,16,128]{2,1,0:T(8,128)(2,1)S(1)}, u32[]{:S(2)}, u32[]{:S(2)}) %all-to-all-start.1) | async-done | bytes 262176 | tf_op jit(solution)/shard_map/all_to_all | solution.py:22
  61.5 2.3 %all_gather.13.packed = bf16[128,16,128]{2,1,0:T(8,128)(2,1)} all-gather(bf16[64,16,128]{2,1,0:T(8,128)(2,1)S(1)} %all-to-all-done.1), channel_id=1, replica_groups=mesh['dp'=4,'kv_0'=8,'kv_1'=8,'tp'=2] {'tp'}, dimensions={0}, use_global_device_ids=true | all-gather | bytes 786432 | tf_op jit(solution)/shard_map/all_gather | solution.py:409
  63.9 11.2 %shard_map.195 = (bf16[16,256,256]{2,1,0:T(8,128)(2,1)}, bf16[16,32,256]{2,1,0:T(8,128)(2,1)}, bf16[64,40,128]{2,1,0:T(8,128)(2,1)}) custom-call(s32[16]{0:T(128)} %copy-done.7, s32[1]{0:T(128)} %bitcast.base, bf16[128,16,128]{2,1,0:T(8,128)(2,1)} %all_gather.13.packed, bf16[512,1024]{1,0:T(8,128)(2,1)} %copy.76.w_query, f32[1,128]{1,0:T(1,128)} %maximum_bitcast_fusion.gain, ...), custom_call_target="tpu_custom_call" | custom-call | flops 1000000000 | bytes 8000000 | tf_op jit(solution)/shard_map/pallas_call | solution.py:314
  75.0 5.1 %all-to-all-start.2 = ((bf16[64,40,128]{2,1,0:T(8,128)(2,1)}), bf16[64,40,128]{2,1,0:T(8,128)(2,1)S(1)}, u32[]{:S(2)}, u32[]{:S(2)}) async-start(bf16[64,40,128]{2,1,0:T(8,128)(2,1)} %get-tuple-element.6), calls=%async_computation.2 | async-start | bytes 1310720 | tf_op jit(solution)/shard_map/all_to_all | solution.py:22
  80.2 21.5 %all-to-all-done.2 = bf16[64,40,128]{2,1,0:T(8,128)(2,1)S(1)} async-done(((bf16[64,40,128]{2,1,0:T(8,128)(2,1)}), bf16[64,40,128]{2,1,0:T(8,128)(2,1)S(1)}, u32[]{:S(2)}, u32[]{:S(2)}) %all-to-all-start.2) | async-done | bytes 655392 | tf_op jit(solution)/shard_map/all_to_all | solution.py:22
  102.9 25.0 %all_to_all.25 = bf16[64,32,128]{2,1,0:T(8,128)(2,1)S(1)} all-to-all(bf16[64,32,128]{2,1,0:T(8,128)(2,1)S(1)} %broadcast_in_dim.22), channel_id=1, replica_groups=mesh['dp'=4,'kv_0'=8,'kv_1'=8,'tp'=2] {'kv_0','kv_1'}, dimensions={0} | all-to-all | bytes 1048576 | tf_op jit(solution)/shard_map/all_to_all | solution.py:22
  128.2 2.0 %all-gather = f32[512,32]{1,0:T(8,128)S(1)} all-gather(f32[256,32]{1,0:T(8,128)S(1)} %shard_map.196), channel_id=2, replica_groups=mesh['dp'=4,'kv_0'=8,'kv_1'=8,'tp'=2] {'tp'}, dimensions={0}, use_global_device_ids=true | all-gather | bytes 98304 | tf_op jit(solution)/shard_map/all_gather | solution.py:452
  130.3 0.7 broadcast_in_dim.23
  131.0 5.2 %all-to-all-start.4 = ((f32[64,1,256]{2,1,0:T(1,128)}), f32[64,1,256]{2,1,0:T(1,128)S(1)}, u32[]{:S(2)}, u32[]{:S(2)}) async-start(f32[64,1,256]{2,1,0:T(1,128)} %broadcast_in_dim.23), calls=%async_computation.4 | async-start | bytes 131072 | tf_op jit(solution)/shard_map/all_to_all | solution.py:22
  136.2 12.2 %all-to-all-done.4 = f32[64,1,256]{2,1,0:T(1,128)S(1)} async-done(((f32[64,1,256]{2,1,0:T(1,128)}), f32[64,1,256]{2,1,0:T(1,128)S(1)}, u32[]{:S(2)}, u32[]{:S(2)}) %all-to-all-start.4) | async-done | bytes 65568 | tf_op jit(solution)/shard_map/all_to_all | solution.py:22
  148.5 0.8 multiply_convert_fusion
  (62 shorter events, 4.8 us)
Async XLA Ops:
  2.3 20.4 %copy-start.9 = (s32[16,16]{1,0:T(8,128)S(1)}, s32[16,16]{1,0:T(8,128)}, u32[]{:S(2)}) copy-start(s32[16,16]{1,0:T(8,128)} %param.33) | copy-start | bytes 3076
  4.8 19.6 %copy-start.10 = (s32[16]{0:T(128)S(1)}, s32[16]{0:T(128)}, u32[]{:S(2)}) copy-start(s32[16]{0:T(128)} %param.34) | copy-start | bytes 196
  4.8 19.6 %copy-start.11 = (s32[16]{0:T(128)S(1)}, s32[16]{0:T(128)}, u32[]{:S(2)}) copy-start(s32[16]{0:T(128)} %param.35) | copy-start | bytes 196
  4.8 19.8 %copy-start.6 = (f32[96]{0:T(128)S(1)}, f32[96]{0:T(128)}, u32[]{:S(2)}) copy-start(f32[96]{0:T(128)} %param.26) | copy-start | bytes 1156
  4.9 19.8 %copy-start.3 = (bf16[512,8,96]{0,2,1:T(8,128)(2,1)S(1)}, bf16[512,8,96]{0,2,1:T(8,128)(2,1)}, u32[]{:S(2)}) copy-start(bf16[512,8,96]{0,2,1:T(8,128)(2,1)} %param.25) | copy-start | bytes 2359300
  5.9 18.8 %slice-start = ((bf16[512,8,96]{0,2,1:T(8,128)(2,1)}), bf16[512,8,64]{0,2,1:T(8,128)(2,1)S(1)}, s32[]{:S(2)}) async-start(bf16[512,8,96]{0,2,1:T(8,128)(2,1)} %param.25), calls=%async_computation.5 | async-start | bytes 1048576 | tf_op jit(solution)/shard_map/split | solution.py:427
  5.9 18.8 %slice-start.1 = ((bf16[512,8,96]{0,2,1:T(8,128)(2,1)}), bf16[512,8,32]{0,2,1:T(8,128)(2,1)S(1)}, s32[]{:S(2)}) async-start(bf16[512,8,96]{0,2,1:T(8,128)(2,1)} %param.25), calls=%async_computation.6 | async-start | bytes 524288 | tf_op jit(solution)/shard_map/split | solution.py:427
  5.9 35.4 %all-to-all-start = ((f32[64,2,896]{2,1,0:T(2,128)}), f32[64,2,896]{2,1,0:T(2,128)S(1)}, u32[]{:S(2)}, u32[]{:S(2)}) async-start(f32[64,2,896]{2,1,0:T(2,128)} %reshape.128), calls=%async_computation | async-start | bytes 917504 | tf_op jit(solution)/shard_map/all_to_all | solution.py:22
  22.6 18.7 %copy-start.1 = (f32[512]{0:T(512)S(1)}, f32[512]{0:T(512)}, u32[]{:S(2)}) copy-start(f32[512]{0:T(512)} %param.23) | copy-start | bytes 6148
  22.7 18.7 %copy-start.2 = (f32[256]{0:T(256)S(1)}, f32[256]{0:T(256)}, u32[]{:S(2)}) copy-start(f32[256]{0:T(256)} %param.24) | copy-start | bytes 3076
  24.4 23.0 %copy-start.7 = (s32[16]{0:T(128)}, s32[16]{0:T(128)S(1)}, u32[]{:S(2)}) copy-start(s32[16]{0:T(128)S(1)} %add.112.starts) | copy-start | bytes 196
  41.3 8.8 %copy-start.4 = (bf16[256,8,128]{2,1,0:T(8,128)(2,1)S(1)}, bf16[256,8,128]{2,1,0:T(8,128)(2,1)}, u32[]{:S(2)}) copy-start(bf16[256,8,128]{2,1,0:T(8,128)(2,1)} %param.28) | copy-start | bytes 1572868
  42.4 19.2 %all-to-all-start.1 = ((bf16[64,16,128]{2,1,0:T(8,128)(2,1)}), bf16[64,16,128]{2,1,0:T(8,128)(2,1)S(1)}, u32[]{:S(2)}, u32[]{:S(2)}) async-start(bf16[64,16,128]{2,1,0:T(8,128)(2,1)} %shard_map.194), calls=%async_computation.1 | async-start | bytes 524288 | tf_op jit(solution)/shard_map/all_to_all | solution.py:22
  47.3 3.8 %copy-start.5 = (bf16[256,8,64]{0,2,1:T(8,128)(2,1)S(1)}, bf16[256,8,64]{0,2,1:T(8,128)(2,1)}, u32[]{:S(2)}) copy-start(bf16[256,8,64]{0,2,1:T(8,128)(2,1)} %param.27) | copy-start | bytes 786436
  75.0 26.6 %all-to-all-start.2 = ((bf16[64,40,128]{2,1,0:T(8,128)(2,1)}), bf16[64,40,128]{2,1,0:T(8,128)(2,1)S(1)}, u32[]{:S(2)}, u32[]{:S(2)}) async-start(bf16[64,40,128]{2,1,0:T(8,128)(2,1)} %get-tuple-element.6), calls=%async_computation.2 | async-start | bytes 1310720 | tf_op jit(solution)/shard_map/all_to_all | solution.py:22
  102.2 25.7 %copy-start = (bf16[1024,32]{0,1:T(8,128)(2,1)S(1)}, bf16[1024,32]{0,1:T(8,128)(2,1)}, u32[]{:S(2)}) copy-start(bf16[1024,32]{0,1:T(8,128)(2,1)} %param.29) | copy-start | bytes 196612
  102.3 46.2 %copy-start.8 = (f32[16]{0:T(128)S(1)}, f32[16]{0:T(128)}, u32[]{:S(2)}) copy-start(f32[16]{0:T(128)} %param.30) | copy-start | bytes 196
  131.0 17.4 %all-to-all-start.4 = ((f32[64,1,256]{2,1,0:T(1,128)}), f32[64,1,256]{2,1,0:T(1,128)S(1)}, u32[]{:S(2)}, u32[]{:S(2)}) async-start(f32[64,1,256]{2,1,0:T(1,128)} %broadcast_in_dim.23), calls=%async_computation.4 | async-start | bytes 131072 | tf_op jit(solution)/shard_map/all_to_all | solution.py:22

commit v4 on v3

--- a/solution.py
+++ b/solution.py
@@ -147,183 +147,210 @@
     starts,
     base,
     packed,
+    gain,
+    query_turn,
+    reach,
     w_query,
-    gain,
     w_key,
     w_value,
-    query_cos,
-    query_sin,
-    key_cos,
-    key_sin,
-    reach,
+    key_turn,
+    cache_rope,
     cache_lat,
-    cache_rope,
     lat_out,
     rope_out,
-    sent,
+    sent_out,
     q_lat,
     q_rot,
     k_rot,
     bias,
     numer,
     lat_rows,
+    lat,
+    rope,
+    sent,
+    lat_came,
+    rope_came,
+    lat_left,
+    rope_left,
+    sent_left,
 ):
-    step = pl.program_id(0)
-    block, pos_count, kvrank = cache_lat.shape
-    heads = w_key.shape[0]
+    block = k_rot.shape[0]
+    seq_count, pos_count, kvrank = cache_lat.shape
+    qrank = w_query.shape[0]
+    heads, lanes, _ = w_key.shape
     rope_dim = cache_rope.shape[1]
     half_dim = rope_dim // 2
     proposals = reach.shape[2]
-    seq_count = q_lat.shape[0]
-    qrank = w_query.shape[0]
-    lanes = w_key.shape[1]
     qkhead = lanes - rope_dim
+    chunks = heads // 2
     scale = qkhead ** (-0.5)
-
-    @pl.when(step == 0)
-    def _():
-        for c in range(lat_rows.shape[1] // 128):
-            piece = packed[:, 2 * c : 2 * c + 2, :]
-            lat_rows[:, c * 128 : (c + 1) * 128] = piece.reshape(lat_rows.shape[0], 128)
-        projected = jnp.dot(
-            lat_rows[:, :qrank], w_query[...], preferred_element_type=F32
+    contract_last = (((1,), (1,)), ((), ()))
+    contract_first = (((0,), (0,)), ((), ()))
+
+    def coming(g):
+        part = pl.ds(g * block, block)
+        return (
+            pltpu.make_async_copy(cache_lat.at[part], lat.at[part], lat_came.at[g]),
+            pltpu.make_async_copy(cache_rope.at[part], rope.at[part], rope_came.at[g]),
         )
-        counted = lax.broadcasted_iota(jnp.int32, (1, lanes), 1) < qkhead
+
+    def leaving(g):
+        part = pl.ds(g * block, block)
+        piece = pl.ds(g * block * chunks, block * chunks)
+        return (
+            pltpu.make_async_copy(lat.at[part], lat_out.at[part], lat_left.at[g]),
+            pltpu.make_async_copy(rope.at[part], rope_out.at[part], rope_left.at[g]),
+            pltpu.make_async_copy(sent.at[piece], sent_out.at[piece], sent_left.at[g]),
+        )
+
+    for g in range(seq_count // block):
+        for copy in coming(g):
+            copy.start()
+    for c in range(lat_rows.shape[1] // 128):
+        piece = packed[:, 2 * c : 2 * c + 2, :]
+        lat_rows[:, c * 128 : (c + 1) * 128] = piece.reshape(lat_rows.shape[0], 128)
+    lane = lax.broadcasted_iota(jnp.int32, (1, lanes), 1)
+    cosine = jnp.where(lane < rope_dim, query_turn[...], 0.0)
+    sine = jnp.where(lane < rope_dim, pltpu.roll(query_turn[...], lanes - rope_dim, 1), 0.0)
+    projected = jnp.dot(lat_rows[:, :qrank], w_query[...], preferred_element_type=F32)
+    for h in range(heads):
+        one = projected[:, h * lanes : (h + 1) * lanes]
+        mean = jnp.sum(jnp.where(lane < qkhead, one * one, 0.0), axis=1, keepdims=True) / qkhead
+        one = one * lax.rsqrt(mean + epsilon) * gain[...]
+        at = pl.ds(h * proposals, proposals)
+        moved = jnp.dot(one.astype(BF16), w_key[h], preferred_element_type=F32)
+        q_lat[:, at, :] = moved.astype(BF16).reshape(seq_count, proposals, kvrank)
+        turned = one * cosine + pltpu.roll(one, rope_dim, 1) * sine
+        q_rot[:, at, :] = turned.astype(BF16).reshape(seq_count, proposals, lanes)
+
+    @pl.loop(0, seq_count // block)
+    def _(step):
+        for copy in coming(step):
+            copy.wait()
+        for j in range(block):
+            s = step * block + j
+            rope32 = rope[s].astype(F32)
+            low, high = rope32[:half_dim], rope32[half_dim:]
+            key_cos, key_sin = key_turn[:half_dim], key_turn[half_dim:]
+            k_rot[j, :half_dim] = (low * key_cos - high * key_sin).astype(BF16)
+            k_rot[j, half_dim:] = (high * key_cos + low * key_sin).astype(BF16)
+            offset = base[0] - starts[s]
+            hit = (offset > -pos_count) & (offset < proposals)
+
+            @pl.when(jnp.logical_not(hit))
+            def _():
+                bias[j] = jnp.full(bias.shape[1:], jnp.where(offset < 0, 0.0, HIDDEN), F32)
+
+            @pl.when(hit)
+            def _():
+                rows = pl.ds(pl.multiple_of(s * proposals, proposals), proposals)
+                down = lax.broadcasted_iota(jnp.int32, (pos_count, proposals), 0) + offset
+                picked = down == lax.broadcasted_iota(jnp.int32, (pos_count, proposals), 1)
+                across = lax.broadcasted_iota(jnp.int32, (proposals, pos_count), 1) + offset
+                chosen = across == lax.broadcasted_iota(jnp.int32, (proposals, pos_count), 0)
+                chosen = chosen.astype(F32).astype(BF16)
+                along = lax.broadcasted_iota(jnp.int32, (1, pos_count), 1) + offset
+                inside = (along >= 0) & (along < proposals)
+                beneath = lax.broadcasted_iota(jnp.int32, (pos_count, 1), 0) + offset
+                placed = jnp.dot(
+                    picked.astype(F32).astype(BF16),
+                    lat_rows[rows, qrank : qrank + kvrank],
+                    preferred_element_type=F32,
+                )
+                lat[s] = jnp.where(
+                    (beneath >= 0) & (beneath < proposals), placed, lat[s].astype(F32)
+                ).astype(BF16)
+                new_rope = lat_rows[rows, qrank + kvrank :].astype(F32)[:, :rope_dim]
+                swapped = jnp.concatenate(
+                    [new_rope[:, half_dim:], new_rope[:, :half_dim]], axis=1
+                )
+                turn = query_turn[rows, :]
+                turned = (
+                    new_rope * turn[:, :rope_dim] + swapped * turn[:, rope_dim : 2 * rope_dim]
+                )
+                put = lax.dot_general(
+                    new_rope.astype(BF16), chosen, contract_first, preferred_element_type=F32
+                )
+                rope[s] = jnp.where(inside, put, rope32).astype(BF16)
+                put = lax.dot_general(
+                    turned.astype(BF16), chosen, contract_first, preferred_element_type=F32
+                )
+                k_rot[j] = jnp.where(inside, put, k_rot[j].astype(F32)).astype(BF16)
+                seen = jnp.dot(reach[s], chosen, preferred_element_type=F32)
+                shown = jnp.where((seen > 0.5) | (along < 0), 0.0, HIDDEN)
+                for h in range(heads):
+                    bias[j, h * proposals : (h + 1) * proposals, :] = shown
+
+        for j in range(block):
+            s = step * block + j
+            keys = lat[s]
+            score = lax.dot_general(
+                q_lat[s], keys, contract_last, preferred_element_type=F32
+            )
+            score = score + jnp.dot(
+                q_rot[s][:, :rope_dim], k_rot[j], preferred_element_type=F32
+            )
+            score = score * scale + bias[j]
+            top = jnp.maximum(jnp.max(score, axis=1, keepdims=True), LOWEST)
+            weights = jnp.exp(score - top)
+            total = jnp.sum(weights, axis=1, keepdims=True)
+            numer[j] = jnp.dot(weights.astype(BF16), keys, preferred_element_type=F32)
+            column = lax.broadcasted_iota(jnp.int32, (1, 128), 1)
+            terms = jnp.zeros((heads * proposals, 128), F32)
+            for first, rest in ((0, top), (3, total)):
+                for k in range(3):
+                    term = rest.astype(BF16).astype(F32)
+                    terms = jnp.where(column == first + k, term, terms)
+                    rest = rest - term
+            extra = jnp.transpose(terms)[:8].astype(BF16)
+            for c in range(chunks):
+                sent[s * chunks + c, 2 * proposals :, :] = extra
+
         for h in range(heads):
-            one = projected[:, h * lanes : (h + 1) * lanes]
-            mean = (
-                jnp.sum(jnp.where(counted, one * one, 0.0), axis=1, keepdims=True) / qkhead
+            part = numer[:, pl.ds(h * proposals, proposals), :]
+            part = part.reshape(block * proposals, kvrank)
+            upper = part.astype(BF16)
+            lower = (part - upper.astype(F32)).astype(BF16)
+            both = jnp.dot(
+                jnp.concatenate([upper, lower], axis=0), w_value[h], preferred_element_type=F32
             )
-            one = one * lax.rsqrt(mean + epsilon) * gain[...]
-            at = pl.ds(h * proposals, proposals)
-            moved = jnp.dot(one.astype(BF16), w_key[h], preferred_element_type=F32)
-            q_lat[:, at, :] = moved.astype(BF16).reshape(seq_count, proposals, kvrank)
-            turned = one * query_cos[...] + pltpu.roll(one, rope_dim, 1) * query_sin[...]
-            q_rot[:, at, :] = turned.astype(BF16).reshape(seq_count, proposals, lanes)
-
-    for j in range(block):
-        s = step * block + j
-        offset = base[0] - starts[s]
-        rope32 = cache_rope[j].astype(F32)
-        low, high = rope32[:half_dim], rope32[half_dim:]
-        cosine, sine = key_cos[...], key_sin[...]
-        k_rot[j, :half_dim] = (low * cosine - high * sine).astype(BF16)
-        k_rot[j, half_dim:] = (high * cosine + low * sine).astype(BF16)
-        hit = (offset > -pos_count) & (offset < proposals)
-
-        @pl.when(jnp.logical_not(hit))
-        def _():
-            lat_out[j] = cache_lat[j]
-            rope_out[j] = cache_rope[j]
-            bias[j] = jnp.full(bias.shape[1:], jnp.where(offset < 0, 0.0, HIDDEN), F32)
-
-        @pl.when(hit)
-        def _():
-            rows = pl.ds(pl.multiple_of(s * proposals, proposals), proposals)
-            down = lax.broadcasted_iota(jnp.int32, (pos_count, proposals), 0) + offset
-            picked = down == lax.broadcasted_iota(jnp.int32, (pos_count, proposals), 1)
-            across = lax.broadcasted_iota(jnp.int32, (proposals, pos_count), 1) + offset
-            chosen = across == lax.broadcasted_iota(jnp.int32, (proposals, pos_count), 0)
-            chosen = chosen.astype(F32).astype(BF16)
-            along = lax.broadcasted_iota(jnp.int32, (1, pos_count), 1) + offset
-            inside = (along >= 0) & (along < proposals)
-            beneath = lax.broadcasted_iota(jnp.int32, (pos_count, 1), 0) + offset
-            placed = jnp.dot(
-                picked.astype(F32).astype(BF16),
-                lat_rows[rows, qrank : qrank + kvrank],
-                preferred_element_type=F32,
-            )
-            lat_out[j] = jnp.where(
-                (beneath >= 0) & (beneath < proposals), placed, cache_lat[j].astype(F32)
-            ).astype(BF16)
-            new_rope = lat_rows[rows, qrank + kvrank :].astype(F32)[:, :rope_dim]
-            swapped = jnp.concatenate([new_rope[:, half_dim:], new_rope[:, :half_dim]], axis=1)
-            turned = (
-                new_rope * query_cos[rows, :rope_dim] + swapped * query_sin[rows, :rope_dim]
-            )
-            contract = (((0,), (0,)), ((), ()))
-            put = lax.dot_general(
-                new_rope.astype(BF16), chosen, contract, preferred_element_type=F32
-            )
-            rope_out[j] = jnp.where(inside, put, rope32).astype(BF16)
-            put = lax.dot_general(
-                turned.astype(BF16), chosen, contract, preferred_element_type=F32
-            )
-            k_rot[j] = jnp.where(inside, put, k_rot[j].astype(F32)).astype(BF16)
-            seen = jnp.dot(reach[s], chosen, preferred_element_type=F32)
-            shown = jnp.where((seen > 0.5) | (along < 0), 0.0, HIDDEN)
-            for h in range(heads):
-                bias[j, h * proposals : (h + 1) * proposals, :] = shown
-
-    for j in range(block):
-        s = step * block + j
-        keys = lat_out[j]
-        score = lax.dot_general(
-            q_lat[s], keys, (((1,), (1,)), ((), ())), preferred_element_type=F32
-        )
-        score = score + jnp.dot(
-            q_rot[s][:, :rope_dim], k_rot[j], preferred_element_type=F32
-        )
-        score = score * scale + bias[j]
-        top = jnp.maximum(jnp.max(score, axis=1, keepdims=True), LOWEST)
-        weights = jnp.exp(score - top)
-        total = jnp.sum(weights, axis=1, keepdims=True)
-        numer[j] = jnp.dot(weights.astype(BF16), keys, preferred_element_type=F32)
-        lane = lax.broadcasted_iota(jnp.int32, (1, 128), 1)
-        terms = jnp.zeros((heads * proposals, 128), F32)
-        for first, rest in ((0, top), (3, total)):
-            for k in range(3):
-                term = rest.astype(BF16).astype(F32)
-                terms = jnp.where(lane == first + k, term, terms)
-                rest = rest - term
-        extra = jnp.transpose(terms)[:8].astype(BF16)
-        for c in range(heads // 2):
-            sent[j * (heads // 2) + c, 2 * proposals :, :] = extra
-
-    for h in range(heads):
-        part = numer[:, pl.ds(h * proposals, proposals), :].reshape(block * proposals, kvrank)
-        upper = part.astype(BF16)
-        lower = (part - upper.astype(F32)).astype(BF16)
-        both = jnp.dot(
-            jnp.concatenate([upper, lower], axis=0), w_value[h], preferred_element_type=F32
-        )
-        value = (both[: block * proposals] + both[block * proposals :]).astype(BF16)
-        for j in range(block):
-            sent[
-                j * (heads // 2) + h // 2,
-                (h % 2) * proposals : (h % 2 + 1) * proposals,
-                :,
-            ] = value[j * proposals : (j + 1) * proposals]
-
-
-def attend(starts, base, lat_rows, weights, tables, reach, cache_lat, cache_rope):
-    w_query, gain, w_key, w_value = weights
+            value = (both[: block * proposals] + both[block * proposals :]).astype(BF16)
+            for j in range(block):
+                sent[
+                    (step * block + j) * chunks + h // 2,
+                    (h % 2) * proposals : (h % 2 + 1) * proposals,
+                    :,
+                ] = value[j * proposals : (j + 1) * proposals]
+        for copy in leaving(step):
+            copy.start()
+
+    for g in range(seq_count // block):
+        for copy in leaving(g):
+            copy.wait()
+
+
+def attend(starts, base, packed, gain, query_turn, reach, weights, key_turn, cache_rope, cache_lat):
+    w_query, w_key, w_value = weights
     seq_count, pos_count, kvrank = cache_lat.shape
     rope_dim = cache_rope.shape[1]
     heads, lanes, _ = w_key.shape
+    qrank = w_query.shape[0]
     proposals = reach.shape[2]
     rows = heads * proposals
-    lat_width = w_query.shape[0] + kvrank + 128
     block = 4
     whole = pl.BlockSpec(memory_space=pltpu.VMEM)
     smem = pl.BlockSpec(memory_space=pltpu.SMEM)
-    lat_spec = pl.BlockSpec((block, pos_count, kvrank), lambda g: (g, 0, 0))
-    rope_spec = pl.BlockSpec((block, rope_dim, pos_count), lambda g: (g, 0, 0))
-    chunks = heads // 2
-    sent_shape = (seq_count * chunks, 2 * proposals + 8, w_value.shape[2])
+    outside = pl.BlockSpec(memory_space=pltpu.HBM)
+    sent_shape = (seq_count * heads // 2, 2 * proposals + 8, w_value.shape[2])
+    groups = seq_count // block
     return pl.pallas_call(
         attend_kernel,
-        grid=(seq_count // block,),
-        in_specs=[smem, smem, *[whole] * 10, lat_spec, rope_spec],
-        out_specs=[
-            lat_spec,
-            rope_spec,
-            pl.BlockSpec((block * chunks, *sent_shape[1:]), lambda g: (g, 0, 0)),
-        ],
+        in_specs=[smem, smem, *[whole] * 8, outside, outside],
+        out_specs=[outside] * 3,
         out_shape=[
-            jax.ShapeDtypeStruct(cache_lat.shape, BF16),
-            jax.ShapeDtypeStruct(cache_rope.shape, BF16),
-            jax.ShapeDtypeStruct(sent_shape, BF16),
+            pltpu.HBM(cache_lat.shape, BF16),
+            pltpu.HBM(cache_rope.shape, BF16),
+            pltpu.HBM(sent_shape, BF16),
         ],
         scratch_shapes=[
             pltpu.VMEM((seq_count, rows, kvrank), BF16),
@@ -331,12 +358,17 @@
             pltpu.VMEM((block, rope_dim, pos_count), BF16),
             pltpu.VMEM((block, rows, pos_count), F32),
             pltpu.VMEM((block, rows, kvrank), F32),
-            pltpu.VMEM((seq_count * proposals, lat_width), BF16),
+            pltpu.VMEM((seq_count * proposals, qrank + kvrank + 128), BF16),
+            pltpu.VMEM(cache_lat.shape, BF16),
+            pltpu.VMEM(cache_rope.shape, BF16),
+            pltpu.VMEM(sent_shape, BF16),
+            *[pltpu.SemaphoreType.DMA((groups,))] * 5,
         ],
+        compiler_params=pltpu.CompilerParams(vmem_limit_bytes=50 * 1024 * 1024),
         cost_estimate=pl.CostEstimate(
             flops=10**9, bytes_accessed=8 * 10**6, transcendentals=10**6
         ),
-    )(starts, base, lat_rows, w_query, gain, w_key, w_value, *tables, reach, cache_lat, cache_rope)
+    )(starts, base, packed, gain, query_turn, reach, *weights, key_turn, cache_rope, cache_lat)
 
 
 def project_kernel(heads_in, w_out, result):
@@ -412,16 +444,14 @@
     angles = rope_angles(starts[:, None] + depths, half_dim).reshape(rows, half_dim)
     cosine, sine = jnp.cos(angles), jnp.sin(angles)
     lanes = qkhead + rope_dim
-    spare = ((0, 0), (0, lanes - rope_dim))
     pos_count = cache_lat.shape[1]
     base = lax.axis_index(KV) * pos_count
     slot_angles = rope_angles(base + jnp.arange(pos_count, dtype=jnp.int32), half_dim).T
-    tables = (
-        jnp.pad(jnp.concatenate([cosine, cosine], axis=1), spare),
-        jnp.pad(jnp.concatenate([-sine, sine], axis=1), spare),
-        jnp.cos(slot_angles),
-        jnp.sin(slot_angles),
-    )
+    query_turn = jnp.pad(
+        jnp.concatenate([cosine, cosine, -sine, sine], axis=1),
+        ((0, 0), (0, lanes - 2 * rope_dim)),
+    )
+    key_turn = jnp.concatenate([jnp.cos(slot_angles), jnp.sin(slot_angles)], axis=0)
 
     def arranged(values):
         nope, low, high = jnp.split(values, [nope_dim, nope_dim + half_dim], axis=-1)
@@ -429,13 +459,20 @@
 
     weights = (
         arranged(w_qup).reshape(qrank, heads_here * lanes),
-        arranged(gain_q)[None],
         jnp.pad(jnp.transpose(w_ukey, (1, 2, 0)), ((0, 0), (rope_dim, rope_dim), (0, 0))),
         jnp.transpose(w_uval, (1, 0, 2)),
     )
-    reach = reaches.astype(BF16)
     lat_out, rope_out, sent = attend(
-        starts, base[None], everyone, weights, tables, reach, cache_lat, cache_rope
+        starts,
+        base[None],
+        everyone,
+        arranged(gain_q)[None],
+        query_turn,
+        reaches.astype(BF16),
+        weights,
+        key_turn,
+        cache_rope,
+        cache_lat,
     )
     arrived = exchange(sent, KV).astype(F32)
     group = 2 * proposals

time: 150 us -> 148 us (0.987)
  the two profiles are of different devices: /device:TPU:2 before, /device:TPU:4 now
where the time goes in v4:
time: 148 us
  waiting for transfers between devices  62.6 us (42%)
  starting transfers between devices  31.5 us (21%)
  blocking collectives  31.3 us (21%)
  Pallas kernels  13 us (9%)
  local copies, waits for them, and re-layouts  3.71 us (3%)
  other arithmetic  3.16 us (2%)
    all_to_all x4, waiting for transfers between devices, exchange(): return lax.all_to_all(parts, axes, split_axis=0, concat_axis=0, tiled=True)  62.6 us
    all_to_all x4, starting transfers between devices, exchange(): return lax.all_to_all(parts, axes, split_axis=0, concat_axis=0, tiled=True)  31.5 us
    all_to_all x1, blocking collectives, exchange(): return lax.all_to_all(parts, axes, split_axis=0, concat_axis=0, tiled=True)  25 us
    pallas_call x1, Pallas kernels, attend(): pl.pallas_call(attend_kernel, in_specs=[smem, smem, *[whole] * 8, outside...  9.99 us
  transfers between devices with their start and end apart: 4, of which 4 were waited for; matrix products, arithmetic and copies ran while one was open for 3% of the time, Pallas kernels for 0%

profile of v4, /device:TPU:4, one launch (start us, length us, event | category | flops | bytes accessed | tf_op | source)
XLA Modules:
  0.0 147.8 jit_solution(7735759346864651720)
XLA Ops:
  0.7 1.7 %shard_map.193 = bf16[32,1152]{1,0:T(8,128)(2,1)} custom-call(s32[1]{0:T(128)} %bitcast.1.index, bf16[16,16,16]{2,1,0:T(8,128)(2,1)} %tokens.1, f32[1,16]{1,0:T(1,128)} %bitcast.53, bf16[16,512]{1,0:T(8,128)(2,1)} %w_qdown.1, bf16[16,256]{1,0:T(8,128)(2,1)} %w_kvdown.1, bf16[32,2048]{1,0:T(8,128)(2,1)} %bitcast.50), custom_call_target="tpu_custom_call" | custom-call | flops 100000 | bytes 100000 | tf_op jit(solution)/shard_map/pallas_call | solution.py:92
  2.4 2.1 %all_gather.12 = bf16[64,1152]{1,0:T(8,128)(2,1)S(1)} all-gather(bf16[32,1152]{1,0:T(8,128)(2,1)} %shard_map.193), channel_id=1, replica_groups=mesh['dp'=4,'kv_0'=8,'kv_1'=8,'tp'=2] {'tp'}, dimensions={0}, use_global_device_ids=true | all-gather | bytes 221184 | tf_op jit(solution)/shard_map/all_gather | solution.py:434
  4.8 1.0 reshape.128
  5.8 16.7 %all-to-all-start = ((f32[64,2,896]{2,1,0:T(2,128)}), f32[64,2,896]{2,1,0:T(2,128)S(1)}, u32[]{:S(2)}, u32[]{:S(2)}) async-start(f32[64,2,896]{2,1,0:T(2,128)} %reshape.128), calls=%async_computation | async-start | bytes 917504 | tf_op jit(solution)/shard_map/all_to_all | solution.py:22
  23.8 0.4 convert_reduce_fusion
  24.4 16.9 %all-to-all-done.arrived = f32[64,2,896]{2,1,0:T(2,128)S(1)} async-done(((f32[64,2,896]{2,1,0:T(2,128)}), f32[64,2,896]{2,1,0:T(2,128)S(1)}, u32[]{:S(2)}, u32[]{:S(2)}) %all-to-all-start) | async-done | bytes 458784 | tf_op jit(solution)/shard_map/all_to_all | solution.py:22
  41.3 1.0 shard_map.194
  42.3 4.9 %all-to-all-start.1 = ((bf16[64,16,128]{2,1,0:T(8,128)(2,1)}), bf16[64,16,128]{2,1,0:T(8,128)(2,1)S(1)}, u32[]{:S(2)}, u32[]{:S(2)}) async-start(bf16[64,16,128]{2,1,0:T(8,128)(2,1)} %shard_map.194), calls=%async_computation.1 | async-start | bytes 524288 | tf_op jit(solution)/shard_map/all_to_all | solution.py:22
  47.4 0.5 copy.83.w_query
  48.0 1.0 pad.9.w_key
  49.1 0.5 multiply_cosine_fusion
  49.8 11.7 %all-to-all-done.1 = bf16[64,16,128]{2,1,0:T(8,128)(2,1)S(1)} async-done(((bf16[64,16,128]{2,1,0:T(8,128)(2,1)}), bf16[64,16,128]{2,1,0:T(8,128)(2,1)S(1)}, u32[]{:S(2)}, u32[]{:S(2)}) %all-to-all-start.1) | async-done | bytes 262176 | tf_op jit(solution)/shard_map/all_to_all | solution.py:22
  61.5 2.2 %all_gather.13.packed = bf16[128,16,128]{2,1,0:T(8,128)(2,1)S(1)} all-gather(bf16[64,16,128]{2,1,0:T(8,128)(2,1)S(1)} %all-to-all-done.1), channel_id=1, replica_groups=mesh['dp'=4,'kv_0'=8,'kv_1'=8,'tp'=2] {'tp'}, dimensions={0}, use_global_device_ids=true | all-gather | bytes 786432 | tf_op jit(solution)/shard_map/all_gather | solution.py:441
  63.7 10.0 %shard_map.195 = (bf16[16,256,256]{2,1,0:T(8,128)(2,1)}, bf16[16,32,256]{2,1,0:T(8,128)(2,1)}, bf16[64,40,128]{2,1,0:T(8,128)(2,1)}) custom-call(s32[16]{0:T(128)S(1)} %add.110.starts, s32[1]{0:T(128)} %bitcast.base, bf16[128,16,128]{2,1,0:T(8,128)(2,1)S(1)} %all_gather.13.packed, f32[1,128]{1,0:T(1,128)S(1)} %maximum_bitcast_fusion.gain, ...), custom_call_target="tpu_custom_call" | custom-call | flops 1000000000 | bytes 8000000 | tf_op jit(solution)/shard_map/pallas_call | solution.py:346
  73.7 4.7 %all-to-all-start.2 = ((bf16[64,40,128]{2,1,0:T(8,128)(2,1)}), bf16[64,40,128]{2,1,0:T(8,128)(2,1)S(1)}, u32[]{:S(2)}, u32[]{:S(2)}) async-start(bf16[64,40,128]{2,1,0:T(8,128)(2,1)} %get-tuple-element.6), calls=%async_computation.2 | async-start | bytes 1310720 | tf_op jit(solution)/shard_map/all_to_all | solution.py:22
  78.3 21.8 %all-to-all-done.2 = bf16[64,40,128]{2,1,0:T(8,128)(2,1)S(1)} async-done(((bf16[64,40,128]{2,1,0:T(8,128)(2,1)}), bf16[64,40,128]{2,1,0:T(8,128)(2,1)S(1)}, u32[]{:S(2)}, u32[]{:S(2)}) %all-to-all-start.2) | async-done | bytes 655392 | tf_op jit(solution)/shard_map/all_to_all | solution.py:22
  100.2 0.5 constant_dynamic-slice_fusion.1
  100.8 0.3 fusion.3
  101.3 25.0 %all_to_all.25 = bf16[64,32,128]{2,1,0:T(8,128)(2,1)S(1)} all-to-all(bf16[64,32,128]{2,1,0:T(8,128)(2,1)S(1)} %broadcast_in_dim.22), channel_id=1, replica_groups=mesh['dp'=4,'kv_0'=8,'kv_1'=8,'tp'=2] {'kv_0','kv_1'}, dimensions={0} | all-to-all | bytes 1048576 | tf_op jit(solution)/shard_map/all_to_all | solution.py:22
  126.6 2.0 %all-gather = f32[512,32]{1,0:T(8,128)S(1)} all-gather(f32[256,32]{1,0:T(8,128)S(1)} %shard_map.196), channel_id=2, replica_groups=mesh['dp'=4,'kv_0'=8,'kv_1'=8,'tp'=2] {'tp'}, dimensions={0}, use_global_device_ids=true | all-gather | bytes 98304 | tf_op jit(solution)/shard_map/all_gather | solution.py:489
  128.8 0.7 broadcast_in_dim.23
  129.5 5.2 %all-to-all-start.4 = ((f32[64,1,256]{2,1,0:T(1,128)}), f32[64,1,256]{2,1,0:T(1,128)S(1)}, u32[]{:S(2)}, u32[]{:S(2)}) async-start(f32[64,1,256]{2,1,0:T(1,128)} %broadcast_in_dim.23), calls=%async_computation.4 | async-start | bytes 131072 | tf_op jit(solution)/shard_map/all_to_all | solution.py:22
  134.6 12.2 %all-to-all-done.4 = f32[64,1,256]{2,1,0:T(1,128)S(1)} async-done(((f32[64,1,256]{2,1,0:T(1,128)}), f32[64,1,256]{2,1,0:T(1,128)S(1)}, u32[]{:S(2)}, u32[]{:S(2)}) %all-to-all-start.4) | async-done | bytes 65568 | tf_op jit(solution)/shard_map/all_to_all | solution.py:22
  147.0 0.8 multiply_convert_fusion
  (57 shorter events, 2.8 us)
Async XLA Ops:
  0.6 22.0 %copy-start.4 = (bf16[512,8,96]{0,2,1:T(8,128)(2,1)S(1)}, bf16[512,8,96]{0,2,1:T(8,128)(2,1)}, u32[]{:S(2)}) copy-start(bf16[512,8,96]{0,2,1:T(8,128)(2,1)} %param.25) | copy-start | bytes 2359300
  4.8 17.9 %copy-start.8 = (s32[16,16]{1,0:T(8,128)S(1)}, s32[16,16]{1,0:T(8,128)}, u32[]{:S(2)}) copy-start(s32[16,16]{1,0:T(8,128)} %param.33) | copy-start | bytes 3076
  4.8 18.6 %copy-start.6 = (f32[96]{0:T(128)S(1)}, f32[96]{0:T(128)}, u32[]{:S(2)}) copy-start(f32[96]{0:T(128)} %param.26) | copy-start | bytes 1156
  5.8 17.8 %copy-start.9 = (s32[16]{0:T(128)S(1)}, s32[16]{0:T(128)}, u32[]{:S(2)}) copy-start(s32[16]{0:T(128)} %param.34) | copy-start | bytes 196
  5.8 17.8 %copy-start.10 = (s32[16]{0:T(128)S(1)}, s32[16]{0:T(128)}, u32[]{:S(2)}) copy-start(s32[16]{0:T(128)} %param.35) | copy-start | bytes 196
  5.8 17.8 %slice-start = ((bf16[512,8,96]{0,2,1:T(8,128)(2,1)}), bf16[512,8,64]{0,2,1:T(8,128)(2,1)S(1)}, s32[]{:S(2)}) async-start(bf16[512,8,96]{0,2,1:T(8,128)(2,1)} %param.25), calls=%async_computation.5 | async-start | bytes 1048576 | tf_op jit(solution)/shard_map/split | solution.py:457
  5.8 17.8 %slice-start.1 = ((bf16[512,8,96]{0,2,1:T(8,128)(2,1)}), bf16[512,8,32]{0,2,1:T(8,128)(2,1)S(1)}, s32[]{:S(2)}) async-start(bf16[512,8,96]{0,2,1:T(8,128)(2,1)} %param.25), calls=%async_computation.6 | async-start | bytes 524288 | tf_op jit(solution)/shard_map/split | solution.py:457
  5.8 35.4 %all-to-all-start = ((f32[64,2,896]{2,1,0:T(2,128)}), f32[64,2,896]{2,1,0:T(2,128)S(1)}, u32[]{:S(2)}, u32[]{:S(2)}) async-start(f32[64,2,896]{2,1,0:T(2,128)} %reshape.128), calls=%async_computation | async-start | bytes 917504 | tf_op jit(solution)/shard_map/all_to_all | solution.py:22
  22.6 18.6 %copy-start.2 = (f32[512]{0:T(512)S(1)}, f32[512]{0:T(512)}, u32[]{:S(2)}) copy-start(f32[512]{0:T(512)} %param.23) | copy-start | bytes 6148
  22.6 18.6 %copy-start.3 = (f32[256]{0:T(256)S(1)}, f32[256]{0:T(256)}, u32[]{:S(2)}) copy-start(f32[256]{0:T(256)} %param.24) | copy-start | bytes 3076
  23.7 24.2 %copy-start.5 = (bf16[256,8,128]{2,1,0:T(8,128)(2,1)S(1)}, bf16[256,8,128]{2,1,0:T(8,128)(2,1)}, u32[]{:S(2)}) copy-start(bf16[256,8,128]{2,1,0:T(8,128)(2,1)} %param.28) | copy-start | bytes 1572868
  42.3 19.2 %all-to-all-start.1 = ((bf16[64,16,128]{2,1,0:T(8,128)(2,1)}), bf16[64,16,128]{2,1,0:T(8,128)(2,1)S(1)}, u32[]{:S(2)}, u32[]{:S(2)}) async-start(bf16[64,16,128]{2,1,0:T(8,128)(2,1)} %shard_map.194), calls=%async_computation.1 | async-start | bytes 524288 | tf_op jit(solution)/shard_map/all_to_all | solution.py:22
  48.0 15.7 %copy-start = (bf16[16,32,256]{2,1,0:T(8,128)(2,1)S(1)}, bf16[16,32,256]{2,1,0:T(8,128)(2,1)}, u32[]{:S(2)}) copy-start(bf16[16,32,256]{2,1,0:T(8,128)(2,1)} %cache_rope.1) | copy-start | bytes 786436
  73.7 26.5 %all-to-all-start.2 = ((bf16[64,40,128]{2,1,0:T(8,128)(2,1)}), bf16[64,40,128]{2,1,0:T(8,128)(2,1)S(1)}, u32[]{:S(2)}, u32[]{:S(2)}) async-start(bf16[64,40,128]{2,1,0:T(8,128)(2,1)} %get-tuple-element.6), calls=%async_computation.2 | async-start | bytes 1310720 | tf_op jit(solution)/shard_map/all_to_all | solution.py:22
  100.7 25.7 %copy-start.1 = (bf16[1024,32]{0,1:T(8,128)(2,1)S(1)}, bf16[1024,32]{0,1:T(8,128)(2,1)}, u32[]{:S(2)}) copy-start(bf16[1024,32]{0,1:T(8,128)(2,1)} %param.29) | copy-start | bytes 196612
  100.8 46.2 %copy-start.7 = (f32[16]{0:T(128)S(1)}, f32[16]{0:T(128)}, u32[]{:S(2)}) copy-start(f32[16]{0:T(128)} %param.30) | copy-start | bytes 196
  129.5 17.4 %all-to-all-start.4 = ((f32[64,1,256]{2,1,0:T(1,128)}), f32[64,1,256]{2,1,0:T(1,128)S(1)}, u32[]{:S(2)}, u32[]{:S(2)}) async-start(f32[64,1,256]{2,1,0:T(1,128)} %broadcast_in_dim.23), calls=%async_computation.4 | async-start | bytes 131072 | tf_op jit(solution)/shard_map/all_to_all | solution.py:22

commit v5 on v4

--- a/solution.py
+++ b/solution.py
@@ -102,7 +102,7 @@
             ],
             out_specs=whole,
         ),
-        out_shape=jax.ShapeDtypeStruct(shape, BF16),
+        out_shape=pltpu.VMEM(shape, BF16),
         cost_estimate=pl.CostEstimate(flops=10**5, bytes_accessed=10**5, transcendentals=0),
     )(index, tokens, gain_in[None], w_qdown, w_kvdown, w_ropek.T)
 
@@ -281,6 +281,8 @@
                 for h in range(heads):
                     bias[j, h * proposals : (h + 1) * proposals, :] = shown
 
+        for copy in leaving(step)[:2]:
+            copy.start()
         for j in range(block):
             s = step * block + j
             keys = lat[s]
@@ -321,8 +323,7 @@
                     (h % 2) * proposals : (h % 2 + 1) * proposals,
                     :,
                 ] = value[j * proposals : (j + 1) * proposals]
-        for copy in leaving(step):
-            copy.start()
+        leaving(step)[2].start()
 
     for g in range(seq_count // block):
         for copy in leaving(g):
@@ -337,7 +338,7 @@
     qrank = w_query.shape[0]
     proposals = reach.shape[2]
     rows = heads * proposals
-    block = 4
+    block = 16
     whole = pl.BlockSpec(memory_space=pltpu.VMEM)
     smem = pl.BlockSpec(memory_space=pltpu.SMEM)
     outside = pl.BlockSpec(memory_space=pltpu.HBM)

time: 148 us -> 147 us (level)
  Pallas kernels: 13 us -> 11.5 us
where the time goes in v5:
time: 147 us; the launch traced here: 146 us
  waiting for transfers between devices  62.6 us (43%)
  starting transfers between devices  31.7 us (22%)
  blocking collectives  31.1 us (21%)
  Pallas kernels  11.5 us (8%)
  local copies, waits for them, and re-layouts  3.71 us (3%)
  other arithmetic  3.15 us (2%)
    all_to_all x4, waiting for transfers between devices, exchange(): return lax.all_to_all(parts, axes, split_axis=0, concat_axis=0, tiled=True)  62.6 us
    all_to_all x4, starting transfers between devices, exchange(): return lax.all_to_all(parts, axes, split_axis=0, concat_axis=0, tiled=True)  31.7 us
    all_to_all x1, blocking collectives, exchange(): return lax.all_to_all(parts, axes, split_axis=0, concat_axis=0, tiled=True)  25 us
    pallas_call x1, Pallas kernels, attend(): pl.pallas_call(attend_kernel, in_specs=[smem, smem, *[whole] * 8, outside...  9.07 us
  transfers between devices with their start and end apart: 4, of which 4 were waited for; matrix products, arithmetic and copies ran while one was open for 3% of the time, Pallas kernels for 0%

profile of v5, /device:TPU:4, one launch (start us, length us, event | category | flops | bytes accessed | tf_op | source)
XLA Modules:
  0.0 146.2 jit_solution(9257201948576635859)
XLA Ops:
  0.7 1.1 shard_map.193
  1.8 1.9 %all_gather.12 = bf16[64,1152]{1,0:T(8,128)(2,1)S(1)} all-gather(bf16[32,1152]{1,0:T(8,128)(2,1)S(1)} %shard_map.193), channel_id=1, replica_groups=mesh['dp'=4,'kv_0'=8,'kv_1'=8,'tp'=2] {'tp'}, dimensions={0}, use_global_device_ids=true | all-gather | bytes 221184 | tf_op jit(solution)/shard_map/all_gather | solution.py:435
  4.0 1.0 reshape.128
  5.0 16.7 %all-to-all-start = ((f32[64,2,896]{2,1,0:T(2,128)}), f32[64,2,896]{2,1,0:T(2,128)S(1)}, u32[]{:S(2)}, u32[]{:S(2)}) async-start(f32[64,2,896]{2,1,0:T(2,128)} %reshape.128), calls=%async_computation | async-start | bytes 917504 | tf_op jit(solution)/shard_map/all_to_all | solution.py:22
  23.0 0.4 convert_reduce_fusion
  23.5 16.9 %all-to-all-done.arrived = f32[64,2,896]{2,1,0:T(2,128)S(1)} async-done(((f32[64,2,896]{2,1,0:T(2,128)}), f32[64,2,896]{2,1,0:T(2,128)S(1)}, u32[]{:S(2)}, u32[]{:S(2)}) %all-to-all-start) | async-done | bytes 458784 | tf_op jit(solution)/shard_map/all_to_all | solution.py:22
  40.4 1.0 shard_map.194
  41.5 4.9 %all-to-all-start.1 = ((bf16[64,16,128]{2,1,0:T(8,128)(2,1)}), bf16[64,16,128]{2,1,0:T(8,128)(2,1)S(1)}, u32[]{:S(2)}, u32[]{:S(2)}) async-start(bf16[64,16,128]{2,1,0:T(8,128)(2,1)} %shard_map.194), calls=%async_computation.1 | async-start | bytes 524288 | tf_op jit(solution)/shard_map/all_to_all | solution.py:22
  46.6 0.5 copy.83.w_query
  47.2 1.0 pad.9.w_key
  48.2 0.5 multiply_cosine_fusion
  48.9 11.7 %all-to-all-done.1 = bf16[64,16,128]{2,1,0:T(8,128)(2,1)S(1)} async-done(((bf16[64,16,128]{2,1,0:T(8,128)(2,1)}), bf16[64,16,128]{2,1,0:T(8,128)(2,1)S(1)}, u32[]{:S(2)}, u32[]{:S(2)}) %all-to-all-start.1) | async-done | bytes 262176 | tf_op jit(solution)/shard_map/all_to_all | solution.py:22
  60.7 2.2 %all_gather.13.packed = bf16[128,16,128]{2,1,0:T(8,128)(2,1)S(1)} all-gather(bf16[64,16,128]{2,1,0:T(8,128)(2,1)S(1)} %all-to-all-done.1), channel_id=1, replica_groups=mesh['dp'=4,'kv_0'=8,'kv_1'=8,'tp'=2] {'tp'}, dimensions={0}, use_global_device_ids=true | all-gather | bytes 786432 | tf_op jit(solution)/shard_map/all_gather | solution.py:442
  62.8 9.1 %shard_map.195 = (bf16[16,256,256]{2,1,0:T(8,128)(2,1)}, bf16[16,32,256]{2,1,0:T(8,128)(2,1)}, bf16[64,40,128]{2,1,0:T(8,128)(2,1)}) custom-call(s32[16]{0:T(128)S(1)} %add.110.starts, s32[1]{0:T(128)} %bitcast.base, bf16[128,16,128]{2,1,0:T(8,128)(2,1)S(1)} %all_gather.13.packed, f32[1,128]{1,0:T(1,128)S(1)} %maximum_bitcast_fusion.gain, ...), custom_call_target="tpu_custom_call" | custom-call | flops 1000000000 | bytes 8000000 | tf_op jit(solution)/shard_map/pallas_call | solution.py:347
  71.9 4.9 %all-to-all-start.2 = ((bf16[64,40,128]{2,1,0:T(8,128)(2,1)}), bf16[64,40,128]{2,1,0:T(8,128)(2,1)S(1)}, u32[]{:S(2)}, u32[]{:S(2)}) async-start(bf16[64,40,128]{2,1,0:T(8,128)(2,1)} %get-tuple-element.6), calls=%async_computation.2 | async-start | bytes 1310720 | tf_op jit(solution)/shard_map/all_to_all | solution.py:22
  76.8 21.7 %all-to-all-done.2 = bf16[64,40,128]{2,1,0:T(8,128)(2,1)S(1)} async-done(((bf16[64,40,128]{2,1,0:T(8,128)(2,1)}), bf16[64,40,128]{2,1,0:T(8,128)(2,1)S(1)}, u32[]{:S(2)}, u32[]{:S(2)}) %all-to-all-start.2) | async-done | bytes 655392 | tf_op jit(solution)/shard_map/all_to_all | solution.py:22
  98.6 0.5 constant_dynamic-slice_fusion.1
  99.3 0.3 fusion.3
  99.8 25.0 %all_to_all.25 = bf16[64,32,128]{2,1,0:T(8,128)(2,1)S(1)} all-to-all(bf16[64,32,128]{2,1,0:T(8,128)(2,1)S(1)} %broadcast_in_dim.22), channel_id=1, replica_groups=mesh['dp'=4,'kv_0'=8,'kv_1'=8,'tp'=2] {'kv_0','kv_1'}, dimensions={0} | all-to-all | bytes 1048576 | tf_op jit(solution)/shard_map/all_to_all | solution.py:22
  125.1 2.0 %all-gather = f32[512,32]{1,0:T(8,128)S(1)} all-gather(f32[256,32]{1,0:T(8,128)S(1)} %shard_map.196), channel_id=2, replica_groups=mesh['dp'=4,'kv_0'=8,'kv_1'=8,'tp'=2] {'tp'}, dimensions={0}, use_global_device_ids=true | all-gather | bytes 98304 | tf_op jit(solution)/shard_map/all_gather | solution.py:490
  127.2 0.7 broadcast_in_dim.23
  127.9 5.2 %all-to-all-start.4 = ((f32[64,1,256]{2,1,0:T(1,128)}), f32[64,1,256]{2,1,0:T(1,128)S(1)}, u32[]{:S(2)}, u32[]{:S(2)}) async-start(f32[64,1,256]{2,1,0:T(1,128)} %broadcast_in_dim.23), calls=%async_computation.4 | async-start | bytes 131072 | tf_op jit(solution)/shard_map/all_to_all | solution.py:22
  133.1 12.2 %all-to-all-done.4 = f32[64,1,256]{2,1,0:T(1,128)S(1)} async-done(((f32[64,1,256]{2,1,0:T(1,128)}), f32[64,1,256]{2,1,0:T(1,128)S(1)}, u32[]{:S(2)}, u32[]{:S(2)}) %all-to-all-start.4) | async-done | bytes 65568 | tf_op jit(solution)/shard_map/all_to_all | solution.py:22
  145.4 0.8 multiply_convert_fusion
  (57 shorter events, 2.8 us)
Async XLA Ops:
  0.6 21.1 %copy-start.4 = (bf16[512,8,96]{0,2,1:T(8,128)(2,1)S(1)}, bf16[512,8,96]{0,2,1:T(8,128)(2,1)}, u32[]{:S(2)}) copy-start(bf16[512,8,96]{0,2,1:T(8,128)(2,1)} %param.25) | copy-start | bytes 2359300
  3.9 17.9 %copy-start.8 = (s32[16,16]{1,0:T(8,128)S(1)}, s32[16,16]{1,0:T(8,128)}, u32[]{:S(2)}) copy-start(s32[16,16]{1,0:T(8,128)} %param.33) | copy-start | bytes 3076
  3.9 18.6 %copy-start.6 = (f32[96]{0:T(128)S(1)}, f32[96]{0:T(128)}, u32[]{:S(2)}) copy-start(f32[96]{0:T(128)} %param.26) | copy-start | bytes 1156
  5.0 17.8 %copy-start.9 = (s32[16]{0:T(128)S(1)}, s32[16]{0:T(128)}, u32[]{:S(2)}) copy-start(s32[16]{0:T(128)} %param.34) | copy-start | bytes 196
  5.0 17.8 %copy-start.10 = (s32[16]{0:T(128)S(1)}, s32[16]{0:T(128)}, u32[]{:S(2)}) copy-start(s32[16]{0:T(128)} %param.35) | copy-start | bytes 196
  5.0 17.8 %slice-start = ((bf16[512,8,96]{0,2,1:T(8,128)(2,1)}), bf16[512,8,64]{0,2,1:T(8,128)(2,1)S(1)}, s32[]{:S(2)}) async-start(bf16[512,8,96]{0,2,1:T(8,128)(2,1)} %param.25), calls=%async_computation.5 | async-start | bytes 1048576 | tf_op jit(solution)/shard_map/split | solution.py:458
  5.0 17.8 %slice-start.1 = ((bf16[512,8,96]{0,2,1:T(8,128)(2,1)}), bf16[512,8,32]{0,2,1:T(8,128)(2,1)S(1)}, s32[]{:S(2)}) async-start(bf16[512,8,96]{0,2,1:T(8,128)(2,1)} %param.25), calls=%async_computation.6 | async-start | bytes 524288 | tf_op jit(solution)/shard_map/split | solution.py:458
  5.0 35.4 %all-to-all-start = ((f32[64,2,896]{2,1,0:T(2,128)}), f32[64,2,896]{2,1,0:T(2,128)S(1)}, u32[]{:S(2)}, u32[]{:S(2)}) async-start(f32[64,2,896]{2,1,0:T(2,128)} %reshape.128), calls=%async_computation | async-start | bytes 917504 | tf_op jit(solution)/shard_map/all_to_all | solution.py:22
  21.8 18.6 %copy-start.2 = (f32[512]{0:T(512)S(1)}, f32[512]{0:T(512)}, u32[]{:S(2)}) copy-start(f32[512]{0:T(512)} %param.23) | copy-start | bytes 6148
  21.8 18.6 %copy-start.3 = (f32[256]{0:T(256)S(1)}, f32[256]{0:T(256)}, u32[]{:S(2)}) copy-start(f32[256]{0:T(256)} %param.24) | copy-start | bytes 3076
  22.9 24.2 %copy-start.5 = (bf16[256,8,128]{2,1,0:T(8,128)(2,1)S(1)}, bf16[256,8,128]{2,1,0:T(8,128)(2,1)}, u32[]{:S(2)}) copy-start(bf16[256,8,128]{2,1,0:T(8,128)(2,1)} %param.28) | copy-start | bytes 1572868
  41.5 19.2 %all-to-all-start.1 = ((bf16[64,16,128]{2,1,0:T(8,128)(2,1)}), bf16[64,16,128]{2,1,0:T(8,128)(2,1)S(1)}, u32[]{:S(2)}, u32[]{:S(2)}) async-start(bf16[64,16,128]{2,1,0:T(8,128)(2,1)} %shard_map.194), calls=%async_computation.1 | async-start | bytes 524288 | tf_op jit(solution)/shard_map/all_to_all | solution.py:22
  47.1 15.7 %copy-start = (bf16[16,32,256]{2,1,0:T(8,128)(2,1)S(1)}, bf16[16,32,256]{2,1,0:T(8,128)(2,1)}, u32[]{:S(2)}) copy-start(bf16[16,32,256]{2,1,0:T(8,128)(2,1)} %cache_rope.1) | copy-start | bytes 786436
  71.9 26.7 %all-to-all-start.2 = ((bf16[64,40,128]{2,1,0:T(8,128)(2,1)}), bf16[64,40,128]{2,1,0:T(8,128)(2,1)S(1)}, u32[]{:S(2)}, u32[]{:S(2)}) async-start(bf16[64,40,128]{2,1,0:T(8,128)(2,1)} %get-tuple-element.6), calls=%async_computation.2 | async-start | bytes 1310720 | tf_op jit(solution)/shard_map/all_to_all | solution.py:22
  99.1 25.7 %copy-start.1 = (bf16[1024,32]{0,1:T(8,128)(2,1)S(1)}, bf16[1024,32]{0,1:T(8,128)(2,1)}, u32[]{:S(2)}) copy-start(bf16[1024,32]{0,1:T(8,128)(2,1)} %param.29) | copy-start | bytes 196612
  99.2 46.2 %copy-start.7 = (f32[16]{0:T(128)S(1)}, f32[16]{0:T(128)}, u32[]{:S(2)}) copy-start(f32[16]{0:T(128)} %param.30) | copy-start | bytes 196
  127.9 17.4 %all-to-all-start.4 = ((f32[64,1,256]{2,1,0:T(1,128)}), f32[64,1,256]{2,1,0:T(1,128)S(1)}, u32[]{:S(2)}, u32[]{:S(2)}) async-start(f32[64,1,256]{2,1,0:T(1,128)} %broadcast_in_dim.23), calls=%async_computation.4 | async-start | bytes 131072 | tf_op jit(solution)/shard_map/all_to_all | solution.py:22

commit v6 on v5

--- a/solution.py
+++ b/solution.py
@@ -122,13 +122,12 @@
             normed(summed[:, :qrank] * rescale, gain_qlat[...]),
             normed(summed[:, qrank:at] * rescale, gain_kvlat[...]),
             jnp.where(lane < rope_dim, last * rescale, 0.0),
-            jnp.zeros(last.shape, F32),
         ],
         axis=1,
     )
-    pieces = [share[:, c * lanes : (c + 1) * lanes] for c in range(share.shape[1] // lanes)]
-    stacked = jnp.concatenate(pieces, axis=0).astype(BF16)
-    out[...] = jnp.broadcast_to(stacked[None], out.shape)
+    for c in range(share.shape[1] // lanes):
+        piece = share[:, c * lanes : (c + 1) * lanes].astype(BF16)
+        out[:, c] = jnp.broadcast_to(piece[None], (out.shape[0], *piece.shape))
 
 
 def latents(arrived, full_width, gain_qlat, gain_kvlat):
@@ -137,10 +136,17 @@
         functools.partial(latent_kernel, full_width),
         in_specs=[pl.BlockSpec(memory_space=pltpu.VMEM)] * 3,
         out_specs=pl.BlockSpec(memory_space=pltpu.VMEM),
-        out_shape=jax.ShapeDtypeStruct((owners, 16, 128), BF16),
+        out_shape=jax.ShapeDtypeStruct(
+            (owners, arrived.shape[2] // 128, arrived.shape[1], 128), BF16
+        ),
         compiler_params=pltpu.CompilerParams(vmem_limit_bytes=8 * 1024 * 1024),
         cost_estimate=pl.CostEstimate(flops=10**5, bytes_accessed=10**6, transcendentals=0),
     )(arrived, gain_qlat[None], gain_kvlat[None])
+
+
+def two_terms(values):
+    first = values.astype(BF16).astype(F32)
+    return (first, (values - first).astype(BF16).astype(F32))
 
 
 def attend_kernel(
@@ -207,7 +213,7 @@
         for copy in coming(g):
             copy.start()
     for c in range(lat_rows.shape[1] // 128):
-        piece = packed[:, 2 * c : 2 * c + 2, :]
+        piece = packed[:, c]
         lat_rows[:, c * 128 : (c + 1) * 128] = piece.reshape(lat_rows.shape[0], 128)
     lane = lax.broadcasted_iota(jnp.int32, (1, lanes), 1)
     cosine = jnp.where(lane < rope_dim, query_turn[...], 0.0)
@@ -294,19 +300,18 @@
             )
             score = score * scale + bias[j]
             top = jnp.maximum(jnp.max(score, axis=1, keepdims=True), LOWEST)
+            top_terms = two_terms(top)
+            top = top_terms[0] + top_terms[1]
             weights = jnp.exp(score - top)
             total = jnp.sum(weights, axis=1, keepdims=True)
             numer[j] = jnp.dot(weights.astype(BF16), keys, preferred_element_type=F32)
             column = lax.broadcasted_iota(jnp.int32, (1, 128), 1)
             terms = jnp.zeros((heads * proposals, 128), F32)
-            for first, rest in ((0, top), (3, total)):
-                for k in range(3):
-                    term = rest.astype(BF16).astype(F32)
-                    terms = jnp.where(column == first + k, term, terms)
-                    rest = rest - term
-            extra = jnp.transpose(terms)[:8].astype(BF16)
+            for k, term in enumerate((*top_terms, *two_terms(total))):
+                terms = jnp.where(column == k, term, terms)
+            extra = jnp.transpose(terms)[:4].astype(BF16)
             for c in range(chunks):
-                sent[s * chunks + c, 2 * proposals :, :] = extra
+                sent[s * chunks + c, 8] = extra
 
         for h in range(heads):
             part = numer[:, pl.ds(h * proposals, proposals), :]
@@ -320,9 +325,8 @@
             for j in range(block):
                 sent[
                     (step * block + j) * chunks + h // 2,
-                    (h % 2) * proposals : (h % 2 + 1) * proposals,
-                    :,
-                ] = value[j * proposals : (j + 1) * proposals]
+                    (h % 2) * 4 : (h % 2) * 4 + 4,
+                ] = value[j * proposals : (j + 1) * proposals].reshape(4, 4, 128)
         leaving(step)[2].start()
 
     for g in range(seq_count // block):
@@ -342,7 +346,7 @@
     whole = pl.BlockSpec(memory_space=pltpu.VMEM)
     smem = pl.BlockSpec(memory_space=pltpu.SMEM)
     outside = pl.BlockSpec(memory_space=pltpu.HBM)
-    sent_shape = (seq_count * heads // 2, 2 * proposals + 8, w_value.shape[2])
+    sent_shape = (seq_count * heads // 2, 9, 4, w_value.shape[2])
     groups = seq_count // block
     return pl.pallas_call(
         attend_kernel,
@@ -478,13 +482,12 @@
     arrived = exchange(sent, KV).astype(F32)
     group = 2 * proposals
     chunk = lax.rem(lax.axis_index(KV), heads_here // 2)
-    extras = lax.dynamic_slice_in_dim(arrived[:, group:], chunk * group, group, 2)
-    maxima = extras[:, 0] + extras[:, 1] + extras[:, 2]
-    denominators = extras[:, 3] + extras[:, 4] + extras[:, 5]
+    extras = lax.dynamic_slice_in_dim(arrived[:, 8], chunk * group, group, 2)
+    maxima = extras[:, 0] + extras[:, 1]
     factor = jnp.exp(maxima - jnp.max(maxima, axis=0))
-    denom_all = jnp.sum(factor * denominators, axis=0)
-    values_all = jnp.sum(factor[..., None] * arrived[:, :group], axis=0)
-    head_share = (values_all / denom_all[:, None]).astype(BF16)
+    denom_all = jnp.sum(factor * (extras[:, 2] + extras[:, 3]), axis=0)
+    values_all = jnp.sum(factor.reshape(owners, 8, 4, 1) * arrived[:, :8], axis=0)
+    head_share = (values_all / denom_all.reshape(8, 4, 1)).astype(BF16).reshape(group, vhead)
     head_rows = from_everyone(head_share, KV)
     partial_out = project(head_rows.reshape(seq_count, heads_here, proposals, vhead), w_out.T)
     mixed = lax.all_gather(partial_out, "tp").sum(axis=0)

time: 147 us -> 146 us (level)
  the two profiles are of different devices: /device:TPU:4 before, /device:TPU:2 now
where the time goes in v6:
time: 146 us; the launch traced here: 145 us
  waiting for transfers between devices  59.9 us (41%)
  starting transfers between devices  31.6 us (22%)
  blocking collectives  31.2 us (21%)
  Pallas kernels  11.6 us (8%)
  other arithmetic  4.34 us (3%)
  local copies, waits for them, and re-layouts  4.22 us (3%)
    all_to_all x4, waiting for transfers between devices, exchange(): return lax.all_to_all(parts, axes, split_axis=0, concat_axis=0, tiled=True)  59.9 us
    all_to_all x4, starting transfers between devices, exchange(): return lax.all_to_all(parts, axes, split_axis=0, concat_axis=0, tiled=True)  31.6 us
    all_to_all x1, blocking collectives, exchange(): return lax.all_to_all(parts, axes, split_axis=0, concat_axis=0, tiled=True)  25.1 us
    pallas_call x1, Pallas kernels, attend(): pl.pallas_call(attend_kernel, in_specs=[smem, smem, *[whole] * 8, outside...  9.17 us
  transfers between devices with their start and end apart: 4, of which 4 were waited for; matrix products, arithmetic and copies ran while one was open for 4% of the time, Pallas kernels for 0%

profile of v6, /device:TPU:2, one launch (start us, length us, event | category | flops | bytes accessed | tf_op | source)
XLA Modules:
  0.0 145.2 jit_solution(4593023495684970267)
XLA Ops:
  0.7 1.1 shard_map.193
  1.8 1.9 %all_gather.12 = bf16[64,1152]{1,0:T(8,128)(2,1)S(1)} all-gather(bf16[32,1152]{1,0:T(8,128)(2,1)S(1)} %shard_map.193), channel_id=1, replica_groups=mesh['dp'=4,'kv_0'=8,'kv_1'=8,'tp'=2] {'tp'}, dimensions={0}, use_global_device_ids=true | all-gather | bytes 221184 | tf_op jit(solution)/shard_map/all_gather | solution.py:439
  4.0 1.0 reshape.121
  5.0 16.7 %all-to-all-start = ((f32[64,2,896]{2,1,0:T(2,128)}), f32[64,2,896]{2,1,0:T(2,128)S(1)}, u32[]{:S(2)}, u32[]{:S(2)}) async-start(f32[64,2,896]{2,1,0:T(2,128)} %reshape.121), calls=%async_computation | async-start | bytes 917504 | tf_op jit(solution)/shard_map/all_to_all | solution.py:22
  22.7 0.4 convert_reduce_fusion
  23.4 1.0 pad_maximum_fusion
  24.4 1.5 %copy.88.w_query = bf16[512,1024]{1,0:T(8,128)(2,1)S(1)} copy(bf16[512,1024]{0,1:T(8,128)(2,1)} %bitcast.46) | data formatting | bytes 2097152 | tf_op jit(solution)/shard_map/reshape | solution.py:466
  26.3 14.1 %all-to-all-done.arrived = f32[64,2,896]{2,1,0:T(2,128)S(1)} async-done(((f32[64,2,896]{2,1,0:T(2,128)}), f32[64,2,896]{2,1,0:T(2,128)S(1)}, u32[]{:S(2)}, u32[]{:S(2)}) %all-to-all-start) | async-done | bytes 458784 | tf_op jit(solution)/shard_map/all_to_all | solution.py:22
  40.4 1.1 shard_map.194
  41.5 4.9 %all-to-all-start.1 = ((bf16[64,7,2,128]{3,2,1,0:T(2,128)(2,1)}), bf16[64,7,2,128]{3,2,1,0:T(2,128)(2,1)S(1)}, u32[]{:S(2)}, u32[]{:S(2)}) async-start(bf16[64,7,2,128]{3,2,1,0:T(2,128)(2,1)} %shard_map.194), calls=%async_computation.1 | async-start | bytes 458752 | tf_op jit(solution)/shard_map/all_to_all | solution.py:22
  46.5 0.5 multiply_cosine_fusion
  47.2 13.0 %all-to-all-done.1 = bf16[64,7,2,128]{3,2,1,0:T(2,128)(2,1)S(1)} async-done(((bf16[64,7,2,128]{3,2,1,0:T(2,128)(2,1)}), bf16[64,7,2,128]{3,2,1,0:T(2,128)(2,1)S(1)}, u32[]{:S(2)}, u32[]{:S(2)}) %all-to-all-start.1) | async-done | bytes 229408 | tf_op jit(solution)/shard_map/all_to_all | solution.py:22
  60.3 2.1 %all_gather.13.packed = bf16[128,7,2,128]{3,2,1,0:T(2,128)(2,1)S(1)} all-gather(bf16[64,7,2,128]{3,2,1,0:T(2,128)(2,1)S(1)} %all-to-all-done.1), channel_id=1, replica_groups=mesh['dp'=4,'kv_0'=8,'kv_1'=8,'tp'=2] {'tp'}, dimensions={0}, use_global_device_ids=true | all-gather | bytes 688128 | tf_op jit(solution)/shard_map/all_gather | solution.py:446
  62.4 9.2 %shard_map.195 = (bf16[16,256,256]{2,1,0:T(8,128)(2,1)}, bf16[16,32,256]{2,1,0:T(8,128)(2,1)}, bf16[64,9,4,128]{3,2,1,0:T(4,128)(2,1)}) custom-call(s32[16]{0:T(128)S(1)} %add.101.starts, s32[1]{0:T(128)} %bitcast.base, bf16[128,7,2,128]{3,2,1,0:T(2,128)(2,1)S(1)} %all_gather.13.packed, f32[1,128]{1,0:T(1,128)S(1)} %maximum_bitcast_fusion.gain, ...), custom_call_target="tpu_custom_call" | custom-call | flops 1000000000 | bytes 8000000 | tf_op jit(solution)/shard_map/pallas_call | solution.py:351
  71.6 4.8 %all-to-all-start.2 = ((bf16[64,9,4,128]{3,2,1,0:T(4,128)(2,1)}), bf16[64,9,4,128]{3,2,1,0:T(4,128)(2,1)S(1)}, u32[]{:S(2)}, u32[]{:S(2)}) async-start(bf16[64,9,4,128]{3,2,1,0:T(4,128)(2,1)} %get-tuple-element.6), calls=%async_computation.2 | async-start | bytes 1179648 | tf_op jit(solution)/shard_map/all_to_all | solution.py:22
  76.4 20.5 %all-to-all-done.2 = bf16[64,9,4,128]{3,2,1,0:T(4,128)(2,1)S(1)} async-done(((bf16[64,9,4,128]{3,2,1,0:T(4,128)(2,1)}), bf16[64,9,4,128]{3,2,1,0:T(4,128)(2,1)S(1)}, u32[]{:S(2)}, u32[]{:S(2)}) %all-to-all-start.2) | async-done | bytes 589856 | tf_op jit(solution)/shard_map/all_to_all | solution.py:22
  97.9 0.7 fusion.3
  98.8 25.1 %all_to_all.25 = bf16[64,32,128]{2,1,0:T(8,128)(2,1)S(1)} all-to-all(bf16[64,32,128]{2,1,0:T(8,128)(2,1)S(1)} %broadcast_in_dim.22), channel_id=1, replica_groups=mesh['dp'=4,'kv_0'=8,'kv_1'=8,'tp'=2] {'kv_0','kv_1'}, dimensions={0} | all-to-all | bytes 1048576 | tf_op jit(solution)/shard_map/all_to_all | solution.py:22
  123.9 0.3 shard_map.196
  124.2 2.0 %all-gather = f32[512,32]{1,0:T(8,128)S(1)} all-gather(f32[256,32]{1,0:T(8,128)S(1)} %shard_map.196), channel_id=2, replica_groups=mesh['dp'=4,'kv_0'=8,'kv_1'=8,'tp'=2] {'tp'}, dimensions={0}, use_global_device_ids=true | all-gather | bytes 98304 | tf_op jit(solution)/shard_map/all_gather | solution.py:493
  126.3 0.7 broadcast_in_dim.46
  127.0 5.1 %all-to-all-start.4 = ((f32[64,1,256]{2,1,0:T(1,128)}), f32[64,1,256]{2,1,0:T(1,128)S(1)}, u32[]{:S(2)}, u32[]{:S(2)}) async-start(f32[64,1,256]{2,1,0:T(1,128)} %broadcast_in_dim.46), calls=%async_computation.4 | async-start | bytes 131072 | tf_op jit(solution)/shard_map/all_to_all | solution.py:22
  132.1 12.2 %all-to-all-done.4 = f32[64,1,256]{2,1,0:T(1,128)S(1)} async-done(((f32[64,1,256]{2,1,0:T(1,128)}), f32[64,1,256]{2,1,0:T(1,128)S(1)}, u32[]{:S(2)}, u32[]{:S(2)}) %all-to-all-start.4) | async-done | bytes 65568 | tf_op jit(solution)/shard_map/all_to_all | solution.py:22
  144.5 0.8 multiply_convert_fusion
  (63 shorter events, 3.3 us)
Async XLA Ops:
  0.6 21.1 %copy-start.4 = (bf16[512,8,96]{0,2,1:T(8,128)(2,1)S(1)}, bf16[512,8,96]{0,2,1:T(8,128)(2,1)}, u32[]{:S(2)}) copy-start(bf16[512,8,96]{0,2,1:T(8,128)(2,1)} %param.25) | copy-start | bytes 2359300
  3.9 17.9 %copy-start.7 = (f32[96]{0:T(128)S(1)}, f32[96]{0:T(128)}, u32[]{:S(2)}) copy-start(f32[96]{0:T(128)} %param.26) | copy-start | bytes 1156
  3.9 17.9 %copy-start.9 = (s32[16,16]{1,0:T(8,128)S(1)}, s32[16,16]{1,0:T(8,128)}, u32[]{:S(2)}) copy-start(s32[16,16]{1,0:T(8,128)} %param.33) | copy-start | bytes 3076
  5.0 18.1 %copy-start.10 = (s32[16]{0:T(128)S(1)}, s32[16]{0:T(128)}, u32[]{:S(2)}) copy-start(s32[16]{0:T(128)} %param.34) | copy-start | bytes 196
  5.0 18.1 %copy-start.11 = (s32[16]{0:T(128)S(1)}, s32[16]{0:T(128)}, u32[]{:S(2)}) copy-start(s32[16]{0:T(128)} %param.35) | copy-start | bytes 196
  5.0 18.3 %copy-start.5 = (bf16[256,8,128]{2,1,0:T(8,128)(2,1)S(1)}, bf16[256,8,128]{2,1,0:T(8,128)(2,1)}, u32[]{:S(2)}) copy-start(bf16[256,8,128]{2,1,0:T(8,128)(2,1)} %param.28) | copy-start | bytes 1572868
  5.0 35.4 %all-to-all-start = ((f32[64,2,896]{2,1,0:T(2,128)}), f32[64,2,896]{2,1,0:T(2,128)S(1)}, u32[]{:S(2)}, u32[]{:S(2)}) async-start(f32[64,2,896]{2,1,0:T(2,128)} %reshape.121), calls=%async_computation | async-start | bytes 917504 | tf_op jit(solution)/shard_map/all_to_all | solution.py:22
  21.7 1.6 %slice-start = ((bf16[512,8,96]{0,2,1:T(8,128)(2,1)}), bf16[512,8,32]{0,2,1:T(8,128)(2,1)S(1)}, s32[]{:S(2)}) async-start(bf16[512,8,96]{0,2,1:T(8,128)(2,1)} %param.25), calls=%async_computation.5 | async-start | bytes 524288 | tf_op jit(solution)/shard_map/split | solution.py:462
  21.7 1.6 %slice-start.1 = ((bf16[512,8,96]{0,2,1:T(8,128)(2,1)}), bf16[512,8,64]{0,2,1:T(8,128)(2,1)S(1)}, s32[]{:S(2)}) async-start(bf16[512,8,96]{0,2,1:T(8,128)(2,1)} %param.25), calls=%async_computation.6 | async-start | bytes 1048576 | tf_op jit(solution)/shard_map/split | solution.py:462
  23.4 17.1 %copy-start.2 = (f32[512]{0:T(512)S(1)}, f32[512]{0:T(512)}, u32[]{:S(2)}) copy-start(f32[512]{0:T(512)} %param.23) | copy-start | bytes 6148
  23.4 17.1 %copy-start.3 = (f32[256]{0:T(256)S(1)}, f32[256]{0:T(256)}, u32[]{:S(2)}) copy-start(f32[256]{0:T(256)} %param.24) | copy-start | bytes 3076
  24.4 1.5 %copy-start.6 = (bf16[256,8,64]{0,2,1:T(8,128)(2,1)S(1)}, bf16[256,8,64]{0,2,1:T(8,128)(2,1)}, u32[]{:S(2)}) copy-start(bf16[256,8,64]{0,2,1:T(8,128)(2,1)} %param.27) | copy-start | bytes 786436
  25.9 36.4 %copy-start = (bf16[16,32,256]{2,1,0:T(8,128)(2,1)S(1)}, bf16[16,32,256]{2,1,0:T(8,128)(2,1)}, u32[]{:S(2)}) copy-start(bf16[16,32,256]{2,1,0:T(8,128)(2,1)} %cache_rope.1) | copy-start | bytes 786436
  41.5 18.7 %all-to-all-start.1 = ((bf16[64,7,2,128]{3,2,1,0:T(2,128)(2,1)}), bf16[64,7,2,128]{3,2,1,0:T(2,128)(2,1)S(1)}, u32[]{:S(2)}, u32[]{:S(2)}) async-start(bf16[64,7,2,128]{3,2,1,0:T(2,128)(2,1)} %shard_map.194), calls=%async_computation.1 | async-start | bytes 458752 | tf_op jit(solution)/shard_map/all_to_all | solution.py:22
  71.6 25.3 %all-to-all-start.2 = ((bf16[64,9,4,128]{3,2,1,0:T(4,128)(2,1)}), bf16[64,9,4,128]{3,2,1,0:T(4,128)(2,1)S(1)}, u32[]{:S(2)}, u32[]{:S(2)}) async-start(bf16[64,9,4,128]{3,2,1,0:T(4,128)(2,1)} %get-tuple-element.6), calls=%async_computation.2 | async-start | bytes 1179648 | tf_op jit(solution)/shard_map/all_to_all | solution.py:22
  97.8 26.1 %copy-start.1 = (bf16[1024,32]{0,1:T(8,128)(2,1)S(1)}, bf16[1024,32]{0,1:T(8,128)(2,1)}, u32[]{:S(2)}) copy-start(bf16[1024,32]{0,1:T(8,128)(2,1)} %param.29) | copy-start | bytes 196612
  97.9 46.5 %copy-start.8 = (f32[16]{0:T(128)S(1)}, f32[16]{0:T(128)}, u32[]{:S(2)}) copy-start(f32[16]{0:T(128)} %param.30) | copy-start | bytes 196
  127.0 17.3 %all-to-all-start.4 = ((f32[64,1,256]{2,1,0:T(1,128)}), f32[64,1,256]{2,1,0:T(1,128)S(1)}, u32[]{:S(2)}, u32[]{:S(2)}) async-start(f32[64,1,256]{2,1,0:T(1,128)} %broadcast_in_dim.46), calls=%async_computation.4 | async-start | bytes 131072 | tf_op jit(solution)/shard_map/all_to_all | solution.py:22

commit v7 on v6

--- a/solution.py
+++ b/solution.py
@@ -202,11 +202,15 @@
 
     def leaving(g):
         part = pl.ds(g * block, block)
-        piece = pl.ds(g * block * chunks, block * chunks)
         return (
             pltpu.make_async_copy(lat.at[part], lat_out.at[part], lat_left.at[g]),
             pltpu.make_async_copy(rope.at[part], rope_out.at[part], rope_left.at[g]),
-            pltpu.make_async_copy(sent.at[piece], sent_out.at[piece], sent_left.at[g]),
+            *(
+                pltpu.make_async_copy(
+                    sent.at[part, c], sent_out.at[part, c], sent_left.at[g, c]
+                )
+                for c in range(chunks)
+            ),
         )
 
     for g in range(seq_count // block):
@@ -311,7 +315,7 @@
                 terms = jnp.where(column == k, term, terms)
             extra = jnp.transpose(terms)[:4].astype(BF16)
             for c in range(chunks):
-                sent[s * chunks + c, 8] = extra
+                sent[s, c, 8] = extra
 
         for h in range(heads):
             part = numer[:, pl.ds(h * proposals, proposals), :]
@@ -323,11 +327,11 @@
             )
             value = (both[: block * proposals] + both[block * proposals :]).astype(BF16)
             for j in range(block):
-                sent[
-                    (step * block + j) * chunks + h // 2,
-                    (h % 2) * 4 : (h % 2) * 4 + 4,
-                ] = value[j * proposals : (j + 1) * proposals].reshape(4, 4, 128)
-        leaving(step)[2].start()
+                sent[step * block + j, h // 2, (h % 2) * 4 : (h % 2) * 4 + 4] = value[
+                    j * proposals : (j + 1) * proposals
+                ].reshape(4, 4, 128)
+            if h % 2 == 1:
+                leaving(step)[2 + h // 2].start()
 
     for g in range(seq_count // block):
         for copy in leaving(g):
@@ -346,7 +350,7 @@
     whole = pl.BlockSpec(memory_space=pltpu.VMEM)
     smem = pl.BlockSpec(memory_space=pltpu.SMEM)
     outside = pl.BlockSpec(memory_space=pltpu.HBM)
-    sent_shape = (seq_count * heads // 2, 9, 4, w_value.shape[2])
+    sent_shape = (seq_count, heads // 2, 9, 4, w_value.shape[2])
     groups = seq_count // block
     return pl.pallas_call(
         attend_kernel,
@@ -367,7 +371,8 @@
             pltpu.VMEM(cache_lat.shape, BF16),
             pltpu.VMEM(cache_rope.shape, BF16),
             pltpu.VMEM(sent_shape, BF16),
-            *[pltpu.SemaphoreType.DMA((groups,))] * 5,
+            *[pltpu.SemaphoreType.DMA((groups,))] * 4,
+            pltpu.SemaphoreType.DMA((groups, heads // 2)),
         ],
         compiler_params=pltpu.CompilerParams(vmem_limit_bytes=50 * 1024 * 1024),
         cost_estimate=pl.CostEstimate(
@@ -479,7 +484,7 @@
         cache_rope,
         cache_lat,
     )
-    arrived = exchange(sent, KV).astype(F32)
+    arrived = exchange(sent.reshape(owners, *sent.shape[2:]), KV).astype(F32)
     group = 2 * proposals
     chunk = lax.rem(lax.axis_index(KV), heads_here // 2)
     extras = lax.dynamic_slice_in_dim(arrived[:, 8], chunk * group, group, 2)

time: 146 us -> 149 us (1.021)
  local copies, waits for them, and re-layouts: 4.22 us -> 5.97 us
  transfers between devices with their start and end apart: 4 -> 4, of which waited for: 4 -> 4; matrix products, arithmetic and copies ran while one was open for 4% -> 3% of each run, Pallas kernels for 0% -> 0%
where the time goes in v7:
time: 149 us; the launch traced here: 148 us
  waiting for transfers between devices  59.9 us (40%)
  starting transfers between devices  31.6 us (21%)
  blocking collectives  31.1 us (21%)
  Pallas kernels  11.6 us (8%)
  local copies, waits for them, and re-layouts  5.97 us (4%)
  other arithmetic  5.71 us (4%)
    all_to_all x4, waiting for transfers between devices, exchange(): return lax.all_to_all(parts, axes, split_axis=0, concat_axis=0, tiled=True)  59.9 us
    all_to_all x4, starting transfers between devices, exchange(): return lax.all_to_all(parts, axes, split_axis=0, concat_axis=0, tiled=True)  31.6 us
    all_to_all x1, blocking collectives, exchange(): return lax.all_to_all(parts, axes, split_axis=0, concat_axis=0, tiled=True)  25.1 us
    pallas_call x1, Pallas kernels, attend(): pl.pallas_call(attend_kernel, in_specs=[smem, smem, *[whole] * 8, outside...  9.19 us
  transfers between devices with their start and end apart: 4, of which 4 were waited for; matrix products, arithmetic and copies ran while one was open for 3% of the time, Pallas kernels for 0%

profile of v7, /device:TPU:2, one launch (start us, length us, event | category | flops | bytes accessed | tf_op | source)
XLA Modules:
  0.0 148.3 jit_solution(9959947403774217904)
XLA Ops:
  0.7 1.1 shard_map.193
  1.8 1.9 %all_gather.12 = bf16[64,1152]{1,0:T(8,128)(2,1)S(1)} all-gather(bf16[32,1152]{1,0:T(8,128)(2,1)S(1)} %shard_map.193), channel_id=1, replica_groups=mesh['dp'=4,'kv_0'=8,'kv_1'=8,'tp'=2] {'tp'}, dimensions={0}, use_global_device_ids=true | all-gather | bytes 221184 | tf_op jit(solution)/shard_map/all_gather | solution.py:444
  4.0 1.0 reshape.124
  5.0 16.7 %all-to-all-start = ((f32[64,2,896]{2,1,0:T(2,128)}), f32[64,2,896]{2,1,0:T(2,128)S(1)}, u32[]{:S(2)}, u32[]{:S(2)}) async-start(f32[64,2,896]{2,1,0:T(2,128)} %reshape.124), calls=%async_computation | async-start | bytes 917504 | tf_op jit(solution)/shard_map/all_to_all | solution.py:22
  23.4 1.0 pad_maximum_fusion
  24.4 1.5 %copy.83.w_query = bf16[512,1024]{1,0:T(8,128)(2,1)S(1)} copy(bf16[512,1024]{0,1:T(8,128)(2,1)} %bitcast.48) | data formatting | bytes 2097152 | tf_op jit(solution)/shard_map/reshape | solution.py:471
  26.3 14.1 %all-to-all-done.arrived = f32[64,2,896]{2,1,0:T(2,128)S(1)} async-done(((f32[64,2,896]{2,1,0:T(2,128)}), f32[64,2,896]{2,1,0:T(2,128)S(1)}, u32[]{:S(2)}, u32[]{:S(2)}) %all-to-all-start) | async-done | bytes 458784 | tf_op jit(solution)/shard_map/all_to_all | solution.py:22
  40.4 1.1 shard_map.194
  41.5 4.9 %all-to-all-start.1 = ((bf16[64,7,2,128]{3,2,1,0:T(2,128)(2,1)}), bf16[64,7,2,128]{3,2,1,0:T(2,128)(2,1)S(1)}, u32[]{:S(2)}, u32[]{:S(2)}) async-start(bf16[64,7,2,128]{3,2,1,0:T(2,128)(2,1)} %shard_map.194), calls=%async_computation.1 | async-start | bytes 458752 | tf_op jit(solution)/shard_map/all_to_all | solution.py:22
  47.2 13.0 %all-to-all-done.1 = bf16[64,7,2,128]{3,2,1,0:T(2,128)(2,1)S(1)} async-done(((bf16[64,7,2,128]{3,2,1,0:T(2,128)(2,1)}), bf16[64,7,2,128]{3,2,1,0:T(2,128)(2,1)S(1)}, u32[]{:S(2)}, u32[]{:S(2)}) %all-to-all-start.1) | async-done | bytes 229408 | tf_op jit(solution)/shard_map/all_to_all | solution.py:22
  60.3 2.1 %all_gather.13.packed = bf16[128,7,2,128]{3,2,1,0:T(2,128)(2,1)S(1)} all-gather(bf16[64,7,2,128]{3,2,1,0:T(2,128)(2,1)S(1)} %all-to-all-done.1), channel_id=1, replica_groups=mesh['dp'=4,'kv_0'=8,'kv_1'=8,'tp'=2] {'tp'}, dimensions={0}, use_global_device_ids=true | all-gather | bytes 688128 | tf_op jit(solution)/shard_map/all_gather | solution.py:451
  62.4 9.2 %shard_map.195 = (bf16[16,256,256]{2,1,0:T(8,128)(2,1)}, bf16[16,32,256]{2,1,0:T(8,128)(2,1)}, bf16[16,4,9,4,128]{4,3,2,1,0:T(4,128)(2,1)}) custom-call(s32[16]{0:T(128)S(1)} %add.101.starts, s32[1]{0:T(128)} %bitcast.base, bf16[128,7,2,128]{3,2,1,0:T(2,128)(2,1)S(1)} %all_gather.13.packed, f32[1,128]{1,0:T(1,128)S(1)} %maximum_bitcast_fusion.gain, ...), custom_call_target="tpu_custom_call" | custom-call | flops 1000000000 | bytes 8000000 | tf_op jit(solution)/shard_map/pallas_call | solution.py:355
  71.6 4.8 %all-to-all-start.2 = ((bf16[64,9,4,128]{3,2,1,0:T(4,128)(2,1)}), bf16[64,9,4,128]{3,2,1,0:T(4,128)(2,1)S(1)}, u32[]{:S(2)}, u32[]{:S(2)}) async-start(bf16[64,9,4,128]{3,2,1,0:T(4,128)(2,1)} %bitcast.50), calls=%async_computation.2 | async-start | bytes 1179648 | tf_op jit(solution)/shard_map/all_to_all | solution.py:22
  76.4 20.5 %all-to-all-done.2 = bf16[64,9,4,128]{3,2,1,0:T(4,128)(2,1)S(1)} async-done(((bf16[64,9,4,128]{3,2,1,0:T(4,128)(2,1)}), bf16[64,9,4,128]{3,2,1,0:T(4,128)(2,1)S(1)}, u32[]{:S(2)}, u32[]{:S(2)}) %all-to-all-start.2) | async-done | bytes 589856 | tf_op jit(solution)/shard_map/all_to_all | solution.py:22
  96.9 1.1 copy.75
  98.0 1.0 copy-done.4
  99.0 1.5 %convert_element_type.87 = f32[64,9,4,128]{0,3,2,1:T(8,128)S(1)} convert(bf16[64,9,4,128]{0,3,2,1:T(8,128)(2,1)} %copy-done.4) | non-fusion elementwise | flops 294912 | bytes 1769472 | tf_op jit(solution)/shard_map/convert_element_type | solution.py:487
  101.1 0.6 fusion
  101.9 25.1 %all_to_all.25 = bf16[64,32,128]{2,1,0:T(8,128)(2,1)S(1)} all-to-all(bf16[64,32,128]{2,1,0:T(8,128)(2,1)S(1)} %broadcast_in_dim.22), channel_id=1, replica_groups=mesh['dp'=4,'kv_0'=8,'kv_1'=8,'tp'=2] {'kv_0','kv_1'}, dimensions={0} | all-to-all | bytes 1048576 | tf_op jit(solution)/shard_map/all_to_all | solution.py:22
  127.3 2.0 %all-gather = f32[512,32]{1,0:T(8,128)S(1)} all-gather(f32[256,32]{1,0:T(8,128)S(1)} %shard_map.196), channel_id=2, replica_groups=mesh['dp'=4,'kv_0'=8,'kv_1'=8,'tp'=2] {'tp'}, dimensions={0}, use_global_device_ids=true | all-gather | bytes 98304 | tf_op jit(solution)/shard_map/all_gather | solution.py:498
  129.4 0.7 broadcast_in_dim.46
  130.1 5.1 %all-to-all-start.4 = ((f32[64,1,256]{2,1,0:T(1,128)}), f32[64,1,256]{2,1,0:T(1,128)S(1)}, u32[]{:S(2)}, u32[]{:S(2)}) async-start(f32[64,1,256]{2,1,0:T(1,128)} %broadcast_in_dim.46), calls=%async_computation.4 | async-start | bytes 131072 | tf_op jit(solution)/shard_map/all_to_all | solution.py:22
  135.2 12.2 %all-to-all-done.4 = f32[64,1,256]{2,1,0:T(1,128)S(1)} async-done(((f32[64,1,256]{2,1,0:T(1,128)}), f32[64,1,256]{2,1,0:T(1,128)S(1)}, u32[]{:S(2)}, u32[]{:S(2)}) %all-to-all-start.4) | async-done | bytes 65568 | tf_op jit(solution)/shard_map/all_to_all | solution.py:22
  147.6 0.8 multiply_convert_fusion
  (64 shorter events, 4.0 us)
Async XLA Ops:
  0.6 21.1 %copy-start.5 = (bf16[512,8,96]{0,2,1:T(8,128)(2,1)S(1)}, bf16[512,8,96]{0,2,1:T(8,128)(2,1)}, u32[]{:S(2)}) copy-start(bf16[512,8,96]{0,2,1:T(8,128)(2,1)} %param.25) | copy-start | bytes 2359300
  3.9 17.9 %copy-start.8 = (f32[96]{0:T(128)S(1)}, f32[96]{0:T(128)}, u32[]{:S(2)}) copy-start(f32[96]{0:T(128)} %param.26) | copy-start | bytes 1156
  3.9 17.9 %copy-start.10 = (s32[16,16]{1,0:T(8,128)S(1)}, s32[16,16]{1,0:T(8,128)}, u32[]{:S(2)}) copy-start(s32[16,16]{1,0:T(8,128)} %param.33) | copy-start | bytes 3076
  5.0 18.1 %copy-start.11 = (s32[16]{0:T(128)S(1)}, s32[16]{0:T(128)}, u32[]{:S(2)}) copy-start(s32[16]{0:T(128)} %param.34) | copy-start | bytes 196
  5.0 18.1 %copy-start.12 = (s32[16]{0:T(128)S(1)}, s32[16]{0:T(128)}, u32[]{:S(2)}) copy-start(s32[16]{0:T(128)} %param.35) | copy-start | bytes 196
  5.0 18.3 %copy-start.6 = (bf16[256,8,128]{2,1,0:T(8,128)(2,1)S(1)}, bf16[256,8,128]{2,1,0:T(8,128)(2,1)}, u32[]{:S(2)}) copy-start(bf16[256,8,128]{2,1,0:T(8,128)(2,1)} %param.28) | copy-start | bytes 1572868
  5.0 35.4 %all-to-all-start = ((f32[64,2,896]{2,1,0:T(2,128)}), f32[64,2,896]{2,1,0:T(2,128)S(1)}, u32[]{:S(2)}, u32[]{:S(2)}) async-start(f32[64,2,896]{2,1,0:T(2,128)} %reshape.124), calls=%async_computation | async-start | bytes 917504 | tf_op jit(solution)/shard_map/all_to_all | solution.py:22
  21.7 1.6 %slice-start = ((bf16[512,8,96]{0,2,1:T(8,128)(2,1)}), bf16[512,8,32]{0,2,1:T(8,128)(2,1)S(1)}, s32[]{:S(2)}) async-start(bf16[512,8,96]{0,2,1:T(8,128)(2,1)} %param.25), calls=%async_computation.5 | async-start | bytes 524288 | tf_op jit(solution)/shard_map/split | solution.py:467
  21.8 1.6 %slice-start.1 = ((bf16[512,8,96]{0,2,1:T(8,128)(2,1)}), bf16[512,8,64]{0,2,1:T(8,128)(2,1)S(1)}, s32[]{:S(2)}) async-start(bf16[512,8,96]{0,2,1:T(8,128)(2,1)} %param.25), calls=%async_computation.6 | async-start | bytes 1048576 | tf_op jit(solution)/shard_map/split | solution.py:467
  23.4 17.1 %copy-start.2 = (f32[512]{0:T(512)S(1)}, f32[512]{0:T(512)}, u32[]{:S(2)}) copy-start(f32[512]{0:T(512)} %param.23) | copy-start | bytes 6148
  23.4 17.1 %copy-start.3 = (f32[256]{0:T(256)S(1)}, f32[256]{0:T(256)}, u32[]{:S(2)}) copy-start(f32[256]{0:T(256)} %param.24) | copy-start | bytes 3076
  24.4 1.5 %copy-start.7 = (bf16[256,8,64]{0,2,1:T(8,128)(2,1)S(1)}, bf16[256,8,64]{0,2,1:T(8,128)(2,1)}, u32[]{:S(2)}) copy-start(bf16[256,8,64]{0,2,1:T(8,128)(2,1)} %param.27) | copy-start | bytes 786436
  26.0 36.4 %copy-start = (bf16[16,32,256]{2,1,0:T(8,128)(2,1)S(1)}, bf16[16,32,256]{2,1,0:T(8,128)(2,1)}, u32[]{:S(2)}) copy-start(bf16[16,32,256]{2,1,0:T(8,128)(2,1)} %cache_rope.1) | copy-start | bytes 786436
  41.5 18.7 %all-to-all-start.1 = ((bf16[64,7,2,128]{3,2,1,0:T(2,128)(2,1)}), bf16[64,7,2,128]{3,2,1,0:T(2,128)(2,1)S(1)}, u32[]{:S(2)}, u32[]{:S(2)}) async-start(bf16[64,7,2,128]{3,2,1,0:T(2,128)(2,1)} %shard_map.194), calls=%async_computation.1 | async-start | bytes 458752 | tf_op jit(solution)/shard_map/all_to_all | solution.py:22
  71.6 25.3 %all-to-all-start.2 = ((bf16[64,9,4,128]{3,2,1,0:T(4,128)(2,1)}), bf16[64,9,4,128]{3,2,1,0:T(4,128)(2,1)S(1)}, u32[]{:S(2)}, u32[]{:S(2)}) async-start(bf16[64,9,4,128]{3,2,1,0:T(4,128)(2,1)} %bitcast.50), calls=%async_computation.2 | async-start | bytes 1179648 | tf_op jit(solution)/shard_map/all_to_all | solution.py:22
  98.0 1.0 copy-start.4
  100.6 26.4 %copy-start.1 = (bf16[1024,32]{0,1:T(8,128)(2,1)S(1)}, bf16[1024,32]{0,1:T(8,128)(2,1)}, u32[]{:S(2)}) copy-start(bf16[1024,32]{0,1:T(8,128)(2,1)} %param.29) | copy-start | bytes 196612
  101.7 45.8 %copy-start.9 = (f32[16]{0:T(128)S(1)}, f32[16]{0:T(128)}, u32[]{:S(2)}) copy-start(f32[16]{0:T(128)} %param.30) | copy-start | bytes 196
  130.1 17.3 %all-to-all-start.4 = ((f32[64,1,256]{2,1,0:T(1,128)}), f32[64,1,256]{2,1,0:T(1,128)S(1)}, u32[]{:S(2)}, u32[]{:S(2)}) async-start(f32[64,1,256]{2,1,0:T(1,128)} %broadcast_in_dim.46), calls=%async_computation.4 | async-start | bytes 131072 | tf_op jit(solution)/shard_map/all_to_all | solution.py:22
